TPU v7x, 1024 devices: a 2x16x16 block of a 4x16x16 slice. The times are simulated.
1024 devices in a mesh: grp: 2 (over x), fs: 16 (over z), tp: 32 (over y, core).
Axes of the slice: x: 2, y: 16, z: 16, core: 2. Of those that a mesh axis runs over, the one named last changes fastest.
The devices are a block of a 4x16x16 slice.
Arguments:
- tokens: bfloat16 [8192, 2048], P(('grp', 'fs'), 'tp'), parts along dimension 0, may hold values from -12 to 12
- gain_first: float32 [2048], P('tp'), may hold values from 0.1 to 1.9
- gate_first: float32 [2048, 5632], P('fs', 'tp'), may hold values from -0.125 to 0.125
- gate_scale_first: float32 [5632], P('tp'), may hold values from 0.5 to 2
- up_first: float32 [2048, 5632], P('fs', 'tp'), may hold values from -0.125 to 0.125
- up_scale_first: float32 [5632], P('tp'), may hold values from 0.5 to 2
- down_first: float32 [5632, 2048], P('tp', 'fs'), may hold values from -0.078125 to 0.078125
- down_scale_first: float32 [2048], P('tp'), may hold values from 0.5 to 2
- gain_second: float32 [2048], P('tp'), may hold values from 0.1 to 1.9
- gate_second: float32 [2048, 5632], P('fs', 'tp'), may hold values from -0.125 to 0.125
- gate_scale_second: float32 [5632], P('tp'), may hold values from 0.5 to 2
- up_second: float32 [2048, 5632], P('fs', 'tp'), may hold values from -0.125 to 0.125
- up_scale_second: float32 [5632], P('tp'), may hold values from 0.5 to 2
- down_second: float32 [5632, 2048], P('tp', 'fs'), may hold values from -0.078125 to 0.078125
- down_scale_second: float32 [2048], P('tp'), may hold values from 0.5 to 2
Outputs:
- stream_out: bfloat16 [8192, 2048], P(('grp', 'fs'), 'tp'), parts along dimension 0
There are 2 independent parts, one for each index of `grp`. A program takes and returns all parts, laid end to end along the dimension named above; an argument that names none is the same for every part. Nothing has to cross between parts.
All inputs are finite; a program needn't handle non-finite values.
Results may differ from a plain program's by a relative error of at most 0.028.
Values may be sent and summed in bfloat16 or wider, within the bound.
No kernel may reach another device: no remote copies, remote signals or barrier semaphores. Data moves between devices by JAX's collectives and lax.ppermute only.
A program may use at most 32 MiB of HBM per device.

v0:
```python
import jax
import jax.numpy as jnp
from jax import lax
from jax.sharding import PartitionSpec as P

epsilon = 1e-06


def sent_to_all(value, axis):
    devices = lax.axis_size(axis)
    return lax.all_to_all(
        jnp.broadcast_to(value[None], (devices, *value.shape)), axis, 0, 0, tiled=True
    )


def taken_together(value, axis):
    everything = sent_to_all(value, axis)
    return jnp.sum(everything, axis=0)


def joined_along(parts, dim):
    lengths = list(parts.shape[1:])
    lengths[dim] *= parts.shape[0]
    return jnp.moveaxis(parts, 0, dim).reshape(lengths)


def gather_directly(value, axis, dim):
    return joined_along(sent_to_all(value, axis), dim)


def side_by_side(arrays, axis, dim, along):
    widths = [a.shape[along] for a in arrays]
    both = jnp.concatenate(arrays, axis=along)
    out = lax.all_gather(both, axis, axis=dim, tiled=True)
    return tuple(jnp.split(out, [sum(widths[:k]) for k in range(1, len(widths))], axis=along))


def in_blocks(value, dim, devices):
    lengths = value.shape
    parts = value.reshape(*lengths[:dim], devices, lengths[dim] // devices, *lengths[dim + 1 :])
    return jnp.moveaxis(parts, dim, 0)


def sent_and_summed(value, axis, dim):
    parts = in_blocks(value, dim, lax.axis_size(axis))
    arrived = lax.all_to_all(parts, axis, split_axis=0, concat_axis=0, tiled=True)
    return arrived.astype(jnp.float32).sum(axis=0)


def turned_gather(arrays, axis, dims):
    turned = [jnp.moveaxis(a, dim, 0) for a, dim in zip(arrays, dims)]
    widths = [t[0].size for t in turned]
    both = jnp.concatenate([t.reshape(-1, w) for t, w in zip(turned, widths)], axis=1)
    out = lax.all_gather(both, axis, axis=0, tiled=True)
    parts = jnp.split(out, [sum(widths[:k]) for k in range(1, len(widths))], axis=1)
    return tuple(
        (
            jnp.moveaxis(b.reshape(-1, *t.shape[1:]), 0, dim)
            for b, t, dim in zip(parts, turned, dims)
        )
    )


def normalize(stream, gain):
    values = stream.astype(jnp.float32)
    totals = taken_together(jnp.sum(values * values, axis=1), "tp")
    width = values.shape[1] * lax.axis_size("tp")
    normed = (values * lax.rsqrt(totals / width + epsilon)[:, None] * gain).astype(jnp.bfloat16)
    whole = gather_directly(normed, "tp", 1)
    return (values, whole)


def add_rows(whole, piece):
    return jnp.dot(whole, piece, preferred_element_type=jnp.float32)


def collect_gate_up(whole, gate_w, up_w):
    gate_bf = gate_w.astype(jnp.bfloat16)
    up_bf = up_w.astype(jnp.bfloat16)
    pieces = side_by_side((gate_bf, up_bf), "fs", 0, 1)
    gate = add_rows(whole, pieces[0])
    up = add_rows(whole, pieces[1])
    return (gate, up)


def collect_down(hidden, down_w):
    return jnp.dot(
        hidden,
        gather_directly(down_w.astype(jnp.bfloat16), "fs", 1),
        preferred_element_type=jnp.float32,
    )


def finish(values, gate, up, gate_s, up_s, down_s, down_fn):
    hidden = (jax.nn.silu(gate * gate_s) * (up * up_s)).astype(jnp.bfloat16)
    terms = down_fn(hidden)
    summed = sent_and_summed(terms.astype(jnp.bfloat16), "tp", 1)
    return (values + 0.5 * summed * down_s).astype(jnp.bfloat16)


def body(
    tokens,
    gain_first,
    gate_first,
    gate_scale_first,
    up_first,
    up_scale_first,
    down_first,
    down_scale_first,
    gain_second,
    gate_second,
    gate_scale_second,
    up_second,
    up_scale_second,
    down_second,
    down_scale_second,
):
    gate_full, up_full, down_full = turned_gather(
        (
            gate_second.astype(jnp.bfloat16),
            up_second.astype(jnp.bfloat16),
            down_second.astype(jnp.bfloat16),
        ),
        "fs",
        (0, 0, 1),
    )
    values, whole = normalize(tokens, gain_first)
    gate, up = collect_gate_up(whole, gate_first, up_first)
    middle = finish(
        values,
        gate,
        up,
        gate_scale_first,
        up_scale_first,
        down_scale_first,
        lambda hidden: collect_down(hidden, down_first),
    )
    values, whole = normalize(middle, gain_second)
    gate = jnp.dot(whole, gate_full, preferred_element_type=jnp.float32)
    up = jnp.dot(whole, up_full, preferred_element_type=jnp.float32)
    return finish(
        values,
        gate,
        up,
        gate_scale_second,
        up_scale_second,
        down_scale_second,
        lambda hidden: jnp.dot(hidden, down_full, preferred_element_type=jnp.float32),
    )


def solution(mesh):
    in_specs = (
        P(("grp", "fs"), "tp"),
        P("tp"),
        P("fs", "tp"),
        P("tp"),
        P("fs", "tp"),
        P("tp"),
        P("tp", "fs"),
        P("tp"),
        P("tp"),
        P("fs", "tp"),
        P("tp"),
        P("fs", "tp"),
        P("tp"),
        P("tp", "fs"),
        P("tp"),
    )
    out_specs = P(("grp", "fs"), "tp")
    return jax.shard_map(body, mesh=mesh, in_specs=in_specs, out_specs=out_specs, check_vma=False)
```

profile of v0, /device:TPU:5, one launch (start us, length us, event | category | flops | bytes accessed | tf_op | source)
XLA Modules:
  0.0 485.3 jit_solution(4008564104469090598)
XLA Ops:
  6.6 0.8 fusion.27
  7.4 98.5 %all_to_all.37 = f32[32,1,256]{2,1,0:T(1,128)S(1)} all-to-all(f32[32,1,256]{2,1,0:T(1,128)S(1)} %broadcast_in_dim.10), channel_id=1, replica_groups=mesh['grp'=2,'fs'=16,'tp'=32] {'tp'}, dimensions={0} | all-to-all | bytes 65536 | tf_op jit(solution)/shard_map/all_to_all | solution.py:11
  105.9 0.1 reduce_sum.55
  105.9 0.8 fusion.29
  106.8 1.1 broadcast_in_dim.11
  107.9 5.0 %all-to-all-start.1 = ((bf16[32,256,64]{1,2,0:T(8,128)(2,1)}), bf16[32,256,64]{1,2,0:T(8,128)(2,1)S(1)}, u32[]{:S(2)}, u32[]{:S(2)}) async-start(bf16[32,256,64]{1,2,0:T(8,128)(2,1)} %broadcast_in_dim.11), calls=%async_computation.1 | async-start | bytes 2097152 | tf_op jit(solution)/shard_map/all_to_all | solution.py:11
  112.9 0.1 all-gather.3.cloned.1.call-start
  113.0 0.6 pad_maximum_fusion.1
  113.6 0.1 all-gather.3.cloned.1.call-update
  113.7 0.0 copy-start.9
  113.7 54.8 %all-to-all-done.1 = bf16[32,256,64]{1,2,0:T(8,128)(2,1)S(1)} async-done(((bf16[32,256,64]{1,2,0:T(8,128)(2,1)}), bf16[32,256,64]{1,2,0:T(8,128)(2,1)S(1)}, u32[]{:S(2)}, u32[]{:S(2)}) %all-to-all-start.1) | async-done | bytes 1048608 | tf_op jit(solution)/shard_map/all_to_all | solution.py:11
  168.5 1.0 broadcast_in_dim.12
  169.4 12.0 %all-to-all-start.2 = ((bf16[16,176,128]{2,1,0:T(8,128)(2,1)}), bf16[16,176,128]{2,1,0:T(8,128)(2,1)S(1)}, u32[]{:S(2)}, u32[]{:S(2)}) async-start(bf16[16,176,128]{2,1,0:T(8,128)(2,1)} %broadcast_in_dim.12), calls=%async_computation.2 | async-start | bytes 1441792 | tf_op jit(solution)/shard_map/all_to_all | solution.py:11
  181.5 16.1 %all-gather.3.cloned.1.call-done = bf16[2048,352]{0,1:T(8,128)(2,1)} async-done(((bf16[128,352]{0,1:T(8,128)(2,1)}), bf16[2048,352]{0,1:T(8,128)(2,1)}) %all-gather.3.cloned.1.call-update) | async-done | bytes 1441808 | tf_op jit(solution)/shard_map/all_gather | solution.py:34
  197.6 0.0 copy-done.8
  197.6 1.5 convolution_multiply_fusion.3
  199.1 15.7 %all-to-all-done.2 = bf16[16,176,128]{2,1,0:T(8,128)(2,1)S(1)} async-done(((bf16[16,176,128]{2,1,0:T(8,128)(2,1)}), bf16[16,176,128]{2,1,0:T(8,128)(2,1)S(1)}, u32[]{:S(2)}, u32[]{:S(2)}) %all-to-all-start.2) | async-done | bytes 720928 | tf_op jit(solution)/shard_map/all_to_all | solution.py:11
  214.8 2.3 convolution_convert_fusion.1
  217.1 0.0 copy-start.4
  217.1 0.0 copy-start.5
  217.1 0.0 copy-start.12
  217.1 1.3 copy.28
  218.4 19.6 %all-to-all-start.3 = ((bf16[32,256,64]{1,2,0:T(8,128)(2,1)}), bf16[32,256,64]{1,2,0:T(8,128)(2,1)S(1)}, u32[]{:S(2)}, u32[]{:S(2)}) async-start(bf16[32,256,64]{1,2,0:T(8,128)(2,1)} %bitcast.5), calls=%async_computation.3 | async-start | bytes 2097152 | tf_op jit(solution)/shard_map/all_to_all | solution.py:46
  238.1 55.4 %all-to-all-done.3 = bf16[32,256,64]{1,2,0:T(8,128)(2,1)S(1)} async-done(((bf16[32,256,64]{1,2,0:T(8,128)(2,1)}), bf16[32,256,64]{1,2,0:T(8,128)(2,1)S(1)}, u32[]{:S(2)}, u32[]{:S(2)}) %all-to-all-start.3) | async-done | bytes 1048608 | tf_op jit(solution)/shard_map/all_to_all | solution.py:46
  293.6 0.2 convert_reduce_fusion.1
  293.7 0.0 copy-start.10
  293.7 0.1 fusion.31
  293.8 0.6 broadcast_in_dim.13
  294.5 4.3 all-to-all-start.4
  298.8 12.1 %all-to-all-done.4 = f32[32,1,256]{2,1,0:T(1,128)S(1)} async-done(((f32[32,1,256]{2,1,0:T(1,128)}), f32[32,1,256]{2,1,0:T(1,128)S(1)}, u32[]{:S(2)}, u32[]{:S(2)}) %all-to-all-start.4) | async-done | bytes 32800 | tf_op jit(solution)/shard_map/all_to_all | solution.py:11
  310.9 0.1 reduce_sum.58
  310.9 0.0 copy-done.7
  311.0 0.1 fusion.33
  311.0 1.1 broadcast_in_dim.14
  312.1 5.0 %all-to-all-start.5 = ((bf16[32,256,64]{1,2,0:T(8,128)(2,1)}), bf16[32,256,64]{1,2,0:T(8,128)(2,1)S(1)}, u32[]{:S(2)}, u32[]{:S(2)}) async-start(bf16[32,256,64]{1,2,0:T(8,128)(2,1)} %broadcast_in_dim.14), calls=%async_computation.5 | async-start | bytes 2097152 | tf_op jit(solution)/shard_map/all_to_all | solution.py:11
  317.1 0.1 all-gather.5.cloned.1.call-start
  317.2 0.7 pad_maximum_fusion
  317.8 0.1 all-gather.5.cloned.1.call-update
  317.9 76.5 %all-gather.5.cloned.1.call-done = bf16[2048,528]{0,1:T(8,128)(2,1)} async-done(((bf16[128,528]{0,1:T(8,128)(2,1)}), bf16[2048,528]{0,1:T(8,128)(2,1)}) %all-gather.5.cloned.1.call-update) | async-done | bytes 2162704 | tf_op jit(solution)/shard_map/all_gather | solution.py:54
  394.4 0.0 all-to-all-done.5
  394.4 1.5 convolution_multiply_fusion.1
  395.9 2.5 convolution_convert_fusion
  398.4 0.0 copy-start.13
  398.4 1.3 copy.30
  399.7 22.4 %all-to-all-start.6 = ((bf16[32,256,64]{1,2,0:T(8,128)(2,1)}), bf16[32,256,64]{1,2,0:T(8,128)(2,1)S(1)}, u32[]{:S(2)}, u32[]{:S(2)}) async-start(bf16[32,256,64]{1,2,0:T(8,128)(2,1)} %bitcast.11), calls=%async_computation.6 | async-start | bytes 2097152 | tf_op jit(solution)/shard_map/all_to_all | solution.py:46
  422.2 55.5 %all-to-all-done.6 = bf16[32,256,64]{1,2,0:T(8,128)(2,1)S(1)} async-done(((bf16[32,256,64]{1,2,0:T(8,128)(2,1)}), bf16[32,256,64]{1,2,0:T(8,128)(2,1)S(1)}, u32[]{:S(2)}, u32[]{:S(2)}) %all-to-all-start.6) | async-done | bytes 1048608 | tf_op jit(solution)/shard_map/all_to_all | solution.py:46
  477.6 0.2 convert_reduce_fusion
  477.8 0.7 fusion.34
  (31 shorter events, 0.1 us)
Async XLA Ops:
  6.5 106.4 %copy-start.1 = (f32[128,176]{0,1:T(8,128)S(1)}, f32[128,176]{0,1:T(8,128)}, u32[]{:S(2)}) copy-start(f32[128,176]{0,1:T(8,128)} %param.17) | copy-start | bytes 270340
  6.5 106.4 %copy-start.2 = (f32[128,176]{0,1:T(8,128)S(1)}, f32[128,176]{0,1:T(8,128)}, u32[]{:S(2)}) copy-start(f32[128,176]{0,1:T(8,128)} %param.19) | copy-start | bytes 270340
  6.6 107.1 %copy-start.3 = (f32[176,128]{1,0:T(8,128)S(1)}, f32[176,128]{1,0:T(8,128)}, u32[]{:S(2)}) copy-start(f32[176,128]{1,0:T(8,128)} %param.21) | copy-start | bytes 270340
  107.9 89.7 %copy-start.8 = (f32[176]{0:T(256)S(1)}, f32[176]{0:T(256)}, u32[]{:S(2)}) copy-start(f32[176]{0:T(256)} %param.18) | copy-start | bytes 2116
  107.9 60.6 %all-to-all-start.1 = ((bf16[32,256,64]{1,2,0:T(8,128)(2,1)}), bf16[32,256,64]{1,2,0:T(8,128)(2,1)S(1)}, u32[]{:S(2)}, u32[]{:S(2)}) async-start(bf16[32,256,64]{1,2,0:T(8,128)(2,1)} %broadcast_in_dim.11), calls=%async_computation.1 | async-start | bytes 2097152 | tf_op jit(solution)/shard_map/all_to_all | solution.py:11
  112.9 84.7 %all-gather.3.cloned.1.call-start = ((), (), s32[]{:S(2)}) async-start(), calls=%async_computation.7 | async-start | bytes 1531904 | tf_op jit(solution)/shard_map/all_gather | solution.py:34
  113.7 101.1 %copy-start.9 = (f32[176]{0:T(256)S(1)}, f32[176]{0:T(256)}, u32[]{:S(2)}) copy-start(f32[176]{0:T(256)} %param.20) | copy-start | bytes 2116
  169.4 45.3 %all-to-all-start.2 = ((bf16[16,176,128]{2,1,0:T(8,128)(2,1)}), bf16[16,176,128]{2,1,0:T(8,128)(2,1)S(1)}, u32[]{:S(2)}, u32[]{:S(2)}) async-start(bf16[16,176,128]{2,1,0:T(8,128)(2,1)} %broadcast_in_dim.12), calls=%async_computation.2 | async-start | bytes 1441792 | tf_op jit(solution)/shard_map/all_to_all | solution.py:11
  217.1 21.0 %copy-start.4 = (f32[128,176]{0,1:T(8,128)S(1)}, f32[128,176]{0,1:T(8,128)}, u32[]{:S(2)}) copy-start(f32[128,176]{0,1:T(8,128)} %param.24) | copy-start | bytes 270340
  217.1 21.0 %copy-start.5 = (f32[128,176]{0,1:T(8,128)S(1)}, f32[128,176]{0,1:T(8,128)}, u32[]{:S(2)}) copy-start(f32[128,176]{0,1:T(8,128)} %param.26) | copy-start | bytes 270340
  217.1 21.0 %copy-start.12 = (f32[64]{0:T(128)S(1)}, f32[64]{0:T(128)}, u32[]{:S(2)}) copy-start(f32[64]{0:T(128)} %param.22) | copy-start | bytes 772
  218.4 75.3 %copy-start = (bf16[256,64]{0,1:T(8,128)(2,1)S(1)}, bf16[256,64]{0,1:T(8,128)(2,1)}, u32[]{:S(2)}) copy-start(bf16[256,64]{0,1:T(8,128)(2,1)} %param.15) | copy-start | bytes 98308
  218.4 80.3 %copy-start.6 = (f32[176,128]{1,0:T(8,128)S(1)}, f32[176,128]{1,0:T(8,128)}, u32[]{:S(2)}) copy-start(f32[176,128]{1,0:T(8,128)} %param.28) | copy-start | bytes 270340
  218.4 92.5 %copy-start.7 = (f32[64]{0:T(128)S(1)}, f32[64]{0:T(128)}, u32[]{:S(2)}) copy-start(f32[64]{0:T(128)} %param.23) | copy-start | bytes 772
  218.4 75.1 %all-to-all-start.3 = ((bf16[32,256,64]{1,2,0:T(8,128)(2,1)}), bf16[32,256,64]{1,2,0:T(8,128)(2,1)S(1)}, u32[]{:S(2)}, u32[]{:S(2)}) async-start(bf16[32,256,64]{1,2,0:T(8,128)(2,1)} %bitcast.5), calls=%async_computation.3 | async-start | bytes 2097152 | tf_op jit(solution)/shard_map/all_to_all | solution.py:46
  293.7 100.7 %copy-start.10 = (f32[176]{0:T(256)S(1)}, f32[176]{0:T(256)}, u32[]{:S(2)}) copy-start(f32[176]{0:T(256)} %param.25) | copy-start | bytes 2116
  294.5 16.4 %all-to-all-start.4 = ((f32[32,1,256]{2,1,0:T(1,128)}), f32[32,1,256]{2,1,0:T(1,128)S(1)}, u32[]{:S(2)}, u32[]{:S(2)}) async-start(f32[32,1,256]{2,1,0:T(1,128)} %broadcast_in_dim.13), calls=%async_computation.4 | async-start | bytes 65536 | tf_op jit(solution)/shard_map/all_to_all | solution.py:11
  312.1 83.8 %copy-start.11 = (f32[176]{0:T(256)S(1)}, f32[176]{0:T(256)}, u32[]{:S(2)}) copy-start(f32[176]{0:T(256)} %param.27) | copy-start | bytes 2116
  312.1 82.3 %all-to-all-start.5 = ((bf16[32,256,64]{1,2,0:T(8,128)(2,1)}), bf16[32,256,64]{1,2,0:T(8,128)(2,1)S(1)}, u32[]{:S(2)}, u32[]{:S(2)}) async-start(bf16[32,256,64]{1,2,0:T(8,128)(2,1)} %broadcast_in_dim.14), calls=%async_computation.5 | async-start | bytes 2097152 | tf_op jit(solution)/shard_map/all_to_all | solution.py:11
  317.1 77.3 %all-gather.5.cloned.1.call-start = ((), (), s32[]{:S(2)}) async-start(), calls=%async_computation.8 | async-start | bytes 2297856 | tf_op jit(solution)/shard_map/all_gather | solution.py:54
  398.4 23.7 %copy-start.13 = (f32[64]{0:T(128)S(1)}, f32[64]{0:T(128)}, u32[]{:S(2)}) copy-start(f32[64]{0:T(128)} %param.29) | copy-start | bytes 772
  399.7 77.9 %all-to-all-start.6 = ((bf16[32,256,64]{1,2,0:T(8,128)(2,1)}), bf16[32,256,64]{1,2,0:T(8,128)(2,1)S(1)}, u32[]{:S(2)}, u32[]{:S(2)}) async-start(bf16[32,256,64]{1,2,0:T(8,128)(2,1)} %bitcast.11), calls=%async_computation.6 | async-start | bytes 2097152 | tf_op jit(solution)/shard_map/all_to_all | solution.py:46
Sparse Core Ops, SparseCore 0:
  116.3 81.2 all-gather.2
  320.5 73.7 all-gather.4
where the time goes:
time: 486 us; the launch traced here: 485 us
  waiting for transfers between devices  286 us (59%)
  blocking collectives  98.5 us (20%)
  starting transfers between devices  68.4 us (14%)
  between operations  13.7 us (3%)
  matrix products  7.77 us (2%)
  local copies, waits for them, and re-layouts  6.52 us (1%)
    all_to_all x2, waiting for transfers between devices, sent_and_summed(): lax.all_to_all(parts, axis, split_axis=0, concat_axis=0, tiled=True)  111 us
    all_to_all x1, blocking collectives, sent_to_all(): lax.all_to_all(jnp.broadcast_to(value[None], (devices, *value.shape)), ax...  98.5 us
    all_to_all x4, waiting for transfers between devices, sent_to_all(): lax.all_to_all(jnp.broadcast_to(value[None], (devices, *value.shape)), ax...  82.6 us
    all_gather x1, waiting for transfers between devices, turned_gather(): out = lax.all_gather(both, axis, axis=0, tiled=True)  76.5 us
    all_to_all x2, starting transfers between devices, sent_and_summed(): lax.all_to_all(parts, axis, split_axis=0, concat_axis=0, tiled=True)  42 us
    all_to_all x4, starting transfers between devices, sent_to_all(): lax.all_to_all(jnp.broadcast_to(value[None], (devices, *value.shape)), ax...  26.2 us
    all_gather x1, waiting for transfers between devices, side_by_side(): out = lax.all_gather(both, axis, axis=dim, tiled=True)  16.1 us
  transfers between devices with their start and end apart: 8, of which 7 were waited for; matrix products, arithmetic and copies ran while one was open for 1% of the time, Pallas kernels for 0%

commit v1 on v0

v1 whole, which is shorter than its diff:
```python
import functools

import jax
import jax.numpy as jnp
from jax import lax
from jax.experimental import pallas as pl
from jax.experimental.pallas import tpu as pltpu
from jax.sharding import Mesh, PartitionSpec as P

epsilon = 1e-06
BF = jnp.bfloat16
F32 = jnp.float32
CORES = 2
UP = 2.0**18
SWAP = [(0, 1), (1, 0)]


def split3(v):
    hi = lax.reduce_precision(v, 8, 7)
    mid = lax.reduce_precision(v - hi, 8, 7)
    lo = v - hi - mid
    return jnp.stack([hi, mid, lo]).astype(BF)


def own_rows(gate, up, down):
    return jnp.concatenate([gate.T, up.T, down], axis=0)


def ffn_kernel(hid, width, s_ref, g_ref, sc_ref, own_ref, sib_ref, out_ref, h_ref, hd_ref):
    chunks = own_ref.shape[0]
    lane = own_ref.shape[2]
    gains = jnp.transpose(g_ref[...])
    total = jnp.zeros((lane, s_ref.shape[1]), F32)
    for z in range(chunks):
        v = s_ref[pl.ds(z * lane, lane), :].astype(F32)
        total = total + v * v
    r = lax.rsqrt(jnp.sum(total, axis=0, keepdims=True) / width + epsilon)
    for z in range(chunks):
        v = s_ref[pl.ds(z * lane, lane), :].astype(F32)
        h_ref[pl.ds(z * lane, lane), :] = (v * r * gains[:, z : z + 1]).astype(BF)
    scales = jnp.transpose(sc_ref[...])
    for k, w in enumerate((own_ref, sib_ref)):
        acc = jnp.zeros((2 * hid, s_ref.shape[1]), F32)
        for z in range(0, chunks, 2):
            lhs = jnp.concatenate([w[z, : 2 * hid, :], w[z + 1, : 2 * hid, :]], axis=1)
            acc = acc + jnp.dot(
                lhs, h_ref[pl.ds(z * lane, 2 * lane), :], preferred_element_type=F32
            )
        gate = acc[:hid] * scales[:hid, 2 * k : 2 * k + 1]
        up = acc[hid:] * scales[:hid, 2 * k + 1 : 2 * k + 2]
        hd_ref[pl.ds(k * hid, hid), :] = (gate / (1.0 + jnp.exp(-gate)) * up).astype(BF)
    hidden = hd_ref[...]
    for z in range(chunks):
        lhs = jnp.concatenate([own_ref[z, 2 * hid :, :], sib_ref[z, 2 * hid :, :]], axis=0)
        part = lax.dot_general(
            lhs, hidden, (((0,), (0,)), ((), ())), preferred_element_type=F32
        )
        out_ref[pl.ds(z * lane, lane), :] = part.astype(BF)


def ffn(s, gain, scales, own, sib, width):
    hid = own.shape[1] // 3
    vmem = pl.BlockSpec(memory_space=pltpu.VMEM)
    tokens = s.shape[1]
    rows = own.shape[0] * own.shape[2]
    flops = 2 * 3 * 2 * hid * rows * tokens
    return pl.pallas_call(
        functools.partial(ffn_kernel, hid, float(width)),
        out_shape=jax.ShapeDtypeStruct((rows, tokens), BF),
        in_specs=[vmem] * 5,
        out_specs=vmem,
        scratch_shapes=[pltpu.VMEM((rows, tokens), BF), pltpu.VMEM((2 * hid, tokens), BF)],
        cost_estimate=pl.CostEstimate(
            flops=flops, bytes_accessed=4 * own.size, transcendentals=2 * hid * tokens
        ),
    )(s, gain, scales, own, sib)


def scale_rows(own, sib):
    rows = jnp.concatenate([own, sib], axis=0)
    return jnp.pad(rows, ((0, 8 - rows.shape[0]), (0, -rows.shape[1] % 128)))


def body(
    tokens,
    gain_1,
    gate_1,
    gate_s1,
    up_1,
    up_s1,
    down_1,
    down_s1,
    gain_2,
    gate_2,
    gate_s2,
    up_2,
    up_s2,
    down_2,
    down_s2,
):
    ny = lax.axis_size("y")
    peers = ny * CORES
    mine, feats = tokens.shape
    half = mine // CORES
    width = feats * peers
    y = lax.axis_index("y")
    core = lax.axis_index("c")

    own_2 = own_rows(gate_2, up_2, down_2).astype(BF)
    own_2 = lax.all_gather(own_2, "fs", axis=0)

    st = tokens.T.reshape(feats, CORES, half).transpose(1, 0, 2)
    vecs = jnp.concatenate([split3(gain_1), split3(gain_2)], axis=1)
    more = jnp.concatenate([split3(down_s1), split3(down_s2)], axis=1)
    extra = jnp.concatenate([vecs, more, jnp.zeros((2, vecs.shape[1]), BF)], axis=0)
    extra = jnp.pad(extra, ((0, 0), (0, half - extra.shape[1])))
    sent = jnp.concatenate([st, jnp.broadcast_to(extra[None], (CORES, *extra.shape))], axis=1)
    sent = jnp.broadcast_to(sent[None], (ny, *sent.shape)).reshape(peers, *sent.shape[1:])
    got = lax.all_to_all(sent, ("y", "c"), 0, 0, tiled=True)

    scales = jnp.stack([gate_s1, up_s1, gate_s2, up_s2])
    scales_sib = lax.ppermute(scales, "c", SWAP)

    own_1 = own_rows(gate_1, up_1, down_1).astype(BF)
    own_1 = (own_1.astype(F32) * UP).astype(jnp.float16)
    own_1 = lax.all_gather(own_1, "fs", axis=0)
    own_1 = (own_1.astype(F32) * (1.0 / UP)).astype(BF)
    sib_1 = lax.ppermute(own_1, "c", SWAP)
    sib_2 = lax.ppermute(own_2, "c", SWAP)

    s = got[:, :feats].reshape(width, half)
    vec = got[:, feats : feats + 3, : 2 * feats].astype(F32).sum(axis=1)
    more = got[:, feats + 3 : feats + 6, : 2 * feats].astype(F32).sum(axis=1)
    gains_1 = vec[:, :feats].reshape(-1, half)
    gains_2 = vec[:, feats:].reshape(-1, half)
    ds_1 = more[:, :feats].reshape(ny, -1)

    part = ffn(s, gains_1, scale_rows(scales[:2], scales_sib[:2]), own_1, sib_1, width)
    chip = feats * CORES
    arrived = lax.all_to_all(part.reshape(ny, chip, half), "y", 0, 0, tiled=True)
    summed = arrived.astype(F32).sum(axis=0)
    resid = lax.dynamic_slice_in_dim(s, y * chip, chip, 0).astype(F32)
    ds = lax.dynamic_index_in_dim(ds_1, y, 0, keepdims=False)
    middle = (resid + 0.5 * summed * ds[:, None]).astype(BF)

    there = lax.dynamic_slice_in_dim(middle, (1 - core) * feats, feats, 0)
    here = lax.dynamic_slice_in_dim(middle, core * feats, feats, 0)
    other = lax.ppermute(there, "c", SWAP)
    s2 = lax.all_gather(middle, "y", axis=0, tiled=True)

    part = ffn(s2, gains_2, scale_rows(scales[2:], scales_sib[2:]), own_2, sib_2, width)
    arrived = lax.all_to_all(part.reshape(peers, feats, half), ("y", "c"), 0, 0, tiled=True)
    summed = arrived.reshape(ny, CORES, feats, half).astype(F32).sum(axis=0)
    both = jnp.where(core == 0, jnp.stack([here, other]), jnp.stack([other, here]))
    out = (both.astype(F32) + 0.5 * summed * down_s2[None, :, None]).astype(BF)
    return out.transpose(0, 2, 1).reshape(mine, feats)


def solution(mesh):
    sizes = mesh.shape
    wide = Mesh(
        mesh.devices.reshape(sizes["grp"], sizes["fs"], sizes["tp"] // CORES, CORES),
        ("grp", "fs", "y", "c"),
    )
    tp = ("y", "c")
    block = (P(tp), P("fs", tp), P(tp), P("fs", tp), P(tp), P(tp, "fs"), P(tp))
    rows = P(("grp", "fs"), tp)
    return jax.shard_map(
        body, mesh=wide, in_specs=(rows, *block, *block), out_specs=rows, check_vma=False
    )
```

time: 486 us -> 302 us (0.62)
  waiting for transfers between devices: 286 us -> 50 us
  starting transfers between devices: 68.4 us -> 130 us
  blocking collectives: 98.5 us -> 84.4 us
  Pallas kernels: 0 us -> 10.1 us
  matrix products: 7.77 us -> 0 us
    all_to_all x6 -> x3, waiting for transfers between devices: 193 us -> 48 us  [the longest x1 30.6 us: body(): lax.all_to_all(part.reshape(peers, feats, half), ('y', 'c'), 0, 0, tiled=...]
    all_to_all x1 -> x0, blocking collectives: 98.5 us -> none  [sent_to_all(): lax.all_to_all(jnp.broadcast_to(value[None], (devices, *value.shape)), ax...]
    all_gather x2 -> x1, waiting for transfers between devices: 92.6 us -> 0.02 us  [body(): own_2 = lax.all_gather(own_2, 'fs', axis=0)]
    all_gather x0 -> x2, blocking collectives: none -> 84.4 us  [the longest x1 53.3 us: body(): own_1 = lax.all_gather(own_1, 'fs', axis=0)]
    all_to_all x6 -> x3, starting transfers between devices: 68.2 us -> 116 us  [the longest x1 87.2 us: body(): got = lax.all_to_all(sent, ('y', 'c'), 0, 0, tiled=True)]
    ppermute x0 -> x4, starting transfers between devices: none -> 14.3 us  [the longest x1 5.91 us: body(): sib_1 = lax.ppermute(own_1, 'c', SWAP)]
    pallas_call x0 -> x2, Pallas kernels: none -> 10.1 us  [ffn(): pl.pallas_call(functools.partial(ffn_kernel, hid, float(width)), out_shap...]
    dot_general x4 -> x0, matrix products: 7.77 us -> none  [the longest x1 2.51 us: body(): jnp.dot(hidden, down_full, preferred_element_type=jnp.float32)]
  transfers between devices with their start and end apart: 8 -> 8, of which waited for: 7 -> 3; matrix products, arithmetic and copies ran while one was open for 1% -> 2% of each run, Pallas kernels for 0% -> 2%
where the time goes in v1:
time: 302 us; the launch traced here: 301 us
  starting transfers between devices  130 us (43%)
  blocking collectives  84.4 us (28%)
  waiting for transfers between devices  50 us (17%)
  between operations  13.7 us (5%)
  Pallas kernels  10.1 us (3%)
  other arithmetic  6.75 us (2%)
  local copies, waits for them, and re-layouts  6.1 us (2%)
    all_to_all x1, starting transfers between devices, body(): got = lax.all_to_all(sent, ('y', 'c'), 0, 0, tiled=True)  87.2 us
    all_gather x1, blocking collectives, body(): own_1 = lax.all_gather(own_1, 'fs', axis=0)  53.3 us
    all_gather x1, blocking collectives, body(): s2 = lax.all_gather(middle, 'y', axis=0, tiled=True)  31.1 us
    all_to_all x1, waiting for transfers between devices, body(): lax.all_to_all(part.reshape(peers, feats, half), ('y', 'c'), 0, 0, tiled=...  30.6 us
    all_to_all x1, waiting for transfers between devices, body(): lax.all_to_all(part.reshape(ny, chip, half), 'y', 0, 0, tiled=True)  17.3 us
    all_to_all x1, starting transfers between devices, body(): lax.all_to_all(part.reshape(peers, feats, half), ('y', 'c'), 0, 0, tiled=...  16.8 us
    all_to_all x1, starting transfers between devices, body(): lax.all_to_all(part.reshape(ny, chip, half), 'y', 0, 0, tiled=True)  11.5 us
    pallas_call x2, Pallas kernels, ffn(): pl.pallas_call(functools.partial(ffn_kernel, hid, float(width)), out_shap...  10.1 us
  transfers between devices with their start and end apart: 8, of which 3 were waited for; matrix products, arithmetic and copies ran while one was open for 2% of the time, Pallas kernels for 2%

profile of v1, /device:TPU:5, one launch (start us, length us, event | category | flops | bytes accessed | tf_op | source)
XLA Modules:
  0.0 301.0 jit_solution(15444431001088306587)
XLA Ops:
  6.6 0.7 broadcast_multiply_fusion
  7.3 0.7 fusion.9
  7.9 0.8 reshape.136
  8.7 0.7 fusion.1
  9.4 0.1 pad.43.clone
  9.5 0.1 maximum_maximum_fusion
  9.6 0.1 pad_maximum_fusion.1
  9.6 0.9 broadcast_in_dim.8
  10.6 87.2 %all-to-all-start = ((bf16[32,72,128]{2,1,0:T(8,128)(2,1)}), bf16[32,72,128]{2,1,0:T(8,128)(2,1)S(1)}, u32[]{:S(2)}, u32[]{:S(2)}) async-start(bf16[32,72,128]{2,1,0:T(8,128)(2,1)} %bitcast.14), calls=%async_computation | async-start | bytes 1179648 | tf_op jit(solution)/shard_map/all_to_all | solution.py:119
  97.8 0.1 all-gather.3.cloned.1.call-start
  97.9 0.9 convert_bitcast_fusion
  98.8 0.0 copy-done.3
  98.8 0.0 copy-done.2
  98.8 0.7 pad_maximum_fusion
  99.5 0.1 all-gather.3.cloned.1.call-update
  99.5 0.0 copy-done.4
  99.7 53.3 %all-gather.4 = f16[16,528,128]{2,1,0:T(8,128)(2,1)S(1)} all-gather(f16[1,528,128]{2,1,0:T(8,128)(2,1)S(1)} %multiply_convert_fusion.1), channel_id=1, replica_groups=mesh['grp'=2,'fs'=16,'y'=16,'c'=2] {'fs'}, dimensions={0}, use_global_device_ids=true | all-gather | bytes 2297856 | tf_op jit(solution)/shard_map/all_gather | solution.py:126
  153.0 0.5 multiply_convert_fusion.own_ref
  153.5 5.9 %collective-permute-start.1 = (bf16[16,528,128]{2,1,0:T(8,128)(2,1)S(1)}, bf16[16,528,128]{2,1,0:T(8,128)(2,1)}, u32[]{:S(2)}, u32[]{:S(2)}) collective-permute-start(bf16[16,528,128]{2,1,0:T(8,128)(2,1)S(1)} %multiply_convert_fusion.own_ref), channel_id=1, source_target_pairs={{0,1},{1,0},{2,3},{3,2},{4,5},{5,4},{6,7},{7,6},{8,9},{9,8},{10,11... | collective-permute-start | bytes 6488072 | tf_op jit(solution)/shard_map/ppermute | solution.py:128
  159.5 2.0 collective-permute-start
  161.4 2.0 collective-permute-done
  163.4 0.6 pad.7.sc_ref
  164.0 0.0 all-to-all-done
  164.0 0.1 convert_reduce_fusion.2
  164.1 0.1 fusion.19
  164.2 0.7 reshape.139.g_ref
  164.8 0.9 slice.36
  165.7 0.0 collective-permute-done.1.sib_ref
  165.7 5.0 %shard_map.145 = bf16[2048,128]{1,0:T(8,128)(2,1)} custom-call(bf16[2048,128]{1,0:T(8,128)(2,1)} %bitcast.68, f32[16,128]{1,0:T(8,128)} %reshape.139.g_ref, f32[8,256]{1,0:T(8,128)} %pad.7.sc_ref, bf16[16,528,128]{2,1,0:T(8,128)(2,1)} %copy-done, bf16[16,528,128]{2,1,0:T(8,128)(2,1)} %collective-permute-done.1.sib_ref), custom_call_target="tpu_custom_call" | custom-call | flops 553648128 | bytes 4325376 | tf_op jit(solution)/shard_map/pallas_call | solution.py:67
  170.8 11.5 %all-to-all-start.1 = ((bf16[16,128,128]{2,1,0:T(8,128)(2,1)}), bf16[16,128,128]{2,1,0:T(8,128)(2,1)S(1)}, u32[]{:S(2)}, u32[]{:S(2)}) async-start(bf16[16,128,128]{2,1,0:T(8,128)(2,1)} %bitcast.71), calls=%async_computation.1 | async-start | bytes 1048576 | tf_op jit(solution)/shard_map/all_to_all | solution.py:140
  182.3 0.0 all-gather.3.cloned.1.call-done.own_ref
  182.4 3.8 %collective-permute-start.3 = (bf16[16,528,128]{2,1,0:T(8,128)(2,1)}, bf16[16,528,128]{2,1,0:T(8,128)(2,1)S(1)}, u32[]{:S(2)}, u32[]{:S(2)}) collective-permute-start(bf16[16,528,128]{2,1,0:T(8,128)(2,1)} %all-gather.3.cloned.1.call-done.own_ref), channel_id=1, source_target_pairs={{0,1},{1,0},{2,3},{3,2},{4,5},{5,4},{6,7},{7,6},{8,9},{9,8},{10,11... | collective-permute-start | bytes 6488072 | tf_op jit(solution)/shard_map/ppermute | solution.py:129
  186.2 0.6 select_maximum_fusion.sc_ref
  186.8 0.1 reshape.141
  186.9 0.7 reshape.142.g_ref
  187.5 17.3 %all-to-all-done.1 = bf16[16,128,128]{2,1,0:T(8,128)(2,1)S(1)} async-done(((bf16[16,128,128]{2,1,0:T(8,128)(2,1)}), bf16[16,128,128]{2,1,0:T(8,128)(2,1)S(1)}, u32[]{:S(2)}, u32[]{:S(2)}) %all-to-all-start.1) | async-done | bytes 524320 | tf_op jit(solution)/shard_map/all_to_all | solution.py:140
  204.9 0.1 convert_reduce_fusion.1
  205.0 0.8 add_convert_fusion.1
  205.8 31.1 %all_gather.12.s_ref = bf16[2048,128]{1,0:T(8,128)(2,1)} all-gather(bf16[128,128]{1,0:T(8,128)(2,1)S(1)} %add_convert_fusion.1), channel_id=1, replica_groups=mesh['grp'=2,'fs'=16,'y'=16,'c'=2] {'y'}, dimensions={0}, use_global_device_ids=true | all-gather | bytes 557056 | tf_op jit(solution)/shard_map/all_gather | solution.py:149
  236.9 0.0 collective-permute-done.3.sib_ref
  236.9 1.3 copy-done.1
  238.2 5.0 %shard_map.146 = bf16[2048,128]{1,0:T(8,128)(2,1)} custom-call(bf16[2048,128]{1,0:T(8,128)(2,1)} %all_gather.12.s_ref, f32[16,128]{1,0:T(8,128)} %reshape.142.g_ref, f32[8,256]{1,0:T(8,128)} %select_maximum_fusion.sc_ref, bf16[16,528,128]{2,1,0:T(8,128)(2,1)} %all-gather.3.cloned.1.call-done.own_ref, bf16[16,528,128]{2,1,0:T(8,128)(2,1)} %copy-done.1), custom_call_target="tpu_custom_call" | custom-call | flops 553648128 | bytes 4325376 | tf_op jit(solution)/shard_map/pallas_call | solution.py:67
  243.2 16.8 %all-to-all-start.2 = ((bf16[32,64,128]{2,1,0:T(8,128)(2,1)}), bf16[32,64,128]{2,1,0:T(8,128)(2,1)S(1)}, u32[]{:S(2)}, u32[]{:S(2)}) async-start(bf16[32,64,128]{2,1,0:T(8,128)(2,1)} %bitcast.72), calls=%async_computation.2 | async-start | bytes 1048576 | tf_op jit(solution)/shard_map/all_to_all | solution.py:152
  260.1 2.6 collective-permute-start.2
  262.7 30.6 %all-to-all-done.2 = bf16[32,64,128]{2,1,0:T(8,128)(2,1)S(1)} async-done(((bf16[32,64,128]{2,1,0:T(8,128)(2,1)}), bf16[32,64,128]{2,1,0:T(8,128)(2,1)S(1)}, u32[]{:S(2)}, u32[]{:S(2)}) %all-to-all-start.2) | async-done | bytes 524320 | tf_op jit(solution)/shard_map/all_to_all | solution.py:152
  293.3 0.1 convert_reduce_fusion
  293.4 0.0 collective-permute-done.2
  293.4 0.7 copy_bitcast_fusion
  (30 shorter events, 0.2 us)
Async XLA Ops:
  6.5 92.2 %copy-start.3 = (f32[128,176]{0,1:T(8,128)S(1)}, f32[128,176]{0,1:T(8,128)}, u32[]{:S(2)}) copy-start(f32[128,176]{0,1:T(8,128)} %param.24) | copy-start | bytes 270340
  6.5 92.2 %copy-start.2 = (f32[128,176]{0,1:T(8,128)S(1)}, f32[128,176]{0,1:T(8,128)}, u32[]{:S(2)}) copy-start(f32[128,176]{0,1:T(8,128)} %param.26) | copy-start | bytes 270340
  6.6 93.0 %copy-start.4 = (f32[176,128]{1,0:T(8,128)S(1)}, f32[176,128]{1,0:T(8,128)}, u32[]{:S(2)}) copy-start(f32[176,128]{1,0:T(8,128)} %param.21) | copy-start | bytes 270340
  6.6 93.0 %copy-start.6 = (f32[128,176]{0,1:T(8,128)S(1)}, f32[128,176]{0,1:T(8,128)}, u32[]{:S(2)}) copy-start(f32[128,176]{0,1:T(8,128)} %param.17) | copy-start | bytes 270340
  6.6 93.0 %copy-start.5 = (f32[128,176]{0,1:T(8,128)S(1)}, f32[128,176]{0,1:T(8,128)}, u32[]{:S(2)}) copy-start(f32[128,176]{0,1:T(8,128)} %param.19) | copy-start | bytes 270340
  10.6 153.5 %all-to-all-start = ((bf16[32,72,128]{2,1,0:T(8,128)(2,1)}), bf16[32,72,128]{2,1,0:T(8,128)(2,1)S(1)}, u32[]{:S(2)}, u32[]{:S(2)}) async-start(bf16[32,72,128]{2,1,0:T(8,128)(2,1)} %bitcast.14), calls=%async_computation | async-start | bytes 1179648 | tf_op jit(solution)/shard_map/all_to_all | solution.py:119
  97.8 84.5 %all-gather.3.cloned.1.call-start = ((), (), s32[]{:S(2)}) async-start(), calls=%async_computation.3 | async-start | bytes 2297856 | tf_op jit(solution)/shard_map/all_gather | solution.py:110
  153.0 6.4 %copy-start.7 = (f32[176]{0:T(256)S(1)}, f32[176]{0:T(256)}, u32[]{:S(2)}) copy-start(f32[176]{0:T(256)} %param.27) | copy-start | bytes 2116
  153.0 6.4 %copy-start.8 = (f32[176]{0:T(256)S(1)}, f32[176]{0:T(256)}, u32[]{:S(2)}) copy-start(f32[176]{0:T(256)} %param.25) | copy-start | bytes 2116
  153.0 6.5 %copy-start.9 = (f32[176]{0:T(256)S(1)}, f32[176]{0:T(256)}, u32[]{:S(2)}) copy-start(f32[176]{0:T(256)} %param.20) | copy-start | bytes 2116
  153.0 6.5 %copy-start.10 = (f32[176]{0:T(256)S(1)}, f32[176]{0:T(256)}, u32[]{:S(2)}) copy-start(f32[176]{0:T(256)} %param.18) | copy-start | bytes 2116
  153.5 12.2 %copy-start = (bf16[16,528,128]{2,1,0:T(8,128)(2,1)}, bf16[16,528,128]{2,1,0:T(8,128)(2,1)S(1)}, u32[]{:S(2)}) copy-start(bf16[16,528,128]{2,1,0:T(8,128)(2,1)S(1)} %multiply_convert_fusion.own_ref) | copy-start | bytes 6488068
  153.5 12.2 %collective-permute-start.1 = (bf16[16,528,128]{2,1,0:T(8,128)(2,1)S(1)}, bf16[16,528,128]{2,1,0:T(8,128)(2,1)}, u32[]{:S(2)}, u32[]{:S(2)}) collective-permute-start(bf16[16,528,128]{2,1,0:T(8,128)(2,1)S(1)} %multiply_convert_fusion.own_ref), channel_id=1, source_target_pairs={{0,1},{1,0},{2,3},{3,2},{4,5},{5,4},{6,7},{7,6},{8,9},{9,8},{10,11... | collective-permute-start | bytes 6488072 | tf_op jit(solution)/shard_map/ppermute | solution.py:128
  159.5 3.9 %collective-permute-start = (f32[4,176]{1,0:T(4,128)S(1)}, f32[4,176]{1,0:T(4,128)S(1)}, u32[]{:S(2)}, u32[]{:S(2)}) collective-permute-start(f32[4,176]{1,0:T(4,128)S(1)} %pad_maximum_fusion.2), channel_id=1, source_target_pairs={{0,1},{1,0},{2,3},{3,2},{4,5},{5,4},{6,7},{7,6},{8,9},{9,8},{10,11... | collective-permute-start | bytes 8456 | tf_op jit(solution)/shard_map/ppermute | solution.py:122
  170.8 34.1 %all-to-all-start.1 = ((bf16[16,128,128]{2,1,0:T(8,128)(2,1)}), bf16[16,128,128]{2,1,0:T(8,128)(2,1)S(1)}, u32[]{:S(2)}, u32[]{:S(2)}) async-start(bf16[16,128,128]{2,1,0:T(8,128)(2,1)} %bitcast.71), calls=%async_computation.1 | async-start | bytes 1048576 | tf_op jit(solution)/shard_map/all_to_all | solution.py:140
  182.4 54.5 %collective-permute-start.3 = (bf16[16,528,128]{2,1,0:T(8,128)(2,1)}, bf16[16,528,128]{2,1,0:T(8,128)(2,1)S(1)}, u32[]{:S(2)}, u32[]{:S(2)}) collective-permute-start(bf16[16,528,128]{2,1,0:T(8,128)(2,1)} %all-gather.3.cloned.1.call-done.own_ref), channel_id=1, source_target_pairs={{0,1},{1,0},{2,3},{3,2},{4,5},{5,4},{6,7},{7,6},{8,9},{9,8},{10,11... | collective-permute-start | bytes 6488072 | tf_op jit(solution)/shard_map/ppermute | solution.py:129
  236.9 1.3 copy-start.1
  243.2 50.1 %all-to-all-start.2 = ((bf16[32,64,128]{2,1,0:T(8,128)(2,1)}), bf16[32,64,128]{2,1,0:T(8,128)(2,1)S(1)}, u32[]{:S(2)}, u32[]{:S(2)}) async-start(bf16[32,64,128]{2,1,0:T(8,128)(2,1)} %bitcast.72), calls=%async_computation.2 | async-start | bytes 1048576 | tf_op jit(solution)/shard_map/all_to_all | solution.py:152
  260.1 33.4 %collective-permute-start.2 = (bf16[64,128]{1,0:T(8,128)(2,1)S(1)}, bf16[64,128]{1,0:T(8,128)(2,1)S(1)}, u32[]{:S(2)}, u32[]{:S(2)}) collective-permute-start(bf16[64,128]{1,0:T(8,128)(2,1)S(1)} %get-tuple-element.8), channel_id=1, source_target_pairs={{0,1},{1,0},{2,3},{3,2},{4,5},{5,4},{6,7},{7,6},{8,9},{9,8},{10,11... | collective-permute-start | bytes 49160 | tf_op jit(solution)/shard_map/ppermute | solution.py:148
Sparse Core Ops, SparseCore 0:
  101.3 73.3 all-gather.2

commit v2 on v1

v2 whole, which is shorter than its diff:
```python
import functools

import jax
import jax.numpy as jnp
from jax import lax
from jax.experimental import pallas as pl
from jax.experimental.pallas import tpu as pltpu
from jax.sharding import Mesh, PartitionSpec as P

epsilon = 1e-06
BF = jnp.bfloat16
F32 = jnp.float32
CORES = 2
SIDE = 4
LANE = 128
EXTRA = 32
UP = 2.0**18
SWAP = [(0, 1), (1, 0)]
VMEM = pl.BlockSpec(memory_space=pltpu.VMEM)


def split3(v):
    hi = v.astype(BF).astype(F32)
    mid = (v - hi).astype(BF).astype(F32)
    return hi, mid, v - hi - mid


def wide_row(a):
    if a.shape[1] == LANE:
        return a
    fill = jnp.zeros((1, LANE - a.shape[1]), F32)
    return jnp.concatenate([a, fill], axis=1)


def prep_kernel(t_ref, g1, g2, d1, d2, s1, s2, s3, s4, out_ref, ext):
    peers, rows, half = out_ref.shape
    feats = t_ref.shape[0]
    ext[...] = jnp.zeros_like(ext)
    for k, (a, b) in enumerate(((g1, g2), (d1, d2))):
        for p, (u, v) in enumerate(zip(split3(a[...]), split3(b[...]))):
            ext[3 * k + p : 3 * k + p + 1, :] = wide_row(jnp.concatenate([u, v], axis=1))
    for j, ref in enumerate((s1, s2, s3, s4)):
        for p, u in enumerate(split3(ref[...])):
            at = 8 + 8 * p + 2 * j
            ext[at : at + 1, :] = u[:, :LANE]
            ext[at + 1 : at + 2, :] = wide_row(u[:, LANE:])
    tail = ext[...].astype(BF)
    for k in range(peers):
        c = k % CORES
        out_ref[k, :feats, :] = t_ref[:, c * half : (c + 1) * half]
        out_ref[k, feats:, :] = tail


def vec_column(got, peer, which, feats, col, size):
    rows = got[peer, feats + 8 : feats + EXTRA, :].astype(F32)
    rows = rows[0:8] + rows[8:16] + rows[16:24]
    turned = jnp.transpose(rows)
    cols = []
    for w in which:
        a = turned[:, 2 * w : 2 * w + 1]
        b = turned[: size - LANE, 2 * w + 1 : 2 * w + 2]
        cols.append(jnp.concatenate([a, b], axis=0))
    return cols


def ffn_kernel(hid, block, s_ref, got, own_ref, sib_ref, out_ref, h_ref, hd_ref, g_ref):
    peers = got.shape[0]
    feats = got.shape[1] - EXTRA
    tokens = got.shape[2]
    chunks, _, lane = own_ref.shape
    width = feats * peers
    me = lax.axis_index("y") * CORES + lax.axis_index("c")
    sib = lax.axis_index("y") * CORES + 1 - lax.axis_index("c")
    for p in range(peers):
        rows = got[p, feats : feats + 8, :].astype(F32)
        g_ref[p : p + 1, :] = rows[0:1] + rows[1:2] + rows[2:3]
    gains = jnp.transpose(g_ref[...])
    gains = gains[:feats] if block == 0 else gains[feats : 2 * feats]

    def piece(p):
        if block == 0:
            return got[p, :feats, :].astype(F32)
        return s_ref[pl.ds(p * feats, feats), :].astype(F32)

    total = jnp.zeros((feats, tokens), F32)
    for p in range(peers):
        v = piece(p)
        total = total + v * v
    r = lax.rsqrt(jnp.sum(total, axis=0, keepdims=True) / float(width) + epsilon)
    for p in range(peers):
        h_ref[pl.ds(p * feats, feats), :] = (piece(p) * r * gains[:, p : p + 1]).astype(BF)
    for k, (w, peer) in enumerate(((own_ref, me), (sib_ref, sib))):
        sg, su = vec_column(got, peer, (2 * block, 2 * block + 1), feats, block, hid)
        acc = jnp.zeros((2 * hid, tokens), F32)
        for z in range(0, chunks, 2):
            lhs = jnp.concatenate([w[z, : 2 * hid, :], w[z + 1, : 2 * hid, :]], axis=1)
            acc = acc + jnp.dot(
                lhs, h_ref[pl.ds(z * lane, 2 * lane), :], preferred_element_type=F32
            )
        gate = acc[:hid] * sg
        up = acc[hid:] * su
        hd_ref[pl.ds(k * hid, hid), :] = (gate / (1.0 + jnp.exp(-gate)) * up).astype(BF)
    hidden = hd_ref[...]
    for z in range(chunks):
        lhs = jnp.concatenate([own_ref[z, 2 * hid :, :], sib_ref[z, 2 * hid :, :]], axis=0)
        part = lax.dot_general(
            lhs, hidden, (((0,), (0,)), ((), ())), preferred_element_type=F32
        )
        out_ref[z % SIDE, z // SIDE] = part.astype(BF)


def chip_column(got, y, block, feats):
    cols = []
    for c in range(CORES):
        rows = got[y * CORES + c, feats : feats + 8, :].astype(F32)
        row = rows[3:4] + rows[4:5] + rows[5:6]
        turned = jnp.transpose(jnp.broadcast_to(row, (8, LANE)))
        cols.append(turned[block * feats : (block + 1) * feats, 0:1])
    return jnp.concatenate(cols, axis=0)


def close_kernel(block, sums, got, mid_ref, out_ref):
    feats = got.shape[1] - EXTRA
    y = lax.axis_index("y")
    total = sums[0].astype(F32)
    for k in range(1, sums.shape[0]):
        total = total + sums[k].astype(F32)
    if block == 0:
        resid = jnp.concatenate([got[y * CORES + c, :feats, :] for c in range(CORES)], axis=0)
    else:
        resid = mid_ref[...]
    scale = chip_column(got, y, block, feats)
    out_ref[...] = (resid.astype(F32) + 0.5 * total * scale).astype(BF)


def partial_kernel(got, out_ref):
    total = got[0].astype(F32)
    for k in range(1, got.shape[0]):
        total = total + got[k].astype(F32)
    out_ref[...] = total.astype(BF)


def call(kernel, out, args, scratch=(), flops=1000, limit=4 << 20):
    return pl.pallas_call(
        kernel,
        out_shape=out,
        in_specs=[VMEM] * len(args),
        out_specs=VMEM,
        scratch_shapes=list(scratch),
        compiler_params=pltpu.CompilerParams(vmem_limit_bytes=limit),
        cost_estimate=pl.CostEstimate(flops=flops, bytes_accessed=1 << 20, transcendentals=0),
    )(*args)


def own_rows(gate, up, down):
    return jnp.concatenate([gate.T, up.T, down], axis=0)


def body(
    tokens,
    gain_1,
    gate_1,
    gate_s1,
    up_1,
    up_s1,
    down_1,
    down_s1,
    gain_2,
    gate_2,
    gate_s2,
    up_2,
    up_s2,
    down_2,
    down_s2,
):
    ny = lax.axis_size("y")
    peers = ny * CORES
    mine, feats = tokens.shape
    half = mine // CORES
    chip = feats * CORES
    hid = gate_1.shape[1]
    near = [[SIDE * i + j for j in range(SIDE)] for i in range(ny // SIDE)]
    far = [[j + SIDE * i for i in range(ny // SIDE)] for j in range(SIDE)]

    vecs = [v[None] for v in (gain_1, gain_2, down_s1, down_s2, gate_s1, up_s1, gate_s2, up_s2)]
    sent = call(
        prep_kernel,
        jax.ShapeDtypeStruct((peers, feats + EXTRA, half), BF),
        (tokens.T, *vecs),
        [pltpu.VMEM((EXTRA, LANE), F32)],
    )
    got = lax.all_to_all(sent, ("y", "c"), 0, 0, tiled=True)

    own_2 = own_rows(gate_2, up_2, down_2).astype(BF)
    own_2 = lax.all_gather(own_2, "fs", axis=0)

    own_1 = own_rows(gate_1, up_1, down_1).astype(BF)
    own_1 = (own_1.astype(F32) * UP).astype(jnp.float16)
    own_1 = lax.all_gather(own_1, "fs", axis=0)
    own_1, got = lax.optimization_barrier((own_1, got))
    own_1 = (own_1.astype(F32) * (1.0 / UP)).astype(BF)
    sib_1 = lax.ppermute(own_1, "c", SWAP)

    def ffn(block, s, own, sib):
        return call(
            functools.partial(ffn_kernel, hid, block),
            jax.ShapeDtypeStruct((SIDE, ny // SIDE, chip, half), BF),
            (s, got, own, sib),
            [
                pltpu.VMEM((peers * feats, half), BF),
                pltpu.VMEM((CORES * hid, half), BF),
                pltpu.VMEM((peers, LANE), F32),
            ],
            flops=12 * hid * peers * feats * half,
            limit=16 << 20,
        )

    def reduced(block, part, mid):
        step = lax.all_to_all(part, "y", 0, 0, axis_index_groups=near, tiled=True)
        step = call(partial_kernel, jax.ShapeDtypeStruct(step.shape[1:], BF), (step,))
        step = lax.all_to_all(step, "y", 0, 0, axis_index_groups=far, tiled=True)
        return call(
            functools.partial(close_kernel, block),
            jax.ShapeDtypeStruct((chip, half), BF),
            (step, got, mid),
        )

    middle = reduced(0, ffn(0, gain_1[None], own_1, sib_1), gain_1[None])
    own_2, middle = lax.optimization_barrier((own_2, middle))
    sib_2 = lax.ppermute(own_2, "c", SWAP)
    whole = lax.all_gather(middle, "y", axis=0, tiled=True)
    last = reduced(1, ffn(1, whole, own_2, sib_2), middle)

    core = lax.axis_index("c")
    there = lax.dynamic_slice_in_dim(last, (1 - core) * feats, feats, 0)
    here = lax.dynamic_slice_in_dim(last, core * feats, feats, 0)
    other = lax.ppermute(there, "c", SWAP)
    first = core == 0
    both = [jnp.where(first, here, other), jnp.where(first, other, here)]
    return jnp.concatenate(both, axis=1).T


def solution(mesh):
    sizes = mesh.shape
    wide = Mesh(
        mesh.devices.reshape(sizes["grp"], sizes["fs"], sizes["tp"] // CORES, CORES),
        ("grp", "fs", "y", "c"),
    )
    tp = ("y", "c")
    block = (P(tp), P("fs", tp), P(tp), P("fs", tp), P(tp), P(tp, "fs"), P(tp))
    rows = P(("grp", "fs"), tp)
    return jax.shard_map(
        body, mesh=wide, in_specs=(rows, *block, *block), out_specs=rows, check_vma=False
    )
```

time: 302 us -> 317 us (1.050)
  blocking collectives: 84.4 us -> 124 us
  waiting for transfers between devices: 50 us -> 32.4 us
  other arithmetic: 6.75 us -> 3.5 us
    all_to_all x0 -> x3, blocking collectives: none -> 51.9 us  [the longest x2 30.2 us: reduced(): step = lax.all_to_all(part, 'y', 0, 0, axis_index_groups=near, tiled=True)]
    all_to_all x2 -> x1, waiting for transfers between devices: 48 us -> 12 us  [reduced(): step = lax.all_to_all(step, 'y', 0, 0, axis_index_groups=far, tiled=True)]
    all_to_all x2 -> x1, starting transfers between devices: 28.3 us -> 7.68 us  [reduced(): step = lax.all_to_all(step, 'y', 0, 0, axis_index_groups=far, tiled=True)]
    all_gather x1, waiting for transfers between devices: 0.02 us -> 16.3 us  [body(): own_2 = lax.all_gather(own_2, 'fs', axis=0)]
    ppermute x1, starting transfers between devices: 2.64 us -> 12.1 us  [body(): other = lax.ppermute(there, 'c', SWAP)]
    ppermute x1, starting transfers between devices: 3.82 us -> 11.6 us  [body(): sib_2 = lax.ppermute(own_2, 'c', SWAP)]
    all_gather x1, blocking collectives: 53.3 us -> 46.6 us  [body(): own_1 = lax.all_gather(own_1, 'fs', axis=0)]
    unnamed x22 -> x34, local copies, waits for them, and re-layouts: 1.36 us -> 7.73 us
  transfers between devices with their start and end apart: 8 -> 6, of which waited for: 3 -> 4; matrix products, arithmetic and copies ran while one was open for 2% -> 0% of each run, Pallas kernels for 2% -> 1%
where the time goes in v2:
time: 317 us
  starting transfers between devices  128 us (40%)
  blocking collectives  124 us (39%)
  waiting for transfers between devices  32.4 us (10%)
  between operations  13.6 us (4%)
  local copies, waits for them, and re-layouts  7.74 us (2%)
  Pallas kernels  7.47 us (2%)
  other arithmetic  3.5 us (1%)
    all_to_all x1, starting transfers between devices, body(): got = lax.all_to_all(sent, ('y', 'c'), 0, 0, tiled=True)  87.3 us
    all_gather x1, blocking collectives, body(): own_1 = lax.all_gather(own_1, 'fs', axis=0)  46.6 us
    all_to_all x2, blocking collectives, reduced(): step = lax.all_to_all(part, 'y', 0, 0, axis_index_groups=near, tiled=True)  30.2 us
    all_gather x1, blocking collectives, body(): whole = lax.all_gather(middle, 'y', axis=0, tiled=True)  25.4 us
    all_to_all x1, blocking collectives, reduced(): step = lax.all_to_all(step, 'y', 0, 0, axis_index_groups=far, tiled=True)  21.7 us
    all_gather x1, waiting for transfers between devices, body(): own_2 = lax.all_gather(own_2, 'fs', axis=0)  16.3 us
    ppermute x1, starting transfers between devices, body(): other = lax.ppermute(there, 'c', SWAP)  12.1 us
    all_to_all x1, waiting for transfers between devices, reduced(): step = lax.all_to_all(step, 'y', 0, 0, axis_index_groups=far, tiled=True)  12 us
  transfers between devices with their start and end apart: 6, of which 4 were waited for; matrix products, arithmetic and copies ran while one was open for 0% of the time, Pallas kernels for 1%

profile of v2, /device:TPU:5, one launch (start us, length us, event | category | flops | bytes accessed | tf_op | source)
XLA Modules:
  0.0 316.7 jit_solution(4707145373757781752)
XLA Ops:
  6.5 0.0 copy-start.1
  6.5 0.8 copy-done.1
  7.3 0.0 copy-start.2
  7.3 0.7 copy-done.2
  8.0 0.7 copy-done.4
  8.6 0.7 copy-done.5
  9.3 0.7 copy-done.6
  10.0 0.7 copy-done.7
  10.7 0.7 copy-done.8
  11.3 0.7 copy-done.9
  12.0 0.7 copy-done.10
  12.7 0.0 copy-start.15
  12.7 1.0 shard_map.145
  13.7 87.3 %all-to-all-start = ((bf16[32,96,128]{2,1,0:T(8,128)(2,1)}), bf16[32,96,128]{2,1,0:T(8,128)(2,1)S(1)}, u32[]{:S(2)}, u32[]{:S(2)}) async-start(bf16[32,96,128]{2,1,0:T(8,128)(2,1)} %shard_map.145), calls=%async_computation | async-start | bytes 1572864 | tf_op jit(solution)/shard_map/all_to_all | solution.py:192
  100.9 0.1 all-gather.3.cloned.1.call-start
  101.0 0.0 copy-done.11
  101.0 0.0 copy-done.12
  101.0 0.0 copy-done.13
  101.1 0.0 copy-done.14
  101.1 0.0 copy-done.15
  101.2 46.6 %all-gather.4 = f16[16,528,128]{2,1,0:T(8,128)(2,1)} all-gather(f16[1,528,128]{2,1,0:T(8,128)(2,1)S(1)} %multiply_convert_fusion.1), channel_id=1, replica_groups=mesh['grp'=2,'fs'=16,'y'=16,'c'=2] {'fs'}, dimensions={0}, use_global_device_ids=true | all-gather | bytes 2297856 | tf_op jit(solution)/shard_map/all_gather | solution.py:199
  147.8 0.0 all-to-all-done.got
  147.8 2.1 multiply_convert_fusion.own_ref
  149.9 9.4 %collective-permute-start = (bf16[16,528,128]{2,1,0:T(8,128)(2,1)S(1)}, bf16[16,528,128]{2,1,0:T(8,128)(2,1)}, u32[]{:S(2)}, u32[]{:S(2)}) collective-permute-start(bf16[16,528,128]{2,1,0:T(8,128)(2,1)S(1)} %multiply_convert_fusion.own_ref), channel_id=1, source_target_pairs={{0,1},{1,0},{2,3},{3,2},{4,5},{5,4},{6,7},{7,6},{8,9},{9,8},{10,11... | collective-permute-start | bytes 6488072 | tf_op jit(solution)/shard_map/ppermute | solution.py:202
  159.3 0.0 copy-done.16
  159.3 0.7 pad_maximum_fusion
  160.0 0.1 all-gather.3.cloned.1.call-update
  160.1 3.2 %collective-permute-done.sib_ref = bf16[16,528,128]{2,1,0:T(8,128)(2,1)} collective-permute-done((bf16[16,528,128]{2,1,0:T(8,128)(2,1)S(1)}, bf16[16,528,128]{2,1,0:T(8,128)(2,1)}, u32[]{:S(2)}, u32[]{:S(2)}) %collective-permute-start) | collective-permute-done | bytes 2162720 | tf_op jit(solution)/shard_map/ppermute | solution.py:202
  163.3 0.0 copy-done.3
  163.3 3.4 %shard_map.146 = bf16[4,4,128,128]{3,2,1,0:T(8,128)(2,1)S(1)} custom-call(f32[1,64]{1,0:T(1,128)S(1)} %bitcast.33, bf16[32,96,128]{2,1,0:T(8,128)(2,1)S(1)} %all-to-all-done.got, bf16[16,528,128]{2,1,0:T(8,128)(2,1)S(1)} %multiply_convert_fusion.own_ref, bf16[16,528,128]{2,1,0:T(8,128)(2,1)} %collective-permute-done.sib_ref), custom_call_target="tpu_custom_call" | custom-call | flops 553648128 | bytes 1048576 | tf_op jit(solution)/shard_map/pallas_call | solution.py:144
  166.7 18.1 %all_to_all.25.got = bf16[4,4,128,128]{3,2,1,0:T(8,128)(2,1)S(1)} all-to-all(bf16[4,4,128,128]{3,2,1,0:T(8,128)(2,1)S(1)} %shard_map.146), channel_id=1, replica_groups={{0,2,4,6},{8,10,12,14},{16,18,20,22},{24,26,28,30},{1,3,5,7},{9,11,13,1..., dimensions={0} | all-to-all | bytes 1048576 | tf_op jit(solution)/shard_map/all_to_all | solution.py:219
  184.8 0.1 shard_map.147
  184.9 21.7 %all_to_all.26.sums = bf16[4,128,128]{2,1,0:T(8,128)(2,1)S(1)} all-to-all(bf16[4,128,128]{2,1,0:T(8,128)(2,1)S(1)} %shard_map.147), channel_id=1, replica_groups={{0,8,16,24},{2,10,18,26},{4,12,20,28},{6,14,22,30},{1,9,17,25},{3,11,19..., dimensions={0} | all-to-all | bytes 262144 | tf_op jit(solution)/shard_map/all_to_all | solution.py:221
  206.5 0.2 shard_map.148.mid_ref
  206.7 16.3 %all-gather.3.cloned.1.call-done.own_ref = bf16[16,528,128]{2,1,0:T(8,128)(2,1)} async-done(((bf16[1,528,128]{2,1,0:T(8,128)(2,1)}), bf16[16,528,128]{2,1,0:T(8,128)(2,1)}) %all-gather.3.cloned.1.call-update) | async-done | bytes 2162704 | tf_op jit(solution)/shard_map/all_gather | solution.py:195
  223.0 11.6 %collective-permute-start.1 = (bf16[16,528,128]{2,1,0:T(8,128)(2,1)}, bf16[16,528,128]{2,1,0:T(8,128)(2,1)S(1)}, u32[]{:S(2)}, u32[]{:S(2)}) collective-permute-start(bf16[16,528,128]{2,1,0:T(8,128)(2,1)} %all-gather.3.cloned.1.call-done.own_ref), channel_id=1, source_target_pairs={{0,1},{1,0},{2,3},{3,2},{4,5},{5,4},{6,7},{7,6},{8,9},{9,8},{10,11... | collective-permute-start | bytes 6488072 | tf_op jit(solution)/shard_map/ppermute | solution.py:230
  234.6 25.4 %all_gather.13.s_ref = bf16[2048,128]{1,0:T(8,128)(2,1)S(1)} all-gather(bf16[128,128]{1,0:T(8,128)(2,1)S(1)} %shard_map.148.mid_ref), channel_id=1, replica_groups=mesh['grp'=2,'fs'=16,'y'=16,'c'=2] {'y'}, dimensions={0}, use_global_device_ids=true | all-gather | bytes 557056 | tf_op jit(solution)/shard_map/all_gather | solution.py:231
  259.9 0.0 collective-permute-done.1.sib_ref
  259.9 1.6 copy-done
  261.6 1.8 shard_map.149
  263.4 12.2 %all_to_all.27.got = bf16[4,4,128,128]{3,2,1,0:T(8,128)(2,1)S(1)} all-to-all(bf16[4,4,128,128]{3,2,1,0:T(8,128)(2,1)S(1)} %shard_map.149), channel_id=1, replica_groups={{0,2,4,6},{8,10,12,14},{16,18,20,22},{24,26,28,30},{1,3,5,7},{9,11,13,1..., dimensions={0} | all-to-all | bytes 1048576 | tf_op jit(solution)/shard_map/all_to_all | solution.py:219
  275.6 0.7 shard_map.150
  276.3 7.7 %all-to-all-start.4 = ((bf16[4,128,128]{2,1,0:T(8,128)(2,1)}), bf16[4,128,128]{2,1,0:T(8,128)(2,1)S(1)}, u32[]{:S(2)}, u32[]{:S(2)}) async-start(bf16[4,128,128]{2,1,0:T(8,128)(2,1)} %shard_map.150), calls=%async_computation.4 | async-start | bytes 262144 | tf_op jit(solution)/shard_map/all_to_all | solution.py:221
  284.0 12.0 %all-to-all-done.4.sums = bf16[4,128,128]{2,1,0:T(8,128)(2,1)S(1)} async-done(((bf16[4,128,128]{2,1,0:T(8,128)(2,1)}), bf16[4,128,128]{2,1,0:T(8,128)(2,1)S(1)}, u32[]{:S(2)}, u32[]{:S(2)}) %all-to-all-start.4) | async-done | bytes 131104 | tf_op jit(solution)/shard_map/all_to_all | solution.py:221
  296.0 0.2 shard_map.151
  296.3 12.1 %collective-permute-start.2 = (bf16[64,128]{1,0:T(8,128)(2,1)S(1)}, bf16[64,128]{1,0:T(8,128)(2,1)S(1)}, u32[]{:S(2)}, u32[]{:S(2)}) collective-permute-start(bf16[64,128]{1,0:T(8,128)(2,1)S(1)} %constant_dynamic-slice_fusion), channel_id=1, source_target_pairs={{0,1},{1,0},{2,3},{3,2},{4,5},{5,4},{6,7},{7,6},{8,9},{9,8},{10,11... | collective-permute-start | bytes 49160 | tf_op jit(solution)/shard_map/ppermute | solution.py:237
  308.4 0.8 collective-permute-done.2
  309.2 0.6 maximum_bitcast_fusion
  (21 shorter events, 0.1 us)
Async XLA Ops:
  6.5 0.8 copy-start.1
  7.3 0.7 copy-start.2
  8.0 0.7 copy-start.4
  8.6 0.7 copy-start.5
  9.3 0.7 copy-start.6
  10.0 0.7 copy-start.7
  10.7 0.7 copy-start.8
  11.3 0.7 copy-start.9
  12.0 0.7 copy-start.10
  12.6 88.4 %copy-start.11 = (f32[176,128]{1,0:T(8,128)S(1)}, f32[176,128]{1,0:T(8,128)}, u32[]{:S(2)}) copy-start(f32[176,128]{1,0:T(8,128)} %param.21) | copy-start | bytes 270340
  12.6 88.4 %copy-start.12 = (f32[128,176]{0,1:T(8,128)S(1)}, f32[128,176]{0,1:T(8,128)}, u32[]{:S(2)}) copy-start(f32[128,176]{0,1:T(8,128)} %param.19) | copy-start | bytes 270340
  12.7 88.4 %copy-start.13 = (f32[128,176]{0,1:T(8,128)S(1)}, f32[128,176]{0,1:T(8,128)}, u32[]{:S(2)}) copy-start(f32[128,176]{0,1:T(8,128)} %param.17) | copy-start | bytes 270340
  12.7 88.5 %copy-start.14 = (f32[128,176]{0,1:T(8,128)S(1)}, f32[128,176]{0,1:T(8,128)}, u32[]{:S(2)}) copy-start(f32[128,176]{0,1:T(8,128)} %param.26) | copy-start | bytes 270340
  12.7 88.5 %copy-start.15 = (f32[128,176]{0,1:T(8,128)S(1)}, f32[128,176]{0,1:T(8,128)}, u32[]{:S(2)}) copy-start(f32[128,176]{0,1:T(8,128)} %param.24) | copy-start | bytes 270340
  13.7 134.1 %all-to-all-start = ((bf16[32,96,128]{2,1,0:T(8,128)(2,1)}), bf16[32,96,128]{2,1,0:T(8,128)(2,1)S(1)}, u32[]{:S(2)}, u32[]{:S(2)}) async-start(bf16[32,96,128]{2,1,0:T(8,128)(2,1)} %shard_map.145), calls=%async_computation | async-start | bytes 1572864 | tf_op jit(solution)/shard_map/all_to_all | solution.py:192
  100.9 122.1 %all-gather.3.cloned.1.call-start = ((), (), s32[]{:S(2)}) async-start(), calls=%async_computation.5 | async-start | bytes 2297856 | tf_op jit(solution)/shard_map/all_gather | solution.py:195
  147.8 11.6 %copy-start.16 = (f32[176,128]{1,0:T(8,128)S(1)}, f32[176,128]{1,0:T(8,128)}, u32[]{:S(2)}) copy-start(f32[176,128]{1,0:T(8,128)} %param.28) | copy-start | bytes 270340
  147.8 15.6 %copy-start.3 = (f32[64]{0:T(128)S(1)}, f32[64]{0:T(128)}, u32[]{:S(2)}) copy-start(f32[64]{0:T(128)} %param.16) | copy-start | bytes 772
  149.9 13.4 %collective-permute-start = (bf16[16,528,128]{2,1,0:T(8,128)(2,1)S(1)}, bf16[16,528,128]{2,1,0:T(8,128)(2,1)}, u32[]{:S(2)}, u32[]{:S(2)}) collective-permute-start(bf16[16,528,128]{2,1,0:T(8,128)(2,1)S(1)} %multiply_convert_fusion.own_ref), channel_id=1, source_target_pairs={{0,1},{1,0},{2,3},{3,2},{4,5},{5,4},{6,7},{7,6},{8,9},{9,8},{10,11... | collective-permute-start | bytes 6488072 | tf_op jit(solution)/shard_map/ppermute | solution.py:202
  223.0 36.9 %collective-permute-start.1 = (bf16[16,528,128]{2,1,0:T(8,128)(2,1)}, bf16[16,528,128]{2,1,0:T(8,128)(2,1)S(1)}, u32[]{:S(2)}, u32[]{:S(2)}) collective-permute-start(bf16[16,528,128]{2,1,0:T(8,128)(2,1)} %all-gather.3.cloned.1.call-done.own_ref), channel_id=1, source_target_pairs={{0,1},{1,0},{2,3},{3,2},{4,5},{5,4},{6,7},{7,6},{8,9},{9,8},{10,11... | collective-permute-start | bytes 6488072 | tf_op jit(solution)/shard_map/ppermute | solution.py:230
  259.9 1.6 copy-start
  276.3 19.7 %all-to-all-start.4 = ((bf16[4,128,128]{2,1,0:T(8,128)(2,1)}), bf16[4,128,128]{2,1,0:T(8,128)(2,1)S(1)}, u32[]{:S(2)}, u32[]{:S(2)}) async-start(bf16[4,128,128]{2,1,0:T(8,128)(2,1)} %shard_map.150), calls=%async_computation.4 | async-start | bytes 262144 | tf_op jit(solution)/shard_map/all_to_all | solution.py:221
  296.3 12.9 %collective-permute-start.2 = (bf16[64,128]{1,0:T(8,128)(2,1)S(1)}, bf16[64,128]{1,0:T(8,128)(2,1)S(1)}, u32[]{:S(2)}, u32[]{:S(2)}) collective-permute-start(bf16[64,128]{1,0:T(8,128)(2,1)S(1)} %constant_dynamic-slice_fusion), channel_id=1, source_target_pairs={{0,1},{1,0},{2,3},{3,2},{4,5},{5,4},{6,7},{7,6},{8,9},{9,8},{10,11... | collective-permute-start | bytes 49160 | tf_op jit(solution)/shard_map/ppermute | solution.py:237
Sparse Core Ops, SparseCore 0:
  160.2 62.7 all-gather.2

commit v3 on v2

--- a/solution.py
+++ b/solution.py
@@ -32,15 +32,26 @@
     return jnp.concatenate([a, fill], axis=1)
 
 
-def prep_kernel(t_ref, g1, g2, d1, d2, s1, s2, s3, s4, out_ref, ext):
+def prep_kernel(t_hbm, *refs):
+    count = 8
+    sources, out_ref = refs[:count], refs[count]
+    t_ref, held, ext, sems = refs[count + 1], refs[count + 2 : 2 * count + 2], *refs[-2:]
     peers, rows, half = out_ref.shape
-    feats = t_ref.shape[0]
+    feats = t_hbm.shape[0]
+    copies = [pltpu.make_async_copy(t_hbm, t_ref, sems.at[count])]
+    for k in range(count):
+        copies.append(pltpu.make_async_copy(sources[k], held[k], sems.at[k]))
+    for copy in copies:
+        copy.start()
     ext[...] = jnp.zeros_like(ext)
-    for k, (a, b) in enumerate(((g1, g2), (d1, d2))):
-        for p, (u, v) in enumerate(zip(split3(a[...]), split3(b[...]))):
+    for copy in copies:
+        copy.wait()
+    vecs = [ref[...] for ref in held]
+    for k in range(2):
+        for p, (u, v) in enumerate(zip(split3(vecs[2 * k]), split3(vecs[2 * k + 1]))):
             ext[3 * k + p : 3 * k + p + 1, :] = wide_row(jnp.concatenate([u, v], axis=1))
-    for j, ref in enumerate((s1, s2, s3, s4)):
-        for p, u in enumerate(split3(ref[...])):
+    for j in range(4):
+        for p, u in enumerate(split3(vecs[4 + j])):
             at = 8 + 8 * p + 2 * j
             ext[at : at + 1, :] = u[:, :LANE]
             ext[at + 1 : at + 2, :] = wide_row(u[:, LANE:])
@@ -106,31 +117,48 @@
         part = lax.dot_general(
             lhs, hidden, (((0,), (0,)), ((), ())), preferred_element_type=F32
         )
-        out_ref[z % SIDE, z // SIDE] = part.astype(BF)
-
-
-def chip_column(got, y, block, feats):
-    cols = []
-    for c in range(CORES):
-        rows = got[y * CORES + c, feats : feats + 8, :].astype(F32)
-        row = rows[3:4] + rows[4:5] + rows[5:6]
-        turned = jnp.transpose(jnp.broadcast_to(row, (8, LANE)))
-        cols.append(turned[block * feats : (block + 1) * feats, 0:1])
-    return jnp.concatenate(cols, axis=0)
-
-
-def close_kernel(block, sums, got, mid_ref, out_ref):
+        if block == 0:
+            out_ref[z % SIDE, z // SIDE] = part.astype(BF)
+        else:
+            out_ref[z] = part.astype(BF)
+
+
+def down_column(got, peer, block, feats):
+    rows = got[peer, feats : feats + 8, :].astype(F32)
+    row = rows[3:4] + rows[4:5] + rows[5:6]
+    turned = jnp.transpose(jnp.broadcast_to(row, (8, LANE)))
+    return turned[block * feats : (block + 1) * feats, 0:1]
+
+
+def middle_kernel(sums, got, mid_ref, there_ref):
     feats = got.shape[1] - EXTRA
     y = lax.axis_index("y")
+    core = lax.axis_index("c")
     total = sums[0].astype(F32)
     for k in range(1, sums.shape[0]):
         total = total + sums[k].astype(F32)
-    if block == 0:
-        resid = jnp.concatenate([got[y * CORES + c, :feats, :] for c in range(CORES)], axis=0)
-    else:
-        resid = mid_ref[...]
-    scale = chip_column(got, y, block, feats)
-    out_ref[...] = (resid.astype(F32) + 0.5 * total * scale).astype(BF)
+    for c in range(CORES):
+        peer = y * CORES + c
+        resid = got[peer, :feats, :].astype(F32)
+        scale = down_column(got, peer, 0, feats)
+        part = total[c * feats : (c + 1) * feats]
+        mid_ref[c * feats : (c + 1) * feats, :] = (resid + 0.5 * part * scale).astype(BF)
+    there_ref[...] = mid_ref[pl.ds((1 - core) * feats, feats), :]
+
+
+def last_kernel(sums, got, mid_ref, other_ref, out_ref):
+    feats = got.shape[1] - EXTRA
+    half = got.shape[2]
+    core = lax.axis_index("c")
+    scale = down_column(got, lax.axis_index("y") * CORES + core, 1, feats)
+    here = mid_ref[pl.ds(core * feats, feats), :].astype(F32)
+    other = other_ref[...].astype(F32)
+    for c in range(CORES):
+        total = sums[c].astype(F32)
+        for k in range(CORES + c, sums.shape[0], CORES):
+            total = total + sums[k].astype(F32)
+        resid = jnp.where(core == c, here, other)
+        out_ref[:, c * half : (c + 1) * half] = (resid + 0.5 * total * scale).astype(BF)
 
 
 def partial_kernel(got, out_ref):
@@ -140,20 +168,17 @@
     out_ref[...] = total.astype(BF)
 
 
-def call(kernel, out, args, scratch=(), flops=1000, limit=4 << 20):
+def call(kernel, out, args, scratch=(), flops=1000, limit=4 << 20, space=pltpu.VMEM):
+    specs = jax.tree.map(lambda _: VMEM, out)
     return pl.pallas_call(
         kernel,
         out_shape=out,
-        in_specs=[VMEM] * len(args),
-        out_specs=VMEM,
+        in_specs=[pl.BlockSpec(memory_space=space)] * len(args),
+        out_specs=specs,
         scratch_shapes=list(scratch),
         compiler_params=pltpu.CompilerParams(vmem_limit_bytes=limit),
         cost_estimate=pl.CostEstimate(flops=flops, bytes_accessed=1 << 20, transcendentals=0),
     )(*args)
-
-
-def own_rows(gate, up, down):
-    return jnp.concatenate([gate.T, up.T, down], axis=0)
 
 
 def body(
@@ -187,25 +212,32 @@
         prep_kernel,
         jax.ShapeDtypeStruct((peers, feats + EXTRA, half), BF),
         (tokens.T, *vecs),
-        [pltpu.VMEM((EXTRA, LANE), F32)],
+        [
+            pltpu.VMEM((feats, mine), BF),
+            *(pltpu.VMEM(v.shape, F32) for v in vecs),
+            pltpu.VMEM((EXTRA, LANE), F32),
+            pltpu.SemaphoreType.DMA((len(vecs) + 1,)),
+        ],
+        limit=56 << 20,
+        space=pltpu.HBM,
     )
     got = lax.all_to_all(sent, ("y", "c"), 0, 0, tiled=True)
 
-    own_2 = own_rows(gate_2, up_2, down_2).astype(BF)
-    own_2 = lax.all_gather(own_2, "fs", axis=0)
-
-    own_1 = own_rows(gate_1, up_1, down_1).astype(BF)
-    own_1 = (own_1.astype(F32) * UP).astype(jnp.float16)
-    own_1 = lax.all_gather(own_1, "fs", axis=0)
-    own_1, got = lax.optimization_barrier((own_1, got))
-    own_1 = (own_1.astype(F32) * (1.0 / UP)).astype(BF)
-    sib_1 = lax.ppermute(own_1, "c", SWAP)
-
-    def ffn(block, s, own, sib):
+    own = jnp.concatenate([gate_1.T, up_1.T, down_1, gate_2.T, up_2.T, down_2], axis=0)
+    own = (own.astype(BF).astype(F32) * UP).astype(jnp.float16)
+    own = lax.all_gather(own, "fs", axis=0)
+    own, got = lax.optimization_barrier((own, got))
+    both = [
+        (own[:, k * 3 * hid : (k + 1) * 3 * hid].astype(F32) * (1.0 / UP)).astype(BF)
+        for k in range(2)
+    ]
+    sib = [lax.ppermute(w, "c", SWAP) for w in both]
+
+    def ffn(block, s, shape):
         return call(
             functools.partial(ffn_kernel, hid, block),
-            jax.ShapeDtypeStruct((SIDE, ny // SIDE, chip, half), BF),
-            (s, got, own, sib),
+            jax.ShapeDtypeStruct((*shape, chip, half), BF),
+            (s, got, both[block], sib[block]),
             [
                 pltpu.VMEM((peers * feats, half), BF),
                 pltpu.VMEM((CORES * hid, half), BF),
@@ -215,29 +247,23 @@
             limit=16 << 20,
         )
 
-    def reduced(block, part, mid):
-        step = lax.all_to_all(part, "y", 0, 0, axis_index_groups=near, tiled=True)
-        step = call(partial_kernel, jax.ShapeDtypeStruct(step.shape[1:], BF), (step,))
-        step = lax.all_to_all(step, "y", 0, 0, axis_index_groups=far, tiled=True)
-        return call(
-            functools.partial(close_kernel, block),
-            jax.ShapeDtypeStruct((chip, half), BF),
-            (step, got, mid),
-        )
-
-    middle = reduced(0, ffn(0, gain_1[None], own_1, sib_1), gain_1[None])
-    own_2, middle = lax.optimization_barrier((own_2, middle))
-    sib_2 = lax.ppermute(own_2, "c", SWAP)
+    step = ffn(0, jnp.zeros((8, LANE), BF), (SIDE, ny // SIDE))
+    step = lax.all_to_all(step, "y", 0, 0, axis_index_groups=near, tiled=True)
+    step = call(partial_kernel, jax.ShapeDtypeStruct(step.shape[1:], BF), (step,))
+    step = lax.all_to_all(step, "y", 0, 0, axis_index_groups=far, tiled=True)
+    middle, there = call(
+        middle_kernel,
+        (jax.ShapeDtypeStruct((chip, half), BF), jax.ShapeDtypeStruct((feats, half), BF)),
+        (step, got),
+    )
+    other = lax.ppermute(there, "c", SWAP)
     whole = lax.all_gather(middle, "y", axis=0, tiled=True)
-    last = reduced(1, ffn(1, whole, own_2, sib_2), middle)
-
-    core = lax.axis_index("c")
-    there = lax.dynamic_slice_in_dim(last, (1 - core) * feats, feats, 0)
-    here = lax.dynamic_slice_in_dim(last, core * feats, feats, 0)
-    other = lax.ppermute(there, "c", SWAP)
-    first = core == 0
-    both = [jnp.where(first, here, other), jnp.where(first, other, here)]
-    return jnp.concatenate(both, axis=1).T
+    step = ffn(1, whole, (ny,)).reshape(peers, feats, half)
+    step = lax.all_to_all(step, ("y", "c"), 0, 0, tiled=True)
+    out = call(
+        last_kernel, jax.ShapeDtypeStruct((feats, mine), BF), (step, got, middle, other)
+    )
+    return out.T
 
 
 def solution(mesh):

time: 317 us -> 289 us (0.912)
  blocking collectives: 124 us -> 108 us
  waiting for transfers between devices: 32.4 us -> 46 us
  between operations: 13.6 us -> 0.18 us
  local copies, waits for them, and re-layouts: 7.74 us -> 0.03 us
  starting transfers between devices: 128 us -> 121 us
    all_to_all x1 -> x2, waiting for transfers between devices: 12 us -> 41.3 us  [the longest x1 29.8 us: body(): step = lax.all_to_all(step, ('y', 'c'), 0, 0, tiled=True)]
    all_to_all x3 -> x1, blocking collectives: 51.9 us -> 23 us  [body(): step = lax.all_to_all(step, 'y', 0, 0, axis_index_groups=far, tiled=True)]
    all_gather x1 -> x0, waiting for transfers between devices: 16.3 us -> none  [body(): own_2 = lax.all_gather(own_2, 'fs', axis=0)]
    all_gather x1, blocking collectives: 46.6 us -> 62.5 us  [body(): own = lax.all_gather(own, 'fs', axis=0)]
    all_to_all x1 -> x2, starting transfers between devices: 7.68 us -> 20.1 us  [the longest x1 15.7 us: body(): step = lax.all_to_all(step, ('y', 'c'), 0, 0, tiled=True)]
    ppermute x2, starting transfers between devices: 21 us -> 11.1 us  [body(): sib = [lax.ppermute(w, 'c', SWAP) for w in both]]
    ppermute x1, starting transfers between devices: 12.1 us -> 2.64 us  [body(): other = lax.ppermute(there, 'c', SWAP)]
    unnamed x34 -> x12, local copies, waits for them, and re-layouts: 7.73 us -> 0.02 us
  transfers between devices with their start and end apart: 6 -> 6, of which waited for: 4 -> 4; matrix products, arithmetic and copies ran while one was open for 0% -> 0% of each run, Pallas kernels for 1% -> 0%
where the time goes in v3:
time: 289 us; the launch traced here: 288 us
  starting transfers between devices  121 us (42%)
  blocking collectives  108 us (37%)
  waiting for transfers between devices  46 us (16%)
  Pallas kernels  9.75 us (3%)
  other arithmetic  3.4 us (1%)
    all_to_all x1, starting transfers between devices, body(): got = lax.all_to_all(sent, ('y', 'c'), 0, 0, tiled=True)  87.3 us
    all_gather x1, blocking collectives, body(): own = lax.all_gather(own, 'fs', axis=0)  62.5 us
    all_to_all x1, waiting for transfers between devices, body(): step = lax.all_to_all(step, ('y', 'c'), 0, 0, tiled=True)  29.8 us
    all_to_all x1, blocking collectives, body(): step = lax.all_to_all(step, 'y', 0, 0, axis_index_groups=far, tiled=True)  23 us
    all_gather x1, blocking collectives, body(): whole = lax.all_gather(middle, 'y', axis=0, tiled=True)  22.6 us
    all_to_all x1, starting transfers between devices, body(): step = lax.all_to_all(step, ('y', 'c'), 0, 0, tiled=True)  15.7 us
    all_to_all x1, waiting for transfers between devices, body(): step = lax.all_to_all(step, 'y', 0, 0, axis_index_groups=near, tiled=True)  11.5 us
    ppermute x2, starting transfers between devices, body(): sib = [lax.ppermute(w, 'c', SWAP) for w in both]  11.1 us
  transfers between devices with their start and end apart: 6, of which 4 were waited for; matrix products, arithmetic and copies ran while one was open for 0% of the time, Pallas kernels for 0%

profile of v3, /device:TPU:5, one launch (start us, length us, event | category | flops | bytes accessed | tf_op | source)
XLA Modules:
  0.0 288.4 jit_solution(11666097808237723682)
XLA Ops:
  0.0 0.0 copy-start
  0.0 0.0 copy-start.1
  0.0 0.0 copy-start.2
  0.0 0.0 copy-start.3
  0.0 0.0 copy-start.4
  0.0 0.0 copy-start.5
  0.0 1.9 shard_map.145
  1.9 87.3 %all-to-all-start = ((bf16[32,96,128]{2,1,0:T(8,128)(2,1)}), bf16[32,96,128]{2,1,0:T(8,128)(2,1)S(1)}, u32[]{:S(2)}, u32[]{:S(2)}) async-start(bf16[32,96,128]{2,1,0:T(8,128)(2,1)} %shard_map.145), calls=%async_computation | async-start | bytes 1572864 | tf_op jit(solution)/shard_map/all_to_all | solution.py:224
  89.2 0.0 copy-done
  89.2 0.0 copy-done.1
  89.3 0.0 copy-done.2
  89.3 0.0 copy-done.3
  89.3 0.0 copy-done.4
  89.4 0.0 copy-done.5
  89.4 0.1 multiply_convert_fusion.2
  89.5 62.5 %all-gather.1 = f16[16,1056,128]{2,1,0:T(8,128)(2,1)} all-gather(f16[1,1056,128]{2,1,0:T(8,128)(2,1)S(1)} %multiply_convert_fusion.2), channel_id=1, replica_groups=mesh['grp'=2,'fs'=16,'y'=16,'c'=2] {'fs'}, dimensions={0}, use_global_device_ids=true | all-gather | bytes 4595712 | tf_op jit(solution)/shard_map/all_gather | solution.py:228
  151.9 0.0 all-to-all-done.got
  151.9 3.2 %multiply_convert_fusion = (bf16[16,528,128]{2,1,0:T(8,128)(2,1)S(1)}, bf16[16,528,128]{2,1,0:T(8,128)(2,1)S(1)}) fusion(f16[16,1056,128]{2,1,0:T(8,128)(2,1)} %all-gather.1), kind=kLoop, calls=%fused_computation | loop fusion | flops 6488064 | bytes 8650752 | tf_op jit(solution)/shard_map/convert_element_type | solution.py:231
  155.2 8.5 %collective-permute-start = (bf16[16,528,128]{2,1,0:T(8,128)(2,1)S(1)}, bf16[16,528,128]{2,1,0:T(8,128)(2,1)S(1)}, u32[]{:S(2)}, u32[]{:S(2)}) collective-permute-start(bf16[16,528,128]{2,1,0:T(8,128)(2,1)S(1)} %get-tuple-element.14.own_ref), channel_id=1, source_target_pairs={{0,1},{1,0},{2,3},{3,2},{4,5},{5,4},{6,7},{7,6},{8,9},{9,8},{10,11... | collective-permute-start | bytes 6488072 | tf_op jit(solution)/shard_map/ppermute | solution.py:234
  163.7 3.9 %collective-permute-done.sib_ref = bf16[16,528,128]{2,1,0:T(8,128)(2,1)S(1)} collective-permute-done((bf16[16,528,128]{2,1,0:T(8,128)(2,1)S(1)}, bf16[16,528,128]{2,1,0:T(8,128)(2,1)S(1)}, u32[]{:S(2)}, u32[]{:S(2)}) %collective-permute-start) | collective-permute-done | bytes 2162720 | tf_op jit(solution)/shard_map/ppermute | solution.py:234
  167.6 2.6 shard_map.146
  170.2 4.3 %all-to-all-start.1 = ((bf16[4,4,128,128]{3,2,1,0:T(8,128)(2,1)}), bf16[4,4,128,128]{3,2,1,0:T(8,128)(2,1)S(1)}, u32[]{:S(2)}, u32[]{:S(2)}) async-start(bf16[4,4,128,128]{3,2,1,0:T(8,128)(2,1)} %shard_map.146), calls=%async_computation.1 | async-start | bytes 1048576 | tf_op jit(solution)/shard_map/all_to_all | solution.py:251
  174.5 2.6 collective-permute-start.1
  177.1 11.5 %all-to-all-done.1.got = bf16[4,4,128,128]{3,2,1,0:T(8,128)(2,1)S(1)} async-done(((bf16[4,4,128,128]{3,2,1,0:T(8,128)(2,1)}), bf16[4,4,128,128]{3,2,1,0:T(8,128)(2,1)S(1)}, u32[]{:S(2)}, u32[]{:S(2)}) %all-to-all-start.1) | async-done | bytes 524320 | tf_op jit(solution)/shard_map/all_to_all | solution.py:251
  188.6 0.1 shard_map.147
  188.6 23.0 %all_to_all.20.sums = bf16[4,128,128]{2,1,0:T(8,128)(2,1)S(1)} all-to-all(bf16[4,128,128]{2,1,0:T(8,128)(2,1)S(1)} %shard_map.147), channel_id=1, replica_groups={{0,8,16,24},{2,10,18,26},{4,12,20,28},{6,14,22,30},{1,9,17,25},{3,11,19..., dimensions={0} | all-to-all | bytes 262144 | tf_op jit(solution)/shard_map/all_to_all | solution.py:253
  211.6 0.2 shard_map.148
  211.8 22.6 %all_gather.8.s_ref = bf16[2048,128]{1,0:T(8,128)(2,1)S(1)} all-gather(bf16[128,128]{1,0:T(8,128)(2,1)S(1)} %get-tuple-element.11.mid_ref), channel_id=1, replica_groups=mesh['grp'=2,'fs'=16,'y'=16,'c'=2] {'y'}, dimensions={0}, use_global_device_ids=true | all-gather | bytes 557056 | tf_op jit(solution)/shard_map/all_gather | solution.py:260
  234.3 0.0 collective-permute-done.1.sib_ref
  234.3 4.2 %shard_map.149 = bf16[16,128,128]{2,1,0:T(8,128)(2,1)} custom-call(bf16[2048,128]{1,0:T(8,128)(2,1)S(1)} %all_gather.8.s_ref, bf16[32,96,128]{2,1,0:T(8,128)(2,1)S(1)} %all-to-all-done.got, bf16[16,528,128]{2,1,0:T(8,128)(2,1)S(1)} %get-tuple-element.13.own_ref, bf16[16,528,128]{2,1,0:T(8,128)(2,1)} %collective-permute-done.1.sib_ref), custom_call_target="tpu_custom_call" | custom-call | flops 553648128 | bytes 1048576 | tf_op jit(solution)/shard_map/pallas_call | solution.py:173
  238.6 15.7 %all-to-all-start.3 = ((bf16[32,64,128]{2,1,0:T(8,128)(2,1)}), bf16[32,64,128]{2,1,0:T(8,128)(2,1)S(1)}, u32[]{:S(2)}, u32[]{:S(2)}) async-start(bf16[32,64,128]{2,1,0:T(8,128)(2,1)} %bitcast.19), calls=%async_computation.3 | async-start | bytes 1048576 | tf_op jit(solution)/shard_map/all_to_all | solution.py:262
  254.3 2.6 collective-permute-start.2
  257.0 0.8 collective-permute-done.2.other_ref
  257.8 29.8 %all-to-all-done.3.sums = bf16[32,64,128]{2,1,0:T(8,128)(2,1)S(1)} async-done(((bf16[32,64,128]{2,1,0:T(8,128)(2,1)}), bf16[32,64,128]{2,1,0:T(8,128)(2,1)S(1)}, u32[]{:S(2)}, u32[]{:S(2)}) %all-to-all-start.3) | async-done | bytes 524320 | tf_op jit(solution)/shard_map/all_to_all | solution.py:262
  287.6 0.8 shard_map.150
  (7 shorter events, 0.1 us)
Async XLA Ops:
  0.0 89.2 %copy-start = (f32[128,176]{0,1:T(8,128)S(1)}, f32[128,176]{0,1:T(8,128)}, u32[]{:S(2)}) copy-start(f32[128,176]{0,1:T(8,128)} %param.17) | copy-start | bytes 270340
  0.0 89.2 %copy-start.1 = (f32[128,176]{0,1:T(8,128)S(1)}, f32[128,176]{0,1:T(8,128)}, u32[]{:S(2)}) copy-start(f32[128,176]{0,1:T(8,128)} %param.19) | copy-start | bytes 270340
  0.0 89.3 %copy-start.2 = (f32[176,128]{1,0:T(8,128)S(1)}, f32[176,128]{1,0:T(8,128)}, u32[]{:S(2)}) copy-start(f32[176,128]{1,0:T(8,128)} %param.21) | copy-start | bytes 270340
  0.0 89.3 %copy-start.3 = (f32[128,176]{0,1:T(8,128)S(1)}, f32[128,176]{0,1:T(8,128)}, u32[]{:S(2)}) copy-start(f32[128,176]{0,1:T(8,128)} %param.24) | copy-start | bytes 270340
  0.0 89.3 %copy-start.4 = (f32[128,176]{0,1:T(8,128)S(1)}, f32[128,176]{0,1:T(8,128)}, u32[]{:S(2)}) copy-start(f32[128,176]{0,1:T(8,128)} %param.26) | copy-start | bytes 270340
  0.0 89.3 %copy-start.5 = (f32[176,128]{1,0:T(8,128)S(1)}, f32[176,128]{1,0:T(8,128)}, u32[]{:S(2)}) copy-start(f32[176,128]{1,0:T(8,128)} %param.28) | copy-start | bytes 270340
  1.9 150.0 %all-to-all-start = ((bf16[32,96,128]{2,1,0:T(8,128)(2,1)}), bf16[32,96,128]{2,1,0:T(8,128)(2,1)S(1)}, u32[]{:S(2)}, u32[]{:S(2)}) async-start(bf16[32,96,128]{2,1,0:T(8,128)(2,1)} %shard_map.145), calls=%async_computation | async-start | bytes 1572864 | tf_op jit(solution)/shard_map/all_to_all | solution.py:224
  155.2 12.4 %collective-permute-start = (bf16[16,528,128]{2,1,0:T(8,128)(2,1)S(1)}, bf16[16,528,128]{2,1,0:T(8,128)(2,1)S(1)}, u32[]{:S(2)}, u32[]{:S(2)}) collective-permute-start(bf16[16,528,128]{2,1,0:T(8,128)(2,1)S(1)} %get-tuple-element.14.own_ref), channel_id=1, source_target_pairs={{0,1},{1,0},{2,3},{3,2},{4,5},{5,4},{6,7},{7,6},{8,9},{9,8},{10,11... | collective-permute-start | bytes 6488072 | tf_op jit(solution)/shard_map/ppermute | solution.py:234
  170.2 18.4 %all-to-all-start.1 = ((bf16[4,4,128,128]{3,2,1,0:T(8,128)(2,1)}), bf16[4,4,128,128]{3,2,1,0:T(8,128)(2,1)S(1)}, u32[]{:S(2)}, u32[]{:S(2)}) async-start(bf16[4,4,128,128]{3,2,1,0:T(8,128)(2,1)} %shard_map.146), calls=%async_computation.1 | async-start | bytes 1048576 | tf_op jit(solution)/shard_map/all_to_all | solution.py:251
  174.5 59.8 %collective-permute-start.1 = (bf16[16,528,128]{2,1,0:T(8,128)(2,1)S(1)}, bf16[16,528,128]{2,1,0:T(8,128)(2,1)}, u32[]{:S(2)}, u32[]{:S(2)}) collective-permute-start(bf16[16,528,128]{2,1,0:T(8,128)(2,1)S(1)} %get-tuple-element.13.own_ref), channel_id=1, source_target_pairs={{0,1},{1,0},{2,3},{3,2},{4,5},{5,4},{6,7},{7,6},{8,9},{9,8},{10,11... | collective-permute-start | bytes 6488072 | tf_op jit(solution)/shard_map/ppermute | solution.py:234
  238.6 49.0 %all-to-all-start.3 = ((bf16[32,64,128]{2,1,0:T(8,128)(2,1)}), bf16[32,64,128]{2,1,0:T(8,128)(2,1)S(1)}, u32[]{:S(2)}, u32[]{:S(2)}) async-start(bf16[32,64,128]{2,1,0:T(8,128)(2,1)} %bitcast.19), calls=%async_computation.3 | async-start | bytes 1048576 | tf_op jit(solution)/shard_map/all_to_all | solution.py:262
  254.3 3.5 %collective-permute-start.2 = (bf16[64,128]{1,0:T(8,128)(2,1)S(1)}, bf16[64,128]{1,0:T(8,128)(2,1)S(1)}, u32[]{:S(2)}, u32[]{:S(2)}) collective-permute-start(bf16[64,128]{1,0:T(8,128)(2,1)S(1)} %get-tuple-element.12), channel_id=1, source_target_pairs={{0,1},{1,0},{2,3},{3,2},{4,5},{5,4},{6,7},{7,6},{8,9},{9,8},{10,11... | collective-permute-start | bytes 49160 | tf_op jit(solution)/shard_map/ppermute | solution.py:259

commit v4 on v3

--- a/solution.py
+++ b/solution.py
@@ -23,6 +23,15 @@
     hi = v.astype(BF).astype(F32)
     mid = (v - hi).astype(BF).astype(F32)
     return hi, mid, v - hi - mid
+
+
+def chip_index():
+    return lax.axis_index("yh") * SIDE + lax.axis_index("yl")
+
+
+def seat(other):
+    core = lax.axis_index("c")
+    return chip_index() * CORES + (1 - core if other else core)
 
 
 def wide_row(a):
@@ -74,14 +83,11 @@
     return cols
 
 
-def ffn_kernel(hid, block, s_ref, got, own_ref, sib_ref, out_ref, h_ref, hd_ref, g_ref):
+def normalize(block, s_ref, got, h_ref, g_ref):
     peers = got.shape[0]
     feats = got.shape[1] - EXTRA
     tokens = got.shape[2]
-    chunks, _, lane = own_ref.shape
     width = feats * peers
-    me = lax.axis_index("y") * CORES + lax.axis_index("c")
-    sib = lax.axis_index("y") * CORES + 1 - lax.axis_index("c")
     for p in range(peers):
         rows = got[p, feats : feats + 8, :].astype(F32)
         g_ref[p : p + 1, :] = rows[0:1] + rows[1:2] + rows[2:3]
@@ -100,27 +106,59 @@
     r = lax.rsqrt(jnp.sum(total, axis=0, keepdims=True) / float(width) + epsilon)
     for p in range(peers):
         h_ref[pl.ds(p * feats, feats), :] = (piece(p) * r * gains[:, p : p + 1]).astype(BF)
-    for k, (w, peer) in enumerate(((own_ref, me), (sib_ref, sib))):
-        sg, su = vec_column(got, peer, (2 * block, 2 * block + 1), feats, block, hid)
-        acc = jnp.zeros((2 * hid, tokens), F32)
-        for z in range(0, chunks, 2):
-            lhs = jnp.concatenate([w[z, : 2 * hid, :], w[z + 1, : 2 * hid, :]], axis=1)
-            acc = acc + jnp.dot(
-                lhs, h_ref[pl.ds(z * lane, 2 * lane), :], preferred_element_type=F32
-            )
-        gate = acc[:hid] * sg
-        up = acc[hid:] * su
-        hd_ref[pl.ds(k * hid, hid), :] = (gate / (1.0 + jnp.exp(-gate)) * up).astype(BF)
-    hidden = hd_ref[...]
-    for z in range(chunks):
-        lhs = jnp.concatenate([own_ref[z, 2 * hid :, :], sib_ref[z, 2 * hid :, :]], axis=0)
+
+
+def hidden_of(hid, block, w, peer, got, h_ref):
+    feats = got.shape[1] - EXTRA
+    chunks, _, lane = w.shape
+    sg, su = vec_column(got, peer, (2 * block, 2 * block + 1), feats, block, hid)
+    acc = jnp.zeros((2 * hid, got.shape[2]), F32)
+    for z in range(0, chunks, 2):
+        lhs = jnp.concatenate([w[z, : 2 * hid, :], w[z + 1, : 2 * hid, :]], axis=1)
+        acc = acc + jnp.dot(
+            lhs, h_ref[pl.ds(z * lane, 2 * lane), :], preferred_element_type=F32
+        )
+    gate = acc[:hid] * sg
+    up = acc[hid:] * su
+    return (gate / (1.0 + jnp.exp(-gate)) * up).astype(BF)
+
+
+def down_blocks(hid, own_ref, sib_ref, hidden, store):
+    for z in range(own_ref.shape[0]):
+        rows = slice(2 * hid, 3 * hid)
+        lhs = jnp.concatenate([own_ref[z, rows, :], sib_ref[z, rows, :]], axis=0)
         part = lax.dot_general(
             lhs, hidden, (((0,), (0,)), ((), ())), preferred_element_type=F32
         )
-        if block == 0:
-            out_ref[z % SIDE, z // SIDE] = part.astype(BF)
-        else:
-            out_ref[z] = part.astype(BF)
+        store(z, part.astype(BF))
+
+
+def first_half_kernel(hid, got, own_ref, h_ref, hd_ref, g_ref):
+    normalize(0, None, got, h_ref, g_ref)
+    hd_ref[...] = hidden_of(hid, 0, own_ref, seat(0), got, h_ref)
+
+
+def second_half_kernel(hid, got, h_ref, hd_own, own_ref, sib_ref, out_ref, hd_ref):
+    hd_ref[:hid, :] = hd_own[...]
+    hd_ref[hid:, :] = hidden_of(hid, 0, sib_ref, seat(1), got, h_ref)
+
+    def store(z, part):
+        out_ref[z % SIDE, z // SIDE] = part
+
+    down_blocks(hid, own_ref, sib_ref, hd_ref[...], store)
+
+
+def second_block_kernel(hid, s_ref, got, own_ref, sib_ref, out_ref, h_ref, hd_ref, g_ref):
+    feats = got.shape[1] - EXTRA
+    normalize(1, s_ref, got, h_ref, g_ref)
+    hd_ref[:hid, :] = hidden_of(hid, 1, own_ref, seat(0), got, h_ref)
+    hd_ref[hid:, :] = hidden_of(hid, 1, sib_ref, seat(1), got, h_ref)
+
+    def store(z, part):
+        for c in range(CORES):
+            out_ref[z % SIDE * CORES + c, z // SIDE] = part[c * feats : (c + 1) * feats]
+
+    down_blocks(hid, own_ref, sib_ref, hd_ref[...], store)
 
 
 def down_column(got, peer, block, feats):
@@ -132,7 +170,7 @@
 
 def middle_kernel(sums, got, mid_ref, there_ref):
     feats = got.shape[1] - EXTRA
-    y = lax.axis_index("y")
+    y = chip_index()
     core = lax.axis_index("c")
     total = sums[0].astype(F32)
     for k in range(1, sums.shape[0]):
@@ -150,13 +188,13 @@
     feats = got.shape[1] - EXTRA
     half = got.shape[2]
     core = lax.axis_index("c")
-    scale = down_column(got, lax.axis_index("y") * CORES + core, 1, feats)
+    scale = down_column(got, seat(0), 1, feats)
     here = mid_ref[pl.ds(core * feats, feats), :].astype(F32)
     other = other_ref[...].astype(F32)
     for c in range(CORES):
-        total = sums[c].astype(F32)
-        for k in range(CORES + c, sums.shape[0], CORES):
-            total = total + sums[k].astype(F32)
+        total = sums[0, c].astype(F32)
+        for k in range(1, sums.shape[0]):
+            total = total + sums[k, c].astype(F32)
         resid = jnp.where(core == c, here, other)
         out_ref[:, c * half : (c + 1) * half] = (resid + 0.5 * total * scale).astype(BF)
 
@@ -166,6 +204,15 @@
     for k in range(1, got.shape[0]):
         total = total + got[k].astype(F32)
     out_ref[...] = total.astype(BF)
+
+
+def last_partial_kernel(got, out_ref):
+    for c in range(CORES):
+        for i in range(out_ref.shape[0]):
+            total = got[c, i].astype(F32)
+            for k in range(CORES + c, got.shape[0], CORES):
+                total = total + got[k, i].astype(F32)
+            out_ref[i, c] = total.astype(BF)
 
 
 def call(kernel, out, args, scratch=(), flops=1000, limit=4 << 20, space=pltpu.VMEM):
@@ -198,14 +245,14 @@
     down_2,
     down_s2,
 ):
-    ny = lax.axis_size("y")
-    peers = ny * CORES
+    groups = lax.axis_size("grp")
+    group = lax.axis_index("grp")
+    far = lax.axis_size("yh")
+    peers = far * SIDE * CORES
     mine, feats = tokens.shape
     half = mine // CORES
     chip = feats * CORES
     hid = gate_1.shape[1]
-    near = [[SIDE * i + j for j in range(SIDE)] for i in range(ny // SIDE)]
-    far = [[j + SIDE * i for i in range(ny // SIDE)] for j in range(SIDE)]
 
     vecs = [v[None] for v in (gain_1, gain_2, down_s1, down_s2, gate_s1, up_s1, gate_s2, up_s2)]
     sent = call(
@@ -221,45 +268,80 @@
         limit=56 << 20,
         space=pltpu.HBM,
     )
-    got = lax.all_to_all(sent, ("y", "c"), 0, 0, tiled=True)
-
-    own = jnp.concatenate([gate_1.T, up_1.T, down_1, gate_2.T, up_2.T, down_2], axis=0)
+    got = lax.all_to_all(sent, ("yh", "yl", "c"), 0, 0, tiled=True)
+
+    rows = 3 * hid
+    share = -(-rows // (16 * groups)) * 16
+    own_2 = jnp.concatenate([gate_2.T, up_2.T, down_2], axis=0)
+    own_2 = jnp.pad(own_2, ((0, groups * share - rows), (0, 0)))
+    own_2 = lax.dynamic_slice_in_dim(own_2, group * share, share, 0)
+    own = jnp.concatenate([gate_1.T, up_1.T, down_1, own_2], axis=0)
     own = (own.astype(BF).astype(F32) * UP).astype(jnp.float16)
     own = lax.all_gather(own, "fs", axis=0)
     own, got = lax.optimization_barrier((own, got))
-    both = [
-        (own[:, k * 3 * hid : (k + 1) * 3 * hid].astype(F32) * (1.0 / UP)).astype(BF)
-        for k in range(2)
+
+    def restored(w):
+        return (w.astype(F32) * (1.0 / UP)).astype(BF)
+
+    own_1 = restored(own[:, :rows])
+    sib_1 = lax.ppermute(own_1, "c", SWAP)
+    width = peers * feats
+    h, hd = call(
+        functools.partial(first_half_kernel, hid),
+        (jax.ShapeDtypeStruct((width, half), BF), jax.ShapeDtypeStruct((hid, half), BF)),
+        (got, own_1),
+        [pltpu.VMEM((peers, LANE), F32)],
+        flops=4 * hid * width * half,
+        limit=16 << 20,
+    )
+    sib_1, h, hd = lax.optimization_barrier((sib_1, h, hd))
+    step = call(
+        functools.partial(second_half_kernel, hid),
+        jax.ShapeDtypeStruct((SIDE, far, chip, half), BF),
+        (got, h, hd, own_1, sib_1),
+        [pltpu.VMEM((CORES * hid, half), BF)],
+        flops=8 * hid * width * half,
+        limit=16 << 20,
+    )
+    later, step = lax.optimization_barrier((own[:, rows:], step))
+    later = restored(later)
+    slices = [later] + [
+        lax.ppermute(later, "grp", [(i, (i + r) % groups) for i in range(groups)])
+        for r in range(1, groups)
     ]
-    sib = [lax.ppermute(w, "c", SWAP) for w in both]
-
-    def ffn(block, s, shape):
-        return call(
-            functools.partial(ffn_kernel, hid, block),
-            jax.ShapeDtypeStruct((*shape, chip, half), BF),
-            (s, got, both[block], sib[block]),
-            [
-                pltpu.VMEM((peers * feats, half), BF),
-                pltpu.VMEM((CORES * hid, half), BF),
-                pltpu.VMEM((peers, LANE), F32),
-            ],
-            flops=12 * hid * peers * feats * half,
-            limit=16 << 20,
-        )
-
-    step = ffn(0, jnp.zeros((8, LANE), BF), (SIDE, ny // SIDE))
-    step = lax.all_to_all(step, "y", 0, 0, axis_index_groups=near, tiled=True)
+    step = lax.all_to_all(step, "yl", 0, 0, tiled=True)
     step = call(partial_kernel, jax.ShapeDtypeStruct(step.shape[1:], BF), (step,))
-    step = lax.all_to_all(step, "y", 0, 0, axis_index_groups=far, tiled=True)
+    step = lax.all_to_all(step, "yh", 0, 0, tiled=True)
+    slices, step = lax.optimization_barrier((slices, step))
+    own_2 = jnp.zeros((later.shape[0], groups * share, LANE), BF)
+    for r, w in enumerate(slices):
+        at = (group + groups - r) % groups * share
+        own_2 = lax.dynamic_update_slice_in_dim(own_2, w, at, 1)
+    sib_2 = lax.ppermute(own_2, "c", SWAP)
     middle, there = call(
         middle_kernel,
         (jax.ShapeDtypeStruct((chip, half), BF), jax.ShapeDtypeStruct((feats, half), BF)),
         (step, got),
     )
     other = lax.ppermute(there, "c", SWAP)
-    whole = lax.all_gather(middle, "y", axis=0, tiled=True)
-    step = ffn(1, whole, (ny,)).reshape(peers, feats, half)
-    step = lax.all_to_all(step, ("y", "c"), 0, 0, tiled=True)
+    whole = lax.all_gather(middle, ("yh", "yl"), axis=0, tiled=True)
+    step = call(
+        functools.partial(second_block_kernel, hid),
+        jax.ShapeDtypeStruct((SIDE * CORES, far, feats, half), BF),
+        (whole, got, own_2, sib_2),
+        [
+            pltpu.VMEM((width, half), BF),
+            pltpu.VMEM((CORES * hid, half), BF),
+            pltpu.VMEM((peers, LANE), F32),
+        ],
+        flops=12 * hid * width * half,
+        limit=16 << 20,
+    )
+    step = lax.all_to_all(step, ("yl", "c"), 0, 0, tiled=True)
+    step = call(
+        last_partial_kernel, jax.ShapeDtypeStruct((far, CORES, feats, half), BF), (step,)
+    )
+    step = lax.all_to_all(step, "yh", 0, 0, tiled=True)
     out = call(
         last_kernel, jax.ShapeDtypeStruct((feats, mine), BF), (step, got, middle, other)
     )
@@ -268,11 +350,9 @@
 
 def solution(mesh):
     sizes = mesh.shape
-    wide = Mesh(
-        mesh.devices.reshape(sizes["grp"], sizes["fs"], sizes["tp"] // CORES, CORES),
-        ("grp", "fs", "y", "c"),
-    )
-    tp = ("y", "c")
+    shape = (sizes["grp"], sizes["fs"], sizes["tp"] // CORES // SIDE, SIDE, CORES)
+    wide = Mesh(mesh.devices.reshape(shape), ("grp", "fs", "yh", "yl", "c"))
+    tp = ("yh", "yl", "c")
     block = (P(tp), P("fs", tp), P(tp), P("fs", tp), P(tp), P(tp, "fs"), P(tp))
     rows = P(("grp", "fs"), tp)
     return jax.shard_map(

time: 289 us -> 281 us (0.972)
  waiting for transfers between devices: 46 us -> 34.7 us
  starting transfers between devices: 121 us -> 128 us
  blocking collectives: 108 us -> 102 us
    all_to_all x3 -> x4, waiting for transfers between devices: 41.3 us -> 28.7 us  [the longest x2 18.4 us: body(): step = lax.all_to_all(step, 'yh', 0, 0, tiled=True)]
    all_gather x1, blocking collectives: 62.5 us -> 54.8 us  [body(): own = lax.all_gather(own, 'fs', axis=0)]
    ppermute x2 -> x3, starting transfers between devices: 11.1 us -> 17.9 us  [the longest x1 9.64 us: body(): sib_1 = lax.ppermute(own_1, 'c', SWAP)]
    all_to_all x3 -> x4, starting transfers between devices: 107 us -> 107 us  [the longest x1 87.3 us: body(): got = lax.all_to_all(sent, ('yh', 'yl', 'c'), 0, 0, tiled=True)]
    pallas_call x6 -> x8, Pallas kernels: 9.75 us -> 9.75 us  [call(): pl.pallas_call(kernel, out_shape=out, in_specs=[pl.BlockSpec(memory_space...]
  transfers between devices with their start and end apart: 6 -> 8, of which waited for: 4 -> 6; matrix products, arithmetic and copies ran while one was open for 0% -> 0% of each run, Pallas kernels for 0% -> 1%
where the time goes in v4:
time: 281 us; the launch traced here: 278 us
  starting transfers between devices  128 us (46%)
  blocking collectives  102 us (36%)
  waiting for transfers between devices  34.7 us (12%)
  Pallas kernels  9.75 us (3%)
    all_to_all x1, starting transfers between devices, body(): got = lax.all_to_all(sent, ('yh', 'yl', 'c'), 0, 0, tiled=True)  87.3 us
    all_gather x1, blocking collectives, body(): own = lax.all_gather(own, 'fs', axis=0)  54.8 us
    all_to_all x1, blocking collectives, body(): step = lax.all_to_all(step, ('yl', 'c'), 0, 0, tiled=True)  24.7 us
    all_gather x1, blocking collectives, body(): whole = lax.all_gather(middle, ('yh', 'yl'), axis=0, tiled=True)  22.4 us
    all_to_all x2, waiting for transfers between devices, body(): step = lax.all_to_all(step, 'yh', 0, 0, tiled=True)  18.4 us
    all_to_all x2, starting transfers between devices, body(): step = lax.all_to_all(step, 'yh', 0, 0, tiled=True)  15.8 us
    all_to_all x1, waiting for transfers between devices, body(): step = lax.all_to_all(step, 'yl', 0, 0, tiled=True)  10.2 us
    pallas_call x8, Pallas kernels, call(): pl.pallas_call(kernel, out_shape=out, in_specs=[pl.BlockSpec(memory_space...  9.75 us
  transfers between devices with their start and end apart: 8, of which 6 were waited for; matrix products, arithmetic and copies ran while one was open for 0% of the time, Pallas kernels for 1%

profile of v4, /device:TPU:5, one launch (start us, length us, event | category | flops | bytes accessed | tf_op | source)
XLA Modules:
  0.0 278.1 jit_solution(9342911569138401294)
XLA Ops:
  0.0 0.0 copy-start.3
  0.0 0.0 copy-start.4
  0.0 0.0 copy-start.5
  0.0 0.0 copy-start
  0.0 0.0 copy-start.1
  0.0 0.0 copy-start.2
  0.0 1.9 shard_map.145
  1.9 87.3 %all-to-all-start = ((bf16[32,96,128]{2,1,0:T(8,128)(2,1)}), bf16[32,96,128]{2,1,0:T(8,128)(2,1)S(1)}, u32[]{:S(2)}, u32[]{:S(2)}) async-start(bf16[32,96,128]{2,1,0:T(8,128)(2,1)} %shard_map.145), calls=%async_computation | async-start | bytes 1572864 | tf_op jit(solution)/shard_map/all_to_all | solution.py:271
  89.2 0.0 copy-done.3
  89.2 0.0 copy-done.4
  89.2 0.0 copy-done.5
  89.3 0.2 fusion.6
  89.4 0.0 copy-done
  89.4 0.0 copy-done.1
  89.4 0.0 copy-done.2
  89.5 0.1 multiply_convert_fusion.2
  89.5 54.8 %all-gather.1 = f16[16,800,128]{2,1,0:T(8,128)(2,1)} all-gather(f16[1,800,128]{2,1,0:T(8,128)(2,1)S(1)} %multiply_convert_fusion.2), channel_id=1, replica_groups=mesh['grp'=2,'fs'=16,'yh'=4,'yl'=4,'c'=2] {'fs'}, dimensions={0}, use_global_device_ids=true | all-gather | bytes 3481600 | tf_op jit(solution)/shard_map/all_gather | solution.py:280
  144.4 0.0 all-to-all-done.got
  144.4 2.1 multiply_convert_fusion.own_ref
  146.5 9.6 %collective-permute-start = (bf16[16,528,128]{2,1,0:T(8,128)(2,1)S(1)}, bf16[16,528,128]{2,1,0:T(8,128)(2,1)S(1)}, u32[]{:S(2)}, u32[]{:S(2)}) collective-permute-start(bf16[16,528,128]{2,1,0:T(8,128)(2,1)S(1)} %multiply_convert_fusion.own_ref), channel_id=1, source_target_pairs={{0,1},{1,0},{2,3},{3,2},{4,5},{5,4},{6,7},{7,6},{8,9},{9,8},{10,11... | collective-permute-start | bytes 6488072 | tf_op jit(solution)/shard_map/ppermute | solution.py:287
  156.1 0.9 shard_map.146
  157.1 2.9 %collective-permute-done.sib_ref = bf16[16,528,128]{2,1,0:T(8,128)(2,1)S(1)} collective-permute-done((bf16[16,528,128]{2,1,0:T(8,128)(2,1)S(1)}, bf16[16,528,128]{2,1,0:T(8,128)(2,1)S(1)}, u32[]{:S(2)}, u32[]{:S(2)}) %collective-permute-start) | collective-permute-done | bytes 2162720 | tf_op jit(solution)/shard_map/ppermute | solution.py:287
  160.0 0.0 slice-start
  160.0 2.7 shard_map.147
  162.6 4.2 %all-to-all-start.1 = ((bf16[4,4,128,128]{3,2,1,0:T(8,128)(2,1)}), bf16[4,4,128,128]{3,2,1,0:T(8,128)(2,1)S(1)}, u32[]{:S(2)}, u32[]{:S(2)}) async-start(bf16[4,4,128,128]{3,2,1,0:T(8,128)(2,1)} %shard_map.147), calls=%async_computation.1 | async-start | bytes 1048576 | tf_op jit(solution)/shard_map/all_to_all | solution.py:312
  166.8 0.0 slice-done
  166.8 0.3 multiply_convert_fusion.1
  167.1 3.6 %collective-permute-start.1 = (bf16[16,272,128]{2,1,0:T(8,128)(2,1)S(1)}, bf16[16,272,128]{2,1,0:T(8,128)(2,1)S(1)}, u32[]{:S(2)}, u32[]{:S(2)}) collective-permute-start(bf16[16,272,128]{2,1,0:T(8,128)(2,1)S(1)} %multiply_convert_fusion.1), channel_id=1, source_target_pairs={{0,512},{512,0},{1,513},{513,1},{2,514},{514,2},{3,515},{515,3},{4... | collective-permute-start | bytes 3342344 | tf_op jit(solution)/shard_map/ppermute | solution.py:309
  170.7 10.2 %all-to-all-done.1.got = bf16[4,4,128,128]{3,2,1,0:T(8,128)(2,1)S(1)} async-done(((bf16[4,4,128,128]{3,2,1,0:T(8,128)(2,1)}), bf16[4,4,128,128]{3,2,1,0:T(8,128)(2,1)S(1)}, u32[]{:S(2)}, u32[]{:S(2)}) %all-to-all-start.1) | async-done | bytes 524320 | tf_op jit(solution)/shard_map/all_to_all | solution.py:312
  180.9 0.7 shard_map.148
  181.6 11.0 %all-to-all-start.2 = ((bf16[4,128,128]{2,1,0:T(8,128)(2,1)}), bf16[4,128,128]{2,1,0:T(8,128)(2,1)S(1)}, u32[]{:S(2)}, u32[]{:S(2)}) async-start(bf16[4,128,128]{2,1,0:T(8,128)(2,1)} %shard_map.148), calls=%async_computation.2 | async-start | bytes 262144 | tf_op jit(solution)/shard_map/all_to_all | solution.py:314
  192.6 2.3 collective-permute-done.1
  194.8 10.3 %all-to-all-done.2.sums = bf16[4,128,128]{2,1,0:T(8,128)(2,1)S(1)} async-done(((bf16[4,128,128]{2,1,0:T(8,128)(2,1)}), bf16[4,128,128]{2,1,0:T(8,128)(2,1)S(1)}, u32[]{:S(2)}, u32[]{:S(2)}) %all-to-all-start.2) | async-done | bytes 131104 | tf_op jit(solution)/shard_map/all_to_all | solution.py:314
  205.2 0.3 broadcast_in_dim.35
  205.5 0.2 constant_dynamic-update-slice_fusion.1
  205.6 0.2 constant_dynamic-update-slice_fusion.own_ref
  205.8 4.7 %collective-permute-start.2 = (bf16[16,544,128]{2,1,0:T(8,128)(2,1)S(1)}, bf16[16,544,128]{2,1,0:T(8,128)(2,1)S(1)}, u32[]{:S(2)}, u32[]{:S(2)}) collective-permute-start(bf16[16,544,128]{2,1,0:T(8,128)(2,1)S(1)} %constant_dynamic-update-slice_fusion.own_ref), channel_id=1, source_target_pairs={{0,1},{1,0},{2,3},{3,2},{4,5},{5,4},{6,7},{7,6},{8,9},{9,8},{10,11... | collective-permute-start | bytes 6684680 | tf_op jit(solution)/shard_map/ppermute | solution.py:320
  210.5 0.2 shard_map.149
  210.6 22.4 %all_gather.8.s_ref = bf16[2048,128]{1,0:T(8,128)(2,1)S(1)} all-gather(bf16[128,128]{1,0:T(8,128)(2,1)S(1)} %get-tuple-element.29.mid_ref), channel_id=1, replica_groups=mesh['grp'=2,'fs'=16,'yh'=4,'yl'=4,'c'=2] {'yh','yl'}, dimensions={0}, use_global_device_ids=true | all-gather | bytes 557056 | tf_op jit(solution)/shard_map/all_gather | solution.py:327
  233.0 0.0 collective-permute-done.2.sib_ref
  233.0 1.9 shard_map.150
  234.9 24.7 %all_to_all.25.got = bf16[8,4,64,128]{3,2,1,0:T(8,128)(2,1)S(1)} all-to-all(bf16[8,4,64,128]{3,2,1,0:T(8,128)(2,1)S(1)} %shard_map.150), channel_id=1, replica_groups=mesh['grp'=2,'fs'=16,'yh'=4,'yl'=4,'c'=2] {'yl','c'}, dimensions={0} | all-to-all | bytes 1048576 | tf_op jit(solution)/shard_map/all_to_all | solution.py:340
  259.6 0.7 shard_map.151
  260.3 4.8 %all-to-all-start.4 = ((bf16[4,2,64,128]{3,2,1,0:T(8,128)(2,1)}), bf16[4,2,64,128]{3,2,1,0:T(8,128)(2,1)S(1)}, u32[]{:S(2)}, u32[]{:S(2)}) async-start(bf16[4,2,64,128]{3,2,1,0:T(8,128)(2,1)} %shard_map.151), calls=%async_computation.4 | async-start | bytes 262144 | tf_op jit(solution)/shard_map/all_to_all | solution.py:344
  265.1 3.2 %collective-permute-start.3 = (bf16[64,128]{1,0:T(8,128)(2,1)S(1)}, bf16[64,128]{1,0:T(8,128)(2,1)S(1)}, u32[]{:S(2)}, u32[]{:S(2)}) collective-permute-start(bf16[64,128]{1,0:T(8,128)(2,1)S(1)} %get-tuple-element.32), channel_id=1, source_target_pairs={{0,1},{1,0},{2,3},{3,2},{4,5},{5,4},{6,7},{7,6},{8,9},{9,8},{10,11... | collective-permute-start | bytes 49160 | tf_op jit(solution)/shard_map/ppermute | solution.py:326
  268.4 0.8 collective-permute-done.3.other_ref
  269.2 8.1 %all-to-all-done.4.sums = bf16[4,2,64,128]{3,2,1,0:T(8,128)(2,1)S(1)} async-done(((bf16[4,2,64,128]{3,2,1,0:T(8,128)(2,1)}), bf16[4,2,64,128]{3,2,1,0:T(8,128)(2,1)S(1)}, u32[]{:S(2)}, u32[]{:S(2)}) %all-to-all-start.4) | async-done | bytes 131104 | tf_op jit(solution)/shard_map/all_to_all | solution.py:344
  277.3 0.8 shard_map.152
  (2 shorter events, 0.0 us)
Async XLA Ops:
  0.0 89.2 %copy-start.3 = (f32[176,128]{1,0:T(8,128)S(1)}, f32[176,128]{1,0:T(8,128)}, u32[]{:S(2)}) copy-start(f32[176,128]{1,0:T(8,128)} %param.28) | copy-start | bytes 270340
  0.0 89.2 %copy-start.4 = (f32[128,176]{0,1:T(8,128)S(1)}, f32[128,176]{0,1:T(8,128)}, u32[]{:S(2)}) copy-start(f32[128,176]{0,1:T(8,128)} %param.26) | copy-start | bytes 270340
  0.0 89.2 %copy-start.5 = (f32[128,176]{0,1:T(8,128)S(1)}, f32[128,176]{0,1:T(8,128)}, u32[]{:S(2)}) copy-start(f32[128,176]{0,1:T(8,128)} %param.24) | copy-start | bytes 270340
  0.0 89.4 %copy-start = (f32[176,128]{1,0:T(8,128)S(1)}, f32[176,128]{1,0:T(8,128)}, u32[]{:S(2)}) copy-start(f32[176,128]{1,0:T(8,128)} %param.21) | copy-start | bytes 270340
  0.0 89.4 %copy-start.1 = (f32[128,176]{0,1:T(8,128)S(1)}, f32[128,176]{0,1:T(8,128)}, u32[]{:S(2)}) copy-start(f32[128,176]{0,1:T(8,128)} %param.19) | copy-start | bytes 270340
  0.0 89.4 %copy-start.2 = (f32[128,176]{0,1:T(8,128)S(1)}, f32[128,176]{0,1:T(8,128)}, u32[]{:S(2)}) copy-start(f32[128,176]{0,1:T(8,128)} %param.17) | copy-start | bytes 270340
  1.9 142.4 %all-to-all-start = ((bf16[32,96,128]{2,1,0:T(8,128)(2,1)}), bf16[32,96,128]{2,1,0:T(8,128)(2,1)S(1)}, u32[]{:S(2)}, u32[]{:S(2)}) async-start(bf16[32,96,128]{2,1,0:T(8,128)(2,1)} %shard_map.145), calls=%async_computation | async-start | bytes 1572864 | tf_op jit(solution)/shard_map/all_to_all | solution.py:271
  146.5 13.5 %collective-permute-start = (bf16[16,528,128]{2,1,0:T(8,128)(2,1)S(1)}, bf16[16,528,128]{2,1,0:T(8,128)(2,1)S(1)}, u32[]{:S(2)}, u32[]{:S(2)}) collective-permute-start(bf16[16,528,128]{2,1,0:T(8,128)(2,1)S(1)} %multiply_convert_fusion.own_ref), channel_id=1, source_target_pairs={{0,1},{1,0},{2,3},{3,2},{4,5},{5,4},{6,7},{7,6},{8,9},{9,8},{10,11... | collective-permute-start | bytes 6488072 | tf_op jit(solution)/shard_map/ppermute | solution.py:287
  160.0 6.8 %slice-start = ((f16[16,800,128]{2,1,0:T(8,128)(2,1)}), f16[16,272,128]{2,1,0:T(8,128)(2,1)S(1)}, s32[]{:S(2)}) async-start(f16[16,800,128]{2,1,0:T(8,128)(2,1)} %all-gather.1), calls=%async_computation.5 | async-start | bytes 2228224 | tf_op jit(solution)/shard_map/slice | solution.py:306
  162.6 18.2 %all-to-all-start.1 = ((bf16[4,4,128,128]{3,2,1,0:T(8,128)(2,1)}), bf16[4,4,128,128]{3,2,1,0:T(8,128)(2,1)S(1)}, u32[]{:S(2)}, u32[]{:S(2)}) async-start(bf16[4,4,128,128]{3,2,1,0:T(8,128)(2,1)} %shard_map.147), calls=%async_computation.1 | async-start | bytes 1048576 | tf_op jit(solution)/shard_map/all_to_all | solution.py:312
  167.1 27.8 %collective-permute-start.1 = (bf16[16,272,128]{2,1,0:T(8,128)(2,1)S(1)}, bf16[16,272,128]{2,1,0:T(8,128)(2,1)S(1)}, u32[]{:S(2)}, u32[]{:S(2)}) collective-permute-start(bf16[16,272,128]{2,1,0:T(8,128)(2,1)S(1)} %multiply_convert_fusion.1), channel_id=1, source_target_pairs={{0,512},{512,0},{1,513},{513,1},{2,514},{514,2},{3,515},{515,3},{4... | collective-permute-start | bytes 3342344 | tf_op jit(solution)/shard_map/ppermute | solution.py:309
  181.6 23.6 %all-to-all-start.2 = ((bf16[4,128,128]{2,1,0:T(8,128)(2,1)}), bf16[4,128,128]{2,1,0:T(8,128)(2,1)S(1)}, u32[]{:S(2)}, u32[]{:S(2)}) async-start(bf16[4,128,128]{2,1,0:T(8,128)(2,1)} %shard_map.148), calls=%async_computation.2 | async-start | bytes 262144 | tf_op jit(solution)/shard_map/all_to_all | solution.py:314
  205.8 27.2 %collective-permute-start.2 = (bf16[16,544,128]{2,1,0:T(8,128)(2,1)S(1)}, bf16[16,544,128]{2,1,0:T(8,128)(2,1)S(1)}, u32[]{:S(2)}, u32[]{:S(2)}) collective-permute-start(bf16[16,544,128]{2,1,0:T(8,128)(2,1)S(1)} %constant_dynamic-update-slice_fusion.own_ref), channel_id=1, source_target_pairs={{0,1},{1,0},{2,3},{3,2},{4,5},{5,4},{6,7},{7,6},{8,9},{9,8},{10,11... | collective-permute-start | bytes 6684680 | tf_op jit(solution)/shard_map/ppermute | solution.py:320
  260.3 17.0 %all-to-all-start.4 = ((bf16[4,2,64,128]{3,2,1,0:T(8,128)(2,1)}), bf16[4,2,64,128]{3,2,1,0:T(8,128)(2,1)S(1)}, u32[]{:S(2)}, u32[]{:S(2)}) async-start(bf16[4,2,64,128]{3,2,1,0:T(8,128)(2,1)} %shard_map.151), calls=%async_computation.4 | async-start | bytes 262144 | tf_op jit(solution)/shard_map/all_to_all | solution.py:344
  265.1 4.1 %collective-permute-start.3 = (bf16[64,128]{1,0:T(8,128)(2,1)S(1)}, bf16[64,128]{1,0:T(8,128)(2,1)S(1)}, u32[]{:S(2)}, u32[]{:S(2)}) collective-permute-start(bf16[64,128]{1,0:T(8,128)(2,1)S(1)} %get-tuple-element.32), channel_id=1, source_target_pairs={{0,1},{1,0},{2,3},{3,2},{4,5},{5,4},{6,7},{7,6},{8,9},{9,8},{10,11... | collective-permute-start | bytes 49160 | tf_op jit(solution)/shard_map/ppermute | solution.py:326

commit v5 on v4

--- a/solution.py
+++ b/solution.py
@@ -6,6 +6,7 @@
 from jax.experimental import pallas as pl
 from jax.experimental.pallas import tpu as pltpu
 from jax.sharding import Mesh, PartitionSpec as P
+
 
 epsilon = 1e-06
 BF = jnp.bfloat16
@@ -45,7 +46,7 @@
     count = 8
     sources, out_ref = refs[:count], refs[count]
     t_ref, held, ext, sems = refs[count + 1], refs[count + 2 : 2 * count + 2], *refs[-2:]
-    peers, rows, half = out_ref.shape
+    peers, _, half = out_ref.shape
     feats = t_hbm.shape[0]
     copies = [pltpu.make_async_copy(t_hbm, t_ref, sems.at[count])]
     for k in range(count):
@@ -71,7 +72,7 @@
         out_ref[k, feats:, :] = tail
 
 
-def vec_column(got, peer, which, feats, col, size):
+def vec_column(got, peer, which, feats, size):
     rows = got[peer, feats + 8 : feats + EXTRA, :].astype(F32)
     rows = rows[0:8] + rows[8:16] + rows[16:24]
     turned = jnp.transpose(rows)
@@ -111,7 +112,7 @@
 def hidden_of(hid, block, w, peer, got, h_ref):
     feats = got.shape[1] - EXTRA
     chunks, _, lane = w.shape
-    sg, su = vec_column(got, peer, (2 * block, 2 * block + 1), feats, block, hid)
+    sg, su = vec_column(got, peer, (2 * block, 2 * block + 1), feats, hid)
     acc = jnp.zeros((2 * hid, got.shape[2]), F32)
     for z in range(0, chunks, 2):
         lhs = jnp.concatenate([w[z, : 2 * hid, :], w[z + 1, : 2 * hid, :]], axis=1)
@@ -149,14 +150,12 @@
 
 
 def second_block_kernel(hid, s_ref, got, own_ref, sib_ref, out_ref, h_ref, hd_ref, g_ref):
-    feats = got.shape[1] - EXTRA
     normalize(1, s_ref, got, h_ref, g_ref)
     hd_ref[:hid, :] = hidden_of(hid, 1, own_ref, seat(0), got, h_ref)
     hd_ref[hid:, :] = hidden_of(hid, 1, sib_ref, seat(1), got, h_ref)
 
     def store(z, part):
-        for c in range(CORES):
-            out_ref[z % SIDE * CORES + c, z // SIDE] = part[c * feats : (c + 1) * feats]
+        out_ref[z % SIDE, z // SIDE] = part
 
     down_blocks(hid, own_ref, sib_ref, hd_ref[...], store)
 
@@ -192,9 +191,9 @@
     here = mid_ref[pl.ds(core * feats, feats), :].astype(F32)
     other = other_ref[...].astype(F32)
     for c in range(CORES):
-        total = sums[0, c].astype(F32)
-        for k in range(1, sums.shape[0]):
-            total = total + sums[k, c].astype(F32)
+        total = sums[c].astype(F32)
+        for k in range(CORES + c, sums.shape[0], CORES):
+            total = total + sums[k].astype(F32)
         resid = jnp.where(core == c, here, other)
         out_ref[:, c * half : (c + 1) * half] = (resid + 0.5 * total * scale).astype(BF)
 
@@ -204,15 +203,6 @@
     for k in range(1, got.shape[0]):
         total = total + got[k].astype(F32)
     out_ref[...] = total.astype(BF)
-
-
-def last_partial_kernel(got, out_ref):
-    for c in range(CORES):
-        for i in range(out_ref.shape[0]):
-            total = got[c, i].astype(F32)
-            for k in range(CORES + c, got.shape[0], CORES):
-                total = total + got[k, i].astype(F32)
-            out_ref[i, c] = total.astype(BF)
 
 
 def call(kernel, out, args, scratch=(), flops=1000, limit=4 << 20, space=pltpu.VMEM):
@@ -228,7 +218,7 @@
     )(*args)
 
 
-def body(
+def blocks(
     tokens,
     gain_1,
     gate_1,
@@ -294,7 +284,13 @@
         flops=4 * hid * width * half,
         limit=16 << 20,
     )
-    sib_1, h, hd = lax.optimization_barrier((sib_1, h, hd))
+    later, h, hd = lax.optimization_barrier((own[:, rows:], h, hd))
+    later = restored(later)
+    slices = [later] + [
+        lax.ppermute(later, "grp", [(i, (i + r) % groups) for i in range(groups)])
+        for r in range(1, groups)
+    ]
+    later, sib_1, h, hd = lax.optimization_barrier((later, sib_1, h, hd))
     step = call(
         functools.partial(second_half_kernel, hid),
         jax.ShapeDtypeStruct((SIDE, far, chip, half), BF),
@@ -303,12 +299,6 @@
         flops=8 * hid * width * half,
         limit=16 << 20,
     )
-    later, step = lax.optimization_barrier((own[:, rows:], step))
-    later = restored(later)
-    slices = [later] + [
-        lax.ppermute(later, "grp", [(i, (i + r) % groups) for i in range(groups)])
-        for r in range(1, groups)
-    ]
     step = lax.all_to_all(step, "yl", 0, 0, tiled=True)
     step = call(partial_kernel, jax.ShapeDtypeStruct(step.shape[1:], BF), (step,))
     step = lax.all_to_all(step, "yh", 0, 0, tiled=True)
@@ -327,7 +317,7 @@
     whole = lax.all_gather(middle, ("yh", "yl"), axis=0, tiled=True)
     step = call(
         functools.partial(second_block_kernel, hid),
-        jax.ShapeDtypeStruct((SIDE * CORES, far, feats, half), BF),
+        jax.ShapeDtypeStruct((SIDE, far, chip, half), BF),
         (whole, got, own_2, sib_2),
         [
             pltpu.VMEM((width, half), BF),
@@ -337,11 +327,10 @@
         flops=12 * hid * width * half,
         limit=16 << 20,
     )
-    step = lax.all_to_all(step, ("yl", "c"), 0, 0, tiled=True)
-    step = call(
-        last_partial_kernel, jax.ShapeDtypeStruct((far, CORES, feats, half), BF), (step,)
-    )
-    step = lax.all_to_all(step, "yh", 0, 0, tiled=True)
+    step = lax.all_to_all(step, "yl", 0, 0, tiled=True)
+    step = call(partial_kernel, jax.ShapeDtypeStruct(step.shape[1:], BF), (step,))
+    step = step.reshape(far * CORES, feats, half)
+    step = lax.all_to_all(step, ("yh", "c"), 0, 0, tiled=True)
     out = call(
         last_kernel, jax.ShapeDtypeStruct((feats, mine), BF), (step, got, middle, other)
     )
@@ -356,5 +345,5 @@
     block = (P(tp), P("fs", tp), P(tp), P("fs", tp), P(tp), P(tp, "fs"), P(tp))
     rows = P(("grp", "fs"), tp)
     return jax.shard_map(
-        body, mesh=wide, in_specs=(rows, *block, *block), out_specs=rows, check_vma=False
-    )
+        blocks, mesh=wide, in_specs=(rows, *block, *block), out_specs=rows, check_vma=False
+    )

time: 281 us -> 277 us (0.986)
  blocking collectives: 102 us -> 90.1 us
  starting transfers between devices: 128 us -> 135 us
    all_to_all x1, blocking collectives: 24.7 us -> 12.9 us  [blocks(): step = lax.all_to_all(step, 'yl', 0, 0, tiled=True)]
    all_to_all x4, starting transfers between devices: 107 us -> 115 us  [the longest x1 87.3 us: blocks(): got = lax.all_to_all(sent, ('yh', 'yl', 'c'), 0, 0, tiled=True)]
where the time goes in v5:
time: 277 us; the launch traced here: 276 us
  starting transfers between devices  135 us (49%)
  blocking collectives  90.1 us (33%)
  waiting for transfers between devices  37.1 us (13%)
  Pallas kernels  9.74 us (4%)
    all_to_all x1, starting transfers between devices, blocks(): got = lax.all_to_all(sent, ('yh', 'yl', 'c'), 0, 0, tiled=True)  87.3 us
    all_gather x1, blocking collectives, blocks(): own = lax.all_gather(own, 'fs', axis=0)  54.8 us
    all_gather x1, blocking collectives, blocks(): whole = lax.all_gather(middle, ('yh', 'yl'), axis=0, tiled=True)  22.4 us
    all_to_all x1, blocking collectives, blocks(): step = lax.all_to_all(step, 'yl', 0, 0, tiled=True)  12.9 us
    all_to_all x1, starting transfers between devices, blocks(): step = lax.all_to_all(step, ('yh', 'c'), 0, 0, tiled=True)  12.8 us
    all_to_all x1, starting transfers between devices, blocks(): step = lax.all_to_all(step, 'yh', 0, 0, tiled=True)  11 us
    all_to_all x1, waiting for transfers between devices, blocks(): step = lax.all_to_all(step, 'yh', 0, 0, tiled=True)  10.6 us
    all_to_all x1, waiting for transfers between devices, blocks(): step = lax.all_to_all(step, 'yl', 0, 0, tiled=True)  10.5 us
  transfers between devices with their start and end apart: 8, of which 6 were waited for; matrix products, arithmetic and copies ran while one was open for 0% of the time, Pallas kernels for 1%

profile of v5, /device:TPU:5, one launch (start us, length us, event | category | flops | bytes accessed | tf_op | source)
XLA Modules:
  0.0 275.6 jit_solution(13305188508698498489)
XLA Ops:
  0.0 0.0 copy-start.5
  0.0 0.0 copy-start.4
  0.0 0.0 copy-start.3
  0.0 0.0 copy-start
  0.0 0.0 copy-start.2
  0.0 0.0 copy-start.1
  0.0 1.9 shard_map.145
  1.9 87.3 %all-to-all-start = ((bf16[32,96,128]{2,1,0:T(8,128)(2,1)}), bf16[32,96,128]{2,1,0:T(8,128)(2,1)S(1)}, u32[]{:S(2)}, u32[]{:S(2)}) async-start(bf16[32,96,128]{2,1,0:T(8,128)(2,1)} %shard_map.145), calls=%async_computation | async-start | bytes 1572864 | tf_op jit(solution)/shard_map/all_to_all | solution.py:261
  89.2 0.0 copy-done.5
  89.2 0.0 copy-done.4
  89.2 0.0 copy-done.3
  89.3 0.2 fusion.6
  89.4 0.0 copy-done
  89.4 0.0 copy-done.2
  89.4 0.0 copy-done.1
  89.5 0.1 multiply_convert_fusion.2
  89.5 54.8 %all-gather.1 = f16[16,800,128]{2,1,0:T(8,128)(2,1)} all-gather(f16[1,800,128]{2,1,0:T(8,128)(2,1)S(1)} %multiply_convert_fusion.2), channel_id=1, replica_groups=mesh['grp'=2,'fs'=16,'yh'=4,'yl'=4,'c'=2] {'fs'}, dimensions={0}, use_global_device_ids=true | all-gather | bytes 3481600 | tf_op jit(solution)/shard_map/all_gather | solution.py:270
  144.4 0.0 all-to-all-done.got
  144.4 2.1 multiply_convert_fusion.own_ref
  146.5 0.0 slice-start
  146.5 9.8 %collective-permute-start.1 = (bf16[16,528,128]{2,1,0:T(8,128)(2,1)S(1)}, bf16[16,528,128]{2,1,0:T(8,128)(2,1)S(1)}, u32[]{:S(2)}, u32[]{:S(2)}) collective-permute-start(bf16[16,528,128]{2,1,0:T(8,128)(2,1)S(1)} %multiply_convert_fusion.own_ref), channel_id=1, source_target_pairs={{0,1},{1,0},{2,3},{3,2},{4,5},{5,4},{6,7},{7,6},{8,9},{9,8},{10,11... | collective-permute-start | bytes 6488072 | tf_op jit(solution)/shard_map/ppermute | solution.py:277
  156.3 0.9 shard_map.146
  157.2 0.0 slice-done
  157.2 0.3 multiply_convert_fusion.1
  157.5 2.6 collective-permute-done.1.sib_ref
  160.1 2.6 shard_map.147
  162.8 4.2 %all-to-all-start.1 = ((bf16[4,4,128,128]{3,2,1,0:T(8,128)(2,1)}), bf16[4,4,128,128]{3,2,1,0:T(8,128)(2,1)S(1)}, u32[]{:S(2)}, u32[]{:S(2)}) async-start(bf16[4,4,128,128]{3,2,1,0:T(8,128)(2,1)} %shard_map.147), calls=%async_computation.1 | async-start | bytes 1048576 | tf_op jit(solution)/shard_map/all_to_all | solution.py:302
  166.9 3.6 %collective-permute-start = (bf16[16,272,128]{2,1,0:T(8,128)(2,1)S(1)}, bf16[16,272,128]{2,1,0:T(8,128)(2,1)S(1)}, u32[]{:S(2)}, u32[]{:S(2)}) collective-permute-start(bf16[16,272,128]{2,1,0:T(8,128)(2,1)S(1)} %multiply_convert_fusion.1), channel_id=1, source_target_pairs={{0,512},{512,0},{1,513},{513,1},{2,514},{514,2},{3,515},{515,3},{4... | collective-permute-start | bytes 3342344 | tf_op jit(solution)/shard_map/ppermute | solution.py:290
  170.5 10.5 %all-to-all-done.1.got = bf16[4,4,128,128]{3,2,1,0:T(8,128)(2,1)S(1)} async-done(((bf16[4,4,128,128]{3,2,1,0:T(8,128)(2,1)}), bf16[4,4,128,128]{3,2,1,0:T(8,128)(2,1)S(1)}, u32[]{:S(2)}, u32[]{:S(2)}) %all-to-all-start.1) | async-done | bytes 524320 | tf_op jit(solution)/shard_map/all_to_all | solution.py:302
  181.0 0.7 shard_map.148
  181.7 11.0 %all-to-all-start.2 = ((bf16[4,128,128]{2,1,0:T(8,128)(2,1)}), bf16[4,128,128]{2,1,0:T(8,128)(2,1)S(1)}, u32[]{:S(2)}, u32[]{:S(2)}) async-start(bf16[4,128,128]{2,1,0:T(8,128)(2,1)} %shard_map.148), calls=%async_computation.2 | async-start | bytes 262144 | tf_op jit(solution)/shard_map/all_to_all | solution.py:304
  192.7 2.0 collective-permute-done
  194.7 10.6 %all-to-all-done.2.sums = bf16[4,128,128]{2,1,0:T(8,128)(2,1)S(1)} async-done(((bf16[4,128,128]{2,1,0:T(8,128)(2,1)}), bf16[4,128,128]{2,1,0:T(8,128)(2,1)S(1)}, u32[]{:S(2)}, u32[]{:S(2)}) %all-to-all-start.2) | async-done | bytes 131104 | tf_op jit(solution)/shard_map/all_to_all | solution.py:304
  205.3 0.3 broadcast_in_dim.35
  205.6 0.2 constant_dynamic-update-slice_fusion.1
  205.7 0.2 constant_dynamic-update-slice_fusion.own_ref
  205.9 4.7 %collective-permute-start.2 = (bf16[16,544,128]{2,1,0:T(8,128)(2,1)S(1)}, bf16[16,544,128]{2,1,0:T(8,128)(2,1)S(1)}, u32[]{:S(2)}, u32[]{:S(2)}) collective-permute-start(bf16[16,544,128]{2,1,0:T(8,128)(2,1)S(1)} %constant_dynamic-update-slice_fusion.own_ref), channel_id=1, source_target_pairs={{0,1},{1,0},{2,3},{3,2},{4,5},{5,4},{6,7},{7,6},{8,9},{9,8},{10,11... | collective-permute-start | bytes 6684680 | tf_op jit(solution)/shard_map/ppermute | solution.py:310
  210.6 0.2 shard_map.149
  210.8 22.4 %all_gather.8.s_ref = bf16[2048,128]{1,0:T(8,128)(2,1)S(1)} all-gather(bf16[128,128]{1,0:T(8,128)(2,1)S(1)} %get-tuple-element.31.mid_ref), channel_id=1, replica_groups=mesh['grp'=2,'fs'=16,'yh'=4,'yl'=4,'c'=2] {'yh','yl'}, dimensions={0}, use_global_device_ids=true | all-gather | bytes 557056 | tf_op jit(solution)/shard_map/all_gather | solution.py:317
  233.1 0.0 collective-permute-done.2.sib_ref
  233.1 1.9 shard_map.150
  235.0 12.9 %all_to_all.25.got = bf16[4,4,128,128]{3,2,1,0:T(8,128)(2,1)S(1)} all-to-all(bf16[4,4,128,128]{3,2,1,0:T(8,128)(2,1)S(1)} %shard_map.150), channel_id=1, replica_groups=mesh['grp'=2,'fs'=16,'yh'=4,'yl'=4,'c'=2] {'yl'}, dimensions={0} | all-to-all | bytes 1048576 | tf_op jit(solution)/shard_map/all_to_all | solution.py:330
  247.9 0.7 shard_map.151
  248.6 12.8 %all-to-all-start.4 = ((bf16[8,64,128]{2,1,0:T(8,128)(2,1)}), bf16[8,64,128]{2,1,0:T(8,128)(2,1)S(1)}, u32[]{:S(2)}, u32[]{:S(2)}) async-start(bf16[8,64,128]{2,1,0:T(8,128)(2,1)} %bitcast.17), calls=%async_computation.4 | async-start | bytes 262144 | tf_op jit(solution)/shard_map/all_to_all | solution.py:333
  261.5 1.9 collective-permute-start.3
  263.4 1.1 collective-permute-done.3.other_ref
  264.6 10.2 %all-to-all-done.4.sums = bf16[8,64,128]{2,1,0:T(8,128)(2,1)S(1)} async-done(((bf16[8,64,128]{2,1,0:T(8,128)(2,1)}), bf16[8,64,128]{2,1,0:T(8,128)(2,1)S(1)}, u32[]{:S(2)}, u32[]{:S(2)}) %all-to-all-start.4) | async-done | bytes 131104 | tf_op jit(solution)/shard_map/all_to_all | solution.py:333
  274.8 0.8 shard_map.152
  (2 shorter events, 0.0 us)
Async XLA Ops:
  0.0 89.2 %copy-start.5 = (f32[128,176]{0,1:T(8,128)S(1)}, f32[128,176]{0,1:T(8,128)}, u32[]{:S(2)}) copy-start(f32[128,176]{0,1:T(8,128)} %param.24) | copy-start | bytes 270340
  0.0 89.2 %copy-start.4 = (f32[128,176]{0,1:T(8,128)S(1)}, f32[128,176]{0,1:T(8,128)}, u32[]{:S(2)}) copy-start(f32[128,176]{0,1:T(8,128)} %param.26) | copy-start | bytes 270340
  0.0 89.2 %copy-start.3 = (f32[176,128]{1,0:T(8,128)S(1)}, f32[176,128]{1,0:T(8,128)}, u32[]{:S(2)}) copy-start(f32[176,128]{1,0:T(8,128)} %param.28) | copy-start | bytes 270340
  0.0 89.4 %copy-start = (f32[176,128]{1,0:T(8,128)S(1)}, f32[176,128]{1,0:T(8,128)}, u32[]{:S(2)}) copy-start(f32[176,128]{1,0:T(8,128)} %param.21) | copy-start | bytes 270340
  0.0 89.4 %copy-start.2 = (f32[128,176]{0,1:T(8,128)S(1)}, f32[128,176]{0,1:T(8,128)}, u32[]{:S(2)}) copy-start(f32[128,176]{0,1:T(8,128)} %param.17) | copy-start | bytes 270340
  0.0 89.4 %copy-start.1 = (f32[128,176]{0,1:T(8,128)S(1)}, f32[128,176]{0,1:T(8,128)}, u32[]{:S(2)}) copy-start(f32[128,176]{0,1:T(8,128)} %param.19) | copy-start | bytes 270340
  1.9 142.4 %all-to-all-start = ((bf16[32,96,128]{2,1,0:T(8,128)(2,1)}), bf16[32,96,128]{2,1,0:T(8,128)(2,1)S(1)}, u32[]{:S(2)}, u32[]{:S(2)}) async-start(bf16[32,96,128]{2,1,0:T(8,128)(2,1)} %shard_map.145), calls=%async_computation | async-start | bytes 1572864 | tf_op jit(solution)/shard_map/all_to_all | solution.py:261
  146.5 10.7 %slice-start = ((f16[16,800,128]{2,1,0:T(8,128)(2,1)}), f16[16,272,128]{2,1,0:T(8,128)(2,1)S(1)}, s32[]{:S(2)}) async-start(f16[16,800,128]{2,1,0:T(8,128)(2,1)} %all-gather.1), calls=%async_computation.5 | async-start | bytes 2228224 | tf_op jit(solution)/shard_map/slice | solution.py:287
  146.5 13.6 %collective-permute-start.1 = (bf16[16,528,128]{2,1,0:T(8,128)(2,1)S(1)}, bf16[16,528,128]{2,1,0:T(8,128)(2,1)S(1)}, u32[]{:S(2)}, u32[]{:S(2)}) collective-permute-start(bf16[16,528,128]{2,1,0:T(8,128)(2,1)S(1)} %multiply_convert_fusion.own_ref), channel_id=1, source_target_pairs={{0,1},{1,0},{2,3},{3,2},{4,5},{5,4},{6,7},{7,6},{8,9},{9,8},{10,11... | collective-permute-start | bytes 6488072 | tf_op jit(solution)/shard_map/ppermute | solution.py:277
  162.8 18.2 %all-to-all-start.1 = ((bf16[4,4,128,128]{3,2,1,0:T(8,128)(2,1)}), bf16[4,4,128,128]{3,2,1,0:T(8,128)(2,1)S(1)}, u32[]{:S(2)}, u32[]{:S(2)}) async-start(bf16[4,4,128,128]{3,2,1,0:T(8,128)(2,1)} %shard_map.147), calls=%async_computation.1 | async-start | bytes 1048576 | tf_op jit(solution)/shard_map/all_to_all | solution.py:302
  166.9 27.7 %collective-permute-start = (bf16[16,272,128]{2,1,0:T(8,128)(2,1)S(1)}, bf16[16,272,128]{2,1,0:T(8,128)(2,1)S(1)}, u32[]{:S(2)}, u32[]{:S(2)}) collective-permute-start(bf16[16,272,128]{2,1,0:T(8,128)(2,1)S(1)} %multiply_convert_fusion.1), channel_id=1, source_target_pairs={{0,512},{512,0},{1,513},{513,1},{2,514},{514,2},{3,515},{515,3},{4... | collective-permute-start | bytes 3342344 | tf_op jit(solution)/shard_map/ppermute | solution.py:290
  181.7 23.6 %all-to-all-start.2 = ((bf16[4,128,128]{2,1,0:T(8,128)(2,1)}), bf16[4,128,128]{2,1,0:T(8,128)(2,1)S(1)}, u32[]{:S(2)}, u32[]{:S(2)}) async-start(bf16[4,128,128]{2,1,0:T(8,128)(2,1)} %shard_map.148), calls=%async_computation.2 | async-start | bytes 262144 | tf_op jit(solution)/shard_map/all_to_all | solution.py:304
  205.9 27.2 %collective-permute-start.2 = (bf16[16,544,128]{2,1,0:T(8,128)(2,1)S(1)}, bf16[16,544,128]{2,1,0:T(8,128)(2,1)S(1)}, u32[]{:S(2)}, u32[]{:S(2)}) collective-permute-start(bf16[16,544,128]{2,1,0:T(8,128)(2,1)S(1)} %constant_dynamic-update-slice_fusion.own_ref), channel_id=1, source_target_pairs={{0,1},{1,0},{2,3},{3,2},{4,5},{5,4},{6,7},{7,6},{8,9},{9,8},{10,11... | collective-permute-start | bytes 6684680 | tf_op jit(solution)/shard_map/ppermute | solution.py:310
  248.6 26.1 %all-to-all-start.4 = ((bf16[8,64,128]{2,1,0:T(8,128)(2,1)}), bf16[8,64,128]{2,1,0:T(8,128)(2,1)S(1)}, u32[]{:S(2)}, u32[]{:S(2)}) async-start(bf16[8,64,128]{2,1,0:T(8,128)(2,1)} %bitcast.17), calls=%async_computation.4 | async-start | bytes 262144 | tf_op jit(solution)/shard_map/all_to_all | solution.py:333
  261.5 3.1 %collective-permute-start.3 = (bf16[64,128]{1,0:T(8,128)(2,1)S(1)}, bf16[64,128]{1,0:T(8,128)(2,1)S(1)}, u32[]{:S(2)}, u32[]{:S(2)}) collective-permute-start(bf16[64,128]{1,0:T(8,128)(2,1)S(1)} %get-tuple-element.34), channel_id=1, source_target_pairs={{0,1},{1,0},{2,3},{3,2},{4,5},{5,4},{6,7},{7,6},{8,9},{9,8},{10,11... | collective-permute-start | bytes 49160 | tf_op jit(solution)/shard_map/ppermute | solution.py:316

commit v6 on v5

--- a/solution.py
+++ b/solution.py
@@ -16,6 +16,7 @@
 LANE = 128
 EXTRA = 32
 UP = 2.0**18
+TOP = 13.0
 SWAP = [(0, 1), (1, 0)]
 VMEM = pl.BlockSpec(memory_space=pltpu.VMEM)
 
@@ -84,22 +85,21 @@
     return cols
 
 
-def normalize(block, s_ref, got, h_ref, g_ref):
+def columns(got, rows, ref):
+    feats = got.shape[1] - EXTRA
+    for p in range(got.shape[0]):
+        v = got[p, feats : feats + 8, :].astype(F32)
+        ref[p : p + 1, :] = v[rows : rows + 1] + v[rows + 1 : rows + 2] + v[rows + 2 : rows + 3]
+    return jnp.transpose(ref[...])
+
+
+def normalize(block, piece, got, h_ref, g_ref):
     peers = got.shape[0]
     feats = got.shape[1] - EXTRA
     tokens = got.shape[2]
     width = feats * peers
-    for p in range(peers):
-        rows = got[p, feats : feats + 8, :].astype(F32)
-        g_ref[p : p + 1, :] = rows[0:1] + rows[1:2] + rows[2:3]
-    gains = jnp.transpose(g_ref[...])
+    gains = columns(got, 0, g_ref)
     gains = gains[:feats] if block == 0 else gains[feats : 2 * feats]
-
-    def piece(p):
-        if block == 0:
-            return got[p, :feats, :].astype(F32)
-        return s_ref[pl.ds(p * feats, feats), :].astype(F32)
-
     total = jnp.zeros((feats, tokens), F32)
     for p in range(peers):
         v = piece(p)
@@ -135,7 +135,8 @@
 
 
 def first_half_kernel(hid, got, own_ref, h_ref, hd_ref, g_ref):
-    normalize(0, None, got, h_ref, g_ref)
+    feats = got.shape[1] - EXTRA
+    normalize(0, lambda p: got[p, :feats, :].astype(F32), got, h_ref, g_ref)
     hd_ref[...] = hidden_of(hid, 0, own_ref, seat(0), got, h_ref)
 
 
@@ -149,8 +150,20 @@
     down_blocks(hid, own_ref, sib_ref, hd_ref[...], store)
 
 
-def second_block_kernel(hid, s_ref, got, own_ref, sib_ref, out_ref, h_ref, hd_ref, g_ref):
-    normalize(1, s_ref, got, h_ref, g_ref)
+def second_block_kernel(
+    hid, sums, got, own_ref, sib_ref, out_ref, mid_ref, there_ref, s_ref, h_ref, hd_ref, g_ref
+):
+    feats = got.shape[1] - EXTRA
+    scales = columns(got, 3, g_ref)[:feats]
+    for p in range(got.shape[0]):
+        chip, c = divmod(p, CORES)
+        part = sums[chip % SIDE, chip // SIDE, c * feats : (c + 1) * feats, :]
+        mid = got[p, :feats, :].astype(F32) + 0.5 * part * scales[:, p : p + 1]
+        s_ref[pl.ds(p * feats, feats), :] = mid.astype(BF)
+    mine = chip_index() * CORES * feats
+    mid_ref[...] = s_ref[pl.ds(mine, CORES * feats), :]
+    there_ref[...] = s_ref[pl.ds(mine + (1 - lax.axis_index("c")) * feats, feats), :]
+    normalize(1, lambda p: s_ref[pl.ds(p * feats, feats), :].astype(F32), got, h_ref, g_ref)
     hd_ref[:hid, :] = hidden_of(hid, 1, own_ref, seat(0), got, h_ref)
     hd_ref[hid:, :] = hidden_of(hid, 1, sib_ref, seat(1), got, h_ref)
 
@@ -165,22 +178,6 @@
     row = rows[3:4] + rows[4:5] + rows[5:6]
     turned = jnp.transpose(jnp.broadcast_to(row, (8, LANE)))
     return turned[block * feats : (block + 1) * feats, 0:1]
-
-
-def middle_kernel(sums, got, mid_ref, there_ref):
-    feats = got.shape[1] - EXTRA
-    y = chip_index()
-    core = lax.axis_index("c")
-    total = sums[0].astype(F32)
-    for k in range(1, sums.shape[0]):
-        total = total + sums[k].astype(F32)
-    for c in range(CORES):
-        peer = y * CORES + c
-        resid = got[peer, :feats, :].astype(F32)
-        scale = down_column(got, peer, 0, feats)
-        part = total[c * feats : (c + 1) * feats]
-        mid_ref[c * feats : (c + 1) * feats, :] = (resid + 0.5 * part * scale).astype(BF)
-    there_ref[...] = mid_ref[pl.ds((1 - core) * feats, feats), :]
 
 
 def last_kernel(sums, got, mid_ref, other_ref, out_ref):
@@ -203,6 +200,20 @@
     for k in range(1, got.shape[0]):
         total = total + got[k].astype(F32)
     out_ref[...] = total.astype(BF)
+
+
+def scaled_kernel(got, out_ref):
+    far, chip, _ = got.shape[1:]
+    total = got[0].astype(F32)
+    for k in range(1, got.shape[0]):
+        total = total + got[k].astype(F32)
+    top = jnp.max(jnp.max(jnp.abs(total), axis=0), axis=0, keepdims=True)
+    power = jnp.clip(jnp.floor(jnp.log2(top)), -100.0, 120.0)
+    factor = jnp.exp2(TOP - power)
+    for i in range(far):
+        out_ref[i * chip : (i + 1) * chip, :] = total[i] * factor
+    tail = out_ref.shape[0] - far * chip
+    out_ref[far * chip :, :] = jnp.broadcast_to(power, (tail, power.shape[1]))
 
 
 def call(kernel, out, args, scratch=(), flops=1000, limit=4 << 20, space=pltpu.VMEM):
@@ -300,26 +311,33 @@
         limit=16 << 20,
     )
     step = lax.all_to_all(step, "yl", 0, 0, tiled=True)
-    step = call(partial_kernel, jax.ShapeDtypeStruct(step.shape[1:], BF), (step,))
-    step = lax.all_to_all(step, "yh", 0, 0, tiled=True)
+    size = far * chip
+    step = call(scaled_kernel, jax.ShapeDtypeStruct((size + 16, half), F32), (step,))
+    step = step.astype(jnp.float16)
     slices, step = lax.optimization_barrier((slices, step))
     own_2 = jnp.zeros((later.shape[0], groups * share, LANE), BF)
     for r, w in enumerate(slices):
         at = (group + groups - r) % groups * share
         own_2 = lax.dynamic_update_slice_in_dim(own_2, w, at, 1)
     sib_2 = lax.ppermute(own_2, "c", SWAP)
-    middle, there = call(
-        middle_kernel,
-        (jax.ShapeDtypeStruct((chip, half), BF), jax.ShapeDtypeStruct((feats, half), BF)),
-        (step, got),
-    )
-    other = lax.ppermute(there, "c", SWAP)
-    whole = lax.all_gather(middle, ("yh", "yl"), axis=0, tiled=True)
-    step = call(
+    shares = lax.all_gather(step, ("yh", "yl"), axis=0)
+    factor = jnp.exp2(shares[:, size].astype(F32) - TOP)
+    shares, factor = lax.optimization_barrier((shares, factor))
+    sums = 0.0
+    for k in range(far):
+        part = slice(k * SIDE, (k + 1) * SIDE)
+        sums = sums + shares[part, :size].astype(F32) * factor[part, None, :]
+    sums = sums.reshape(SIDE, far, chip, half)
+    step, middle, there = call(
         functools.partial(second_block_kernel, hid),
-        jax.ShapeDtypeStruct((SIDE, far, chip, half), BF),
-        (whole, got, own_2, sib_2),
+        (
+            jax.ShapeDtypeStruct((SIDE, far, chip, half), BF),
+            jax.ShapeDtypeStruct((chip, half), BF),
+            jax.ShapeDtypeStruct((feats, half), BF),
+        ),
+        (sums, got, own_2, sib_2),
         [
+            pltpu.VMEM((width, half), BF),
             pltpu.VMEM((width, half), BF),
             pltpu.VMEM((CORES * hid, half), BF),
             pltpu.VMEM((peers, LANE), F32),
@@ -327,6 +345,7 @@
         flops=12 * hid * width * half,
         limit=16 << 20,
     )
+    other = lax.ppermute(there, "c", SWAP)
     step = lax.all_to_all(step, "yl", 0, 0, tiled=True)
     step = call(partial_kernel, jax.ShapeDtypeStruct(step.shape[1:], BF), (step,))
     step = step.reshape(far * CORES, feats, half)

time: 277 us -> 284 us (1.025)
  blocking collectives: 90.1 us -> 107 us
  starting transfers between devices: 135 us -> 125 us
    all_gather x1, blocking collectives: 22.4 us -> 40.8 us  [blocks(): shares = lax.all_gather(step, ('yh', 'yl'), axis=0)]
    ppermute x1, waiting for transfers between devices: 1.99 us -> 13.5 us  [blocks(): lax.ppermute(later, 'grp', [(i, (i + r) % groups) for i in range(groups)])]
    all_to_all x1 -> x0, starting transfers between devices: 11 us -> none  [blocks(): step = lax.all_to_all(step, 'yh', 0, 0, tiled=True)]
    all_to_all x1 -> x0, waiting for transfers between devices: 10.6 us -> none  [blocks(): step = lax.all_to_all(step, 'yh', 0, 0, tiled=True)]
    pallas_call x8 -> x7, Pallas kernels: 9.74 us -> 9.4 us  [call(): pl.pallas_call(kernel, out_shape=out, in_specs=[pl.BlockSpec(memory_space...]
  transfers between devices with their start and end apart: 8 -> 7, of which waited for: 6 -> 5; matrix products, arithmetic and copies ran while one was open for 0% -> 0% of each run, Pallas kernels for 1% -> 0%
where the time goes in v6:
time: 284 us; the launch traced here: 283 us
  starting transfers between devices  125 us (44%)
  blocking collectives  107 us (38%)
  waiting for transfers between devices  38 us (13%)
  Pallas kernels  9.4 us (3%)
  other arithmetic  3.01 us (1%)
    all_to_all x1, starting transfers between devices, blocks(): got = lax.all_to_all(sent, ('yh', 'yl', 'c'), 0, 0, tiled=True)  87.3 us
    all_gather x1, blocking collectives, blocks(): own = lax.all_gather(own, 'fs', axis=0)  54.8 us
    all_gather x1, blocking collectives, blocks(): shares = lax.all_gather(step, ('yh', 'yl'), axis=0)  40.8 us
    all_to_all x1, starting transfers between devices, blocks(): step = lax.all_to_all(step, ('yh', 'c'), 0, 0, tiled=True)  14.8 us
    ppermute x1, waiting for transfers between devices, blocks(): lax.ppermute(later, 'grp', [(i, (i + r) % groups) for i in range(groups)])  13.5 us
    all_to_all x1, blocking collectives, blocks(): step = lax.all_to_all(step, 'yl', 0, 0, tiled=True)  11.6 us
    all_to_all x1, waiting for transfers between devices, blocks(): step = lax.all_to_all(step, 'yl', 0, 0, tiled=True)  10.5 us
    all_to_all x1, waiting for transfers between devices, blocks(): step = lax.all_to_all(step, ('yh', 'c'), 0, 0, tiled=True)  10.2 us
  transfers between devices with their start and end apart: 7, of which 5 were waited for; matrix products, arithmetic and copies ran while one was open for 0% of the time, Pallas kernels for 0%

profile of v6, /device:TPU:5, one launch (start us, length us, event | category | flops | bytes accessed | tf_op | source)
XLA Modules:
  0.0 283.3 jit_solution(5744656392943932317)
XLA Ops:
  0.0 0.0 copy-start.5
  0.0 0.0 copy-start.4
  0.0 0.0 copy-start.3
  0.0 0.0 copy-start
  0.0 0.0 copy-start.2
  0.0 0.0 copy-start.1
  0.0 1.9 shard_map.145
  1.9 87.3 %all-to-all-start = ((bf16[32,96,128]{2,1,0:T(8,128)(2,1)}), bf16[32,96,128]{2,1,0:T(8,128)(2,1)S(1)}, u32[]{:S(2)}, u32[]{:S(2)}) async-start(bf16[32,96,128]{2,1,0:T(8,128)(2,1)} %shard_map.145), calls=%async_computation | async-start | bytes 1572864 | tf_op jit(solution)/shard_map/all_to_all | solution.py:272
  89.2 0.0 copy-done.5
  89.2 0.0 copy-done.4
  89.2 0.0 copy-done.3
  89.3 0.2 fusion.6
  89.4 0.0 copy-done
  89.4 0.0 copy-done.2
  89.5 0.0 copy-done.1
  89.5 0.1 multiply_convert_fusion.2
  89.5 54.8 %all-gather.3 = f16[16,800,128]{2,1,0:T(8,128)(2,1)} all-gather(f16[1,800,128]{2,1,0:T(8,128)(2,1)S(1)} %multiply_convert_fusion.2), channel_id=1, replica_groups=mesh['grp'=2,'fs'=16,'yh'=4,'yl'=4,'c'=2] {'fs'}, dimensions={0}, use_global_device_ids=true | all-gather | bytes 3481600 | tf_op jit(solution)/shard_map/all_gather | solution.py:281
  144.4 0.0 all-to-all-done.got
  144.4 2.1 multiply_convert_fusion.own_ref
  146.5 0.0 slice-start
  146.5 9.8 %collective-permute-start.1 = (bf16[16,528,128]{2,1,0:T(8,128)(2,1)S(1)}, bf16[16,528,128]{2,1,0:T(8,128)(2,1)S(1)}, u32[]{:S(2)}, u32[]{:S(2)}) collective-permute-start(bf16[16,528,128]{2,1,0:T(8,128)(2,1)S(1)} %multiply_convert_fusion.own_ref), channel_id=1, source_target_pairs={{0,1},{1,0},{2,3},{3,2},{4,5},{5,4},{6,7},{7,6},{8,9},{9,8},{10,11... | collective-permute-start | bytes 6488072 | tf_op jit(solution)/shard_map/ppermute | solution.py:288
  156.3 0.9 shard_map.146
  157.2 0.0 slice-done
  157.2 0.3 multiply_convert_fusion.1
  157.5 2.6 collective-permute-done.1.sib_ref
  160.1 2.6 shard_map.147
  162.8 4.2 %all-to-all-start.1 = ((bf16[4,4,128,128]{3,2,1,0:T(8,128)(2,1)}), bf16[4,4,128,128]{3,2,1,0:T(8,128)(2,1)S(1)}, u32[]{:S(2)}, u32[]{:S(2)}) async-start(bf16[4,4,128,128]{3,2,1,0:T(8,128)(2,1)} %shard_map.147), calls=%async_computation.1 | async-start | bytes 1048576 | tf_op jit(solution)/shard_map/all_to_all | solution.py:313
  166.9 3.6 %collective-permute-start = (bf16[16,272,128]{2,1,0:T(8,128)(2,1)S(1)}, bf16[16,272,128]{2,1,0:T(8,128)(2,1)S(1)}, u32[]{:S(2)}, u32[]{:S(2)}) collective-permute-start(bf16[16,272,128]{2,1,0:T(8,128)(2,1)S(1)} %multiply_convert_fusion.1), channel_id=1, source_target_pairs={{0,512},{512,0},{1,513},{513,1},{2,514},{514,2},{3,515},{515,3},{4... | collective-permute-start | bytes 3342344 | tf_op jit(solution)/shard_map/ppermute | solution.py:301
  170.5 10.5 %all-to-all-done.1.got = bf16[4,4,128,128]{3,2,1,0:T(8,128)(2,1)S(1)} async-done(((bf16[4,4,128,128]{3,2,1,0:T(8,128)(2,1)}), bf16[4,4,128,128]{3,2,1,0:T(8,128)(2,1)S(1)}, u32[]{:S(2)}, u32[]{:S(2)}) %all-to-all-start.1) | async-done | bytes 524320 | tf_op jit(solution)/shard_map/all_to_all | solution.py:313
  181.0 0.1 shard_map.148
  181.1 13.5 %collective-permute-done = bf16[16,272,128]{2,1,0:T(8,128)(2,1)S(1)} collective-permute-done((bf16[16,272,128]{2,1,0:T(8,128)(2,1)S(1)}, bf16[16,272,128]{2,1,0:T(8,128)(2,1)S(1)}, u32[]{:S(2)}, u32[]{:S(2)}) %collective-permute-start) | collective-permute-done | bytes 1114144 | tf_op jit(solution)/shard_map/ppermute | solution.py:301
  194.7 0.3 broadcast_in_dim.39
  195.0 0.2 constant_dynamic-update-slice_fusion.1
  195.1 0.2 constant_dynamic-update-slice_fusion.own_ref
  195.3 3.3 %collective-permute-start.2 = (bf16[16,544,128]{2,1,0:T(8,128)(2,1)S(1)}, bf16[16,544,128]{2,1,0:T(8,128)(2,1)S(1)}, u32[]{:S(2)}, u32[]{:S(2)}) collective-permute-start(bf16[16,544,128]{2,1,0:T(8,128)(2,1)S(1)} %constant_dynamic-update-slice_fusion.own_ref), channel_id=1, source_target_pairs={{0,1},{1,0},{2,3},{3,2},{4,5},{5,4},{6,7},{7,6},{8,9},{9,8},{10,11... | collective-permute-start | bytes 6684680 | tf_op jit(solution)/shard_map/ppermute | solution.py:322
  198.6 40.8 %all-gather.4 = f16[8448,128]{1,0:T(8,128)(2,1)S(1)} all-gather(f16[528,128]{1,0:T(8,128)(2,1)S(1)} %convert_element_type.67), channel_id=2, replica_groups=mesh['grp'=2,'fs'=16,'yh'=4,'yl'=4,'c'=2] {'yh','yl'}, dimensions={0}, use_global_device_ids=true | all-gather | bytes 2297856 | tf_op jit(solution)/shard_map/all_gather | solution.py:323
  239.4 0.4 multiply_add_fusion
  239.8 0.0 collective-permute-done.2.sib_ref
  239.8 2.3 shard_map.149
  242.1 11.6 %all_to_all.20.got = bf16[4,4,128,128]{3,2,1,0:T(8,128)(2,1)S(1)} all-to-all(bf16[4,4,128,128]{3,2,1,0:T(8,128)(2,1)S(1)} %get-tuple-element.38), channel_id=1, replica_groups=mesh['grp'=2,'fs'=16,'yh'=4,'yl'=4,'c'=2] {'yl'}, dimensions={0} | all-to-all | bytes 1048576 | tf_op jit(solution)/shard_map/all_to_all | solution.py:349
  253.7 0.7 shard_map.150
  254.4 14.8 %all-to-all-start.3 = ((bf16[8,64,128]{2,1,0:T(8,128)(2,1)}), bf16[8,64,128]{2,1,0:T(8,128)(2,1)S(1)}, u32[]{:S(2)}, u32[]{:S(2)}) async-start(bf16[8,64,128]{2,1,0:T(8,128)(2,1)} %bitcast.20), calls=%async_computation.3 | async-start | bytes 262144 | tf_op jit(solution)/shard_map/all_to_all | solution.py:352
  269.2 1.9 collective-permute-start.3
  271.2 1.1 collective-permute-done.3.other_ref
  272.3 10.2 %all-to-all-done.3.sums = bf16[8,64,128]{2,1,0:T(8,128)(2,1)S(1)} async-done(((bf16[8,64,128]{2,1,0:T(8,128)(2,1)}), bf16[8,64,128]{2,1,0:T(8,128)(2,1)S(1)}, u32[]{:S(2)}, u32[]{:S(2)}) %all-to-all-start.3) | async-done | bytes 131104 | tf_op jit(solution)/shard_map/all_to_all | solution.py:352
  282.5 0.8 shard_map.151
  (6 shorter events, 0.1 us)
Async XLA Ops:
  0.0 89.2 %copy-start.5 = (f32[128,176]{0,1:T(8,128)S(1)}, f32[128,176]{0,1:T(8,128)}, u32[]{:S(2)}) copy-start(f32[128,176]{0,1:T(8,128)} %param.24) | copy-start | bytes 270340
  0.0 89.2 %copy-start.4 = (f32[128,176]{0,1:T(8,128)S(1)}, f32[128,176]{0,1:T(8,128)}, u32[]{:S(2)}) copy-start(f32[128,176]{0,1:T(8,128)} %param.26) | copy-start | bytes 270340
  0.0 89.2 %copy-start.3 = (f32[176,128]{1,0:T(8,128)S(1)}, f32[176,128]{1,0:T(8,128)}, u32[]{:S(2)}) copy-start(f32[176,128]{1,0:T(8,128)} %param.28) | copy-start | bytes 270340
  0.0 89.4 %copy-start = (f32[176,128]{1,0:T(8,128)S(1)}, f32[176,128]{1,0:T(8,128)}, u32[]{:S(2)}) copy-start(f32[176,128]{1,0:T(8,128)} %param.21) | copy-start | bytes 270340
  0.0 89.4 %copy-start.2 = (f32[128,176]{0,1:T(8,128)S(1)}, f32[128,176]{0,1:T(8,128)}, u32[]{:S(2)}) copy-start(f32[128,176]{0,1:T(8,128)} %param.17) | copy-start | bytes 270340
  0.0 89.4 %copy-start.1 = (f32[128,176]{0,1:T(8,128)S(1)}, f32[128,176]{0,1:T(8,128)}, u32[]{:S(2)}) copy-start(f32[128,176]{0,1:T(8,128)} %param.19) | copy-start | bytes 270340
  1.9 142.4 %all-to-all-start = ((bf16[32,96,128]{2,1,0:T(8,128)(2,1)}), bf16[32,96,128]{2,1,0:T(8,128)(2,1)S(1)}, u32[]{:S(2)}, u32[]{:S(2)}) async-start(bf16[32,96,128]{2,1,0:T(8,128)(2,1)} %shard_map.145), calls=%async_computation | async-start | bytes 1572864 | tf_op jit(solution)/shard_map/all_to_all | solution.py:272
  146.5 10.7 %slice-start = ((f16[16,800,128]{2,1,0:T(8,128)(2,1)}), f16[16,272,128]{2,1,0:T(8,128)(2,1)S(1)}, s32[]{:S(2)}) async-start(f16[16,800,128]{2,1,0:T(8,128)(2,1)} %all-gather.3), calls=%async_computation.4 | async-start | bytes 2228224 | tf_op jit(solution)/shard_map/slice | solution.py:298
  146.5 13.6 %collective-permute-start.1 = (bf16[16,528,128]{2,1,0:T(8,128)(2,1)S(1)}, bf16[16,528,128]{2,1,0:T(8,128)(2,1)S(1)}, u32[]{:S(2)}, u32[]{:S(2)}) collective-permute-start(bf16[16,528,128]{2,1,0:T(8,128)(2,1)S(1)} %multiply_convert_fusion.own_ref), channel_id=1, source_target_pairs={{0,1},{1,0},{2,3},{3,2},{4,5},{5,4},{6,7},{7,6},{8,9},{9,8},{10,11... | collective-permute-start | bytes 6488072 | tf_op jit(solution)/shard_map/ppermute | solution.py:288
  162.8 18.2 %all-to-all-start.1 = ((bf16[4,4,128,128]{3,2,1,0:T(8,128)(2,1)}), bf16[4,4,128,128]{3,2,1,0:T(8,128)(2,1)S(1)}, u32[]{:S(2)}, u32[]{:S(2)}) async-start(bf16[4,4,128,128]{3,2,1,0:T(8,128)(2,1)} %shard_map.147), calls=%async_computation.1 | async-start | bytes 1048576 | tf_op jit(solution)/shard_map/all_to_all | solution.py:313
  166.9 27.7 %collective-permute-start = (bf16[16,272,128]{2,1,0:T(8,128)(2,1)S(1)}, bf16[16,272,128]{2,1,0:T(8,128)(2,1)S(1)}, u32[]{:S(2)}, u32[]{:S(2)}) collective-permute-start(bf16[16,272,128]{2,1,0:T(8,128)(2,1)S(1)} %multiply_convert_fusion.1), channel_id=1, source_target_pairs={{0,512},{512,0},{1,513},{513,1},{2,514},{514,2},{3,515},{515,3},{4... | collective-permute-start | bytes 3342344 | tf_op jit(solution)/shard_map/ppermute | solution.py:301
  195.3 44.5 %collective-permute-start.2 = (bf16[16,544,128]{2,1,0:T(8,128)(2,1)S(1)}, bf16[16,544,128]{2,1,0:T(8,128)(2,1)S(1)}, u32[]{:S(2)}, u32[]{:S(2)}) collective-permute-start(bf16[16,544,128]{2,1,0:T(8,128)(2,1)S(1)} %constant_dynamic-update-slice_fusion.own_ref), channel_id=1, source_target_pairs={{0,1},{1,0},{2,3},{3,2},{4,5},{5,4},{6,7},{7,6},{8,9},{9,8},{10,11... | collective-permute-start | bytes 6684680 | tf_op jit(solution)/shard_map/ppermute | solution.py:322
  254.4 28.1 %all-to-all-start.3 = ((bf16[8,64,128]{2,1,0:T(8,128)(2,1)}), bf16[8,64,128]{2,1,0:T(8,128)(2,1)S(1)}, u32[]{:S(2)}, u32[]{:S(2)}) async-start(bf16[8,64,128]{2,1,0:T(8,128)(2,1)} %bitcast.20), calls=%async_computation.3 | async-start | bytes 262144 | tf_op jit(solution)/shard_map/all_to_all | solution.py:352
  269.2 3.1 %collective-permute-start.3 = (bf16[64,128]{1,0:T(8,128)(2,1)S(1)}, bf16[64,128]{1,0:T(8,128)(2,1)S(1)}, u32[]{:S(2)}, u32[]{:S(2)}) collective-permute-start(bf16[64,128]{1,0:T(8,128)(2,1)S(1)} %get-tuple-element.40), channel_id=1, source_target_pairs={{0,1},{1,0},{2,3},{3,2},{4,5},{5,4},{6,7},{7,6},{8,9},{9,8},{10,11... | collective-permute-start | bytes 49160 | tf_op jit(solution)/shard_map/ppermute | solution.py:348

commit v7 on v6

--- a/solution.py
+++ b/solution.py
@@ -6,7 +6,6 @@
 from jax.experimental import pallas as pl
 from jax.experimental.pallas import tpu as pltpu
 from jax.sharding import Mesh, PartitionSpec as P
-
 
 epsilon = 1e-06
 BF = jnp.bfloat16
@@ -47,7 +46,7 @@
     count = 8
     sources, out_ref = refs[:count], refs[count]
     t_ref, held, ext, sems = refs[count + 1], refs[count + 2 : 2 * count + 2], *refs[-2:]
-    peers, _, half = out_ref.shape
+    peers, rows, half = out_ref.shape
     feats = t_hbm.shape[0]
     copies = [pltpu.make_async_copy(t_hbm, t_ref, sems.at[count])]
     for k in range(count):
@@ -73,7 +72,7 @@
         out_ref[k, feats:, :] = tail
 
 
-def vec_column(got, peer, which, feats, size):
+def vec_column(got, peer, which, feats, col, size):
     rows = got[peer, feats + 8 : feats + EXTRA, :].astype(F32)
     rows = rows[0:8] + rows[8:16] + rows[16:24]
     turned = jnp.transpose(rows)
@@ -112,7 +111,7 @@
 def hidden_of(hid, block, w, peer, got, h_ref):
     feats = got.shape[1] - EXTRA
     chunks, _, lane = w.shape
-    sg, su = vec_column(got, peer, (2 * block, 2 * block + 1), feats, hid)
+    sg, su = vec_column(got, peer, (2 * block, 2 * block + 1), feats, block, hid)
     acc = jnp.zeros((2 * hid, got.shape[2]), F32)
     for z in range(0, chunks, 2):
         lhs = jnp.concatenate([w[z, : 2 * hid, :], w[z + 1, : 2 * hid, :]], axis=1)
@@ -229,7 +228,7 @@
     )(*args)
 
 
-def blocks(
+def body(
     tokens,
     gain_1,
     gate_1,
@@ -246,8 +245,6 @@
     down_2,
     down_s2,
 ):
-    groups = lax.axis_size("grp")
-    group = lax.axis_index("grp")
     far = lax.axis_size("yh")
     peers = far * SIDE * CORES
     mine, feats = tokens.shape
@@ -272,11 +269,7 @@
     got = lax.all_to_all(sent, ("yh", "yl", "c"), 0, 0, tiled=True)
 
     rows = 3 * hid
-    share = -(-rows // (16 * groups)) * 16
-    own_2 = jnp.concatenate([gate_2.T, up_2.T, down_2], axis=0)
-    own_2 = jnp.pad(own_2, ((0, groups * share - rows), (0, 0)))
-    own_2 = lax.dynamic_slice_in_dim(own_2, group * share, share, 0)
-    own = jnp.concatenate([gate_1.T, up_1.T, down_1, own_2], axis=0)
+    own = jnp.concatenate([gate_1.T, up_1.T, down_1, gate_2.T, up_2.T, down_2], axis=0)
     own = (own.astype(BF).astype(F32) * UP).astype(jnp.float16)
     own = lax.all_gather(own, "fs", axis=0)
     own, got = lax.optimization_barrier((own, got))
@@ -295,13 +288,9 @@
         flops=4 * hid * width * half,
         limit=16 << 20,
     )
-    later, h, hd = lax.optimization_barrier((own[:, rows:], h, hd))
-    later = restored(later)
-    slices = [later] + [
-        lax.ppermute(later, "grp", [(i, (i + r) % groups) for i in range(groups)])
-        for r in range(1, groups)
-    ]
-    later, sib_1, h, hd = lax.optimization_barrier((later, sib_1, h, hd))
+    own_2, h, hd = lax.optimization_barrier((own[:, rows:], h, hd))
+    own_2 = restored(own_2)
+    own_2, sib_1, h, hd = lax.optimization_barrier((own_2, sib_1, h, hd))
     step = call(
         functools.partial(second_half_kernel, hid),
         jax.ShapeDtypeStruct((SIDE, far, chip, half), BF),
@@ -314,11 +303,7 @@
     size = far * chip
     step = call(scaled_kernel, jax.ShapeDtypeStruct((size + 16, half), F32), (step,))
     step = step.astype(jnp.float16)
-    slices, step = lax.optimization_barrier((slices, step))
-    own_2 = jnp.zeros((later.shape[0], groups * share, LANE), BF)
-    for r, w in enumerate(slices):
-        at = (group + groups - r) % groups * share
-        own_2 = lax.dynamic_update_slice_in_dim(own_2, w, at, 1)
+    own_2, step = lax.optimization_barrier((own_2, step))
     sib_2 = lax.ppermute(own_2, "c", SWAP)
     shares = lax.all_gather(step, ("yh", "yl"), axis=0)
     factor = jnp.exp2(shares[:, size].astype(F32) - TOP)
@@ -364,5 +349,5 @@
     block = (P(tp), P("fs", tp), P(tp), P("fs", tp), P(tp), P(tp, "fs"), P(tp))
     rows = P(("grp", "fs"), tp)
     return jax.shard_map(
-        blocks, mesh=wide, in_specs=(rows, *block, *block), out_specs=rows, check_vma=False
-    )
+        body, mesh=wide, in_specs=(rows, *block, *block), out_specs=rows, check_vma=False
+    )

time: 284 us -> 274 us (0.965)
  waiting for transfers between devices: 38 us -> 13.1 us
  blocking collectives: 107 us -> 130 us
  starting transfers between devices: 125 us -> 117 us
    all_to_all x1 -> x2, blocking collectives: 11.6 us -> 30.3 us  [body(): step = lax.all_to_all(step, 'yl', 0, 0, tiled=True)]
    ppermute x4 -> x3, waiting for transfers between devices: 17.3 us -> 2.91 us  [the longest x1 1.75 us: body(): sib_1 = lax.ppermute(own_1, 'c', SWAP)]
    all_to_all x3 -> x2, waiting for transfers between devices: 20.7 us -> 10.2 us  [the longest x1 10.2 us: body(): step = lax.all_to_all(step, ('yh', 'c'), 0, 0, tiled=True)]
    ppermute x4 -> x3, starting transfers between devices: 18.5 us -> 13.8 us  [the longest x1 8.52 us: body(): sib_1 = lax.ppermute(own_1, 'c', SWAP)]
    all_gather x2, blocking collectives: 95.6 us -> 99.7 us  [the longest x1 62.5 us: body(): own = lax.all_gather(own, 'fs', axis=0)]
    all_to_all x3 -> x2, starting transfers between devices: 106 us -> 103 us  [the longest x1 87.3 us: body(): got = lax.all_to_all(sent, ('yh', 'yl', 'c'), 0, 0, tiled=True)]
  transfers between devices with their start and end apart: 7 -> 5, of which waited for: 5 -> 3; matrix products, arithmetic and copies ran while one was open for 0% -> 0% of each run, Pallas kernels for 0% -> 0%
where the time goes in v7:
time: 274 us; the launch traced here: 273 us
  blocking collectives  130 us (47%)
  starting transfers between devices  117 us (43%)
  waiting for transfers between devices  13.1 us (5%)
  Pallas kernels  8.62 us (3%)
  other arithmetic  3.17 us (1%)
    all_to_all x1, starting transfers between devices, body(): got = lax.all_to_all(sent, ('yh', 'yl', 'c'), 0, 0, tiled=True)  87.3 us
    all_gather x1, blocking collectives, body(): own = lax.all_gather(own, 'fs', axis=0)  62.5 us
    all_gather x1, blocking collectives, body(): shares = lax.all_gather(step, ('yh', 'yl'), axis=0)  37.3 us
    all_to_all x2, blocking collectives, body(): step = lax.all_to_all(step, 'yl', 0, 0, tiled=True)  30.3 us
    all_to_all x1, starting transfers between devices, body(): step = lax.all_to_all(step, ('yh', 'c'), 0, 0, tiled=True)  16 us
    all_to_all x1, waiting for transfers between devices, body(): step = lax.all_to_all(step, ('yh', 'c'), 0, 0, tiled=True)  10.2 us
    pallas_call x7, Pallas kernels, call(): pl.pallas_call(kernel, out_shape=out, in_specs=[pl.BlockSpec(memory_space...  8.62 us
    ppermute x1, starting transfers between devices, body(): sib_1 = lax.ppermute(own_1, 'c', SWAP)  8.52 us
  transfers between devices with their start and end apart: 5, of which 3 were waited for; matrix products, arithmetic and copies ran while one was open for 0% of the time, Pallas kernels for 0%

profile of v7, /device:TPU:5, one launch (start us, length us, event | category | flops | bytes accessed | tf_op | source)
XLA Modules:
  0.0 272.9 jit_solution(10639745686071034060)
XLA Ops:
  0.0 0.0 copy-start
  0.0 0.0 copy-start.1
  0.0 0.0 copy-start.2
  0.0 0.0 copy-start.3
  0.0 0.0 copy-start.4
  0.0 0.0 copy-start.5
  0.0 1.9 shard_map.145
  1.9 87.3 %all-to-all-start = ((bf16[32,96,128]{2,1,0:T(8,128)(2,1)}), bf16[32,96,128]{2,1,0:T(8,128)(2,1)S(1)}, u32[]{:S(2)}, u32[]{:S(2)}) async-start(bf16[32,96,128]{2,1,0:T(8,128)(2,1)} %shard_map.145), calls=%async_computation | async-start | bytes 1572864 | tf_op jit(solution)/shard_map/all_to_all | solution.py:269
  89.2 0.0 copy-done
  89.2 0.0 copy-done.1
  89.3 0.0 copy-done.2
  89.3 0.0 copy-done.3
  89.3 0.0 copy-done.4
  89.4 0.0 copy-done.5
  89.4 0.1 multiply_convert_fusion.2
  89.5 62.5 %all-gather.3 = f16[16,1056,128]{2,1,0:T(8,128)(2,1)} all-gather(f16[1,1056,128]{2,1,0:T(8,128)(2,1)S(1)} %multiply_convert_fusion.2), channel_id=1, replica_groups=mesh['grp'=2,'fs'=16,'yh'=4,'yl'=4,'c'=2] {'fs'}, dimensions={0}, use_global_device_ids=true | all-gather | bytes 4595712 | tf_op jit(solution)/shard_map/all_gather | solution.py:274
  152.0 0.0 all-to-all-done.got
  152.0 2.1 multiply_convert_fusion.1.own_ref
  154.1 8.5 %collective-permute-start = (bf16[16,528,128]{2,1,0:T(8,128)(2,1)S(1)}, bf16[16,528,128]{2,1,0:T(8,128)(2,1)S(1)}, u32[]{:S(2)}, u32[]{:S(2)}) collective-permute-start(bf16[16,528,128]{2,1,0:T(8,128)(2,1)S(1)} %multiply_convert_fusion.1.own_ref), channel_id=1, source_target_pairs={{0,1},{1,0},{2,3},{3,2},{4,5},{5,4},{6,7},{7,6},{8,9},{9,8},{10,11... | collective-permute-start | bytes 6488072 | tf_op jit(solution)/shard_map/ppermute | solution.py:281
  162.6 0.0 slice-start
  162.6 0.9 shard_map.146
  163.5 0.7 slice-done
  164.2 0.5 multiply_convert_fusion.own_ref
  164.7 1.8 collective-permute-done.sib_ref
  166.5 1.8 shard_map.147
  168.3 18.2 %all_to_all.20.got = bf16[4,4,128,128]{3,2,1,0:T(8,128)(2,1)S(1)} all-to-all(bf16[4,4,128,128]{3,2,1,0:T(8,128)(2,1)S(1)} %shard_map.147), channel_id=1, replica_groups=mesh['grp'=2,'fs'=16,'yh'=4,'yl'=4,'c'=2] {'yl'}, dimensions={0} | all-to-all | bytes 1048576 | tf_op jit(solution)/shard_map/all_to_all | solution.py:302
  186.5 0.1 shard_map.148
  186.6 3.3 %collective-permute-start.1 = (bf16[16,528,128]{2,1,0:T(8,128)(2,1)S(1)}, bf16[16,528,128]{2,1,0:T(8,128)(2,1)S(1)}, u32[]{:S(2)}, u32[]{:S(2)}) collective-permute-start(bf16[16,528,128]{2,1,0:T(8,128)(2,1)S(1)} %multiply_convert_fusion.own_ref), channel_id=1, source_target_pairs={{0,1},{1,0},{2,3},{3,2},{4,5},{5,4},{6,7},{7,6},{8,9},{9,8},{10,11... | collective-permute-start | bytes 6488072 | tf_op jit(solution)/shard_map/ppermute | solution.py:307
  190.0 37.3 %all-gather.4 = f16[8448,128]{1,0:T(8,128)(2,1)S(1)} all-gather(f16[528,128]{1,0:T(8,128)(2,1)S(1)} %convert_element_type.65), channel_id=2, replica_groups=mesh['grp'=2,'fs'=16,'yh'=4,'yl'=4,'c'=2] {'yh','yl'}, dimensions={0}, use_global_device_ids=true | all-gather | bytes 2297856 | tf_op jit(solution)/shard_map/all_gather | solution.py:308
  227.3 0.4 multiply_add_fusion
  227.6 0.0 collective-permute-done.1.sib_ref
  227.7 2.3 shard_map.149
  230.0 12.1 %all_to_all.21.got = bf16[4,4,128,128]{3,2,1,0:T(8,128)(2,1)S(1)} all-to-all(bf16[4,4,128,128]{3,2,1,0:T(8,128)(2,1)S(1)} %get-tuple-element.38), channel_id=1, replica_groups=mesh['grp'=2,'fs'=16,'yh'=4,'yl'=4,'c'=2] {'yl'}, dimensions={0} | all-to-all | bytes 1048576 | tf_op jit(solution)/shard_map/all_to_all | solution.py:334
  242.1 0.7 shard_map.150
  242.8 16.0 %all-to-all-start.3 = ((bf16[8,64,128]{2,1,0:T(8,128)(2,1)}), bf16[8,64,128]{2,1,0:T(8,128)(2,1)S(1)}, u32[]{:S(2)}, u32[]{:S(2)}) async-start(bf16[8,64,128]{2,1,0:T(8,128)(2,1)} %bitcast.22), calls=%async_computation.3 | async-start | bytes 262144 | tf_op jit(solution)/shard_map/all_to_all | solution.py:337
  258.8 1.9 collective-permute-start.2
  260.8 1.1 collective-permute-done.2.other_ref
  261.9 10.2 %all-to-all-done.3.sums = bf16[8,64,128]{2,1,0:T(8,128)(2,1)S(1)} async-done(((bf16[8,64,128]{2,1,0:T(8,128)(2,1)}), bf16[8,64,128]{2,1,0:T(8,128)(2,1)S(1)}, u32[]{:S(2)}, u32[]{:S(2)}) %all-to-all-start.3) | async-done | bytes 131104 | tf_op jit(solution)/shard_map/all_to_all | solution.py:337
  272.1 0.8 shard_map.151
  (10 shorter events, 0.1 us)
Async XLA Ops:
  0.0 89.2 %copy-start = (f32[128,176]{0,1:T(8,128)S(1)}, f32[128,176]{0,1:T(8,128)}, u32[]{:S(2)}) copy-start(f32[128,176]{0,1:T(8,128)} %param.17) | copy-start | bytes 270340
  0.0 89.2 %copy-start.1 = (f32[128,176]{0,1:T(8,128)S(1)}, f32[128,176]{0,1:T(8,128)}, u32[]{:S(2)}) copy-start(f32[128,176]{0,1:T(8,128)} %param.19) | copy-start | bytes 270340
  0.0 89.3 %copy-start.2 = (f32[176,128]{1,0:T(8,128)S(1)}, f32[176,128]{1,0:T(8,128)}, u32[]{:S(2)}) copy-start(f32[176,128]{1,0:T(8,128)} %param.21) | copy-start | bytes 270340
  0.0 89.3 %copy-start.3 = (f32[128,176]{0,1:T(8,128)S(1)}, f32[128,176]{0,1:T(8,128)}, u32[]{:S(2)}) copy-start(f32[128,176]{0,1:T(8,128)} %param.24) | copy-start | bytes 270340
  0.0 89.3 %copy-start.4 = (f32[128,176]{0,1:T(8,128)S(1)}, f32[128,176]{0,1:T(8,128)}, u32[]{:S(2)}) copy-start(f32[128,176]{0,1:T(8,128)} %param.26) | copy-start | bytes 270340
  0.0 89.3 %copy-start.5 = (f32[176,128]{1,0:T(8,128)S(1)}, f32[176,128]{1,0:T(8,128)}, u32[]{:S(2)}) copy-start(f32[176,128]{1,0:T(8,128)} %param.28) | copy-start | bytes 270340
  1.9 150.0 %all-to-all-start = ((bf16[32,96,128]{2,1,0:T(8,128)(2,1)}), bf16[32,96,128]{2,1,0:T(8,128)(2,1)S(1)}, u32[]{:S(2)}, u32[]{:S(2)}) async-start(bf16[32,96,128]{2,1,0:T(8,128)(2,1)} %shard_map.145), calls=%async_computation | async-start | bytes 1572864 | tf_op jit(solution)/shard_map/all_to_all | solution.py:269
  154.1 12.4 %collective-permute-start = (bf16[16,528,128]{2,1,0:T(8,128)(2,1)S(1)}, bf16[16,528,128]{2,1,0:T(8,128)(2,1)S(1)}, u32[]{:S(2)}, u32[]{:S(2)}) collective-permute-start(bf16[16,528,128]{2,1,0:T(8,128)(2,1)S(1)} %multiply_convert_fusion.1.own_ref), channel_id=1, source_target_pairs={{0,1},{1,0},{2,3},{3,2},{4,5},{5,4},{6,7},{7,6},{8,9},{9,8},{10,11... | collective-permute-start | bytes 6488072 | tf_op jit(solution)/shard_map/ppermute | solution.py:281
  162.6 1.6 slice-start
  186.6 41.0 %collective-permute-start.1 = (bf16[16,528,128]{2,1,0:T(8,128)(2,1)S(1)}, bf16[16,528,128]{2,1,0:T(8,128)(2,1)S(1)}, u32[]{:S(2)}, u32[]{:S(2)}) collective-permute-start(bf16[16,528,128]{2,1,0:T(8,128)(2,1)S(1)} %multiply_convert_fusion.own_ref), channel_id=1, source_target_pairs={{0,1},{1,0},{2,3},{3,2},{4,5},{5,4},{6,7},{7,6},{8,9},{9,8},{10,11... | collective-permute-start | bytes 6488072 | tf_op jit(solution)/shard_map/ppermute | solution.py:307
  242.8 29.3 %all-to-all-start.3 = ((bf16[8,64,128]{2,1,0:T(8,128)(2,1)}), bf16[8,64,128]{2,1,0:T(8,128)(2,1)S(1)}, u32[]{:S(2)}, u32[]{:S(2)}) async-start(bf16[8,64,128]{2,1,0:T(8,128)(2,1)} %bitcast.22), calls=%async_computation.3 | async-start | bytes 262144 | tf_op jit(solution)/shard_map/all_to_all | solution.py:337
  258.8 3.1 %collective-permute-start.2 = (bf16[64,128]{1,0:T(8,128)(2,1)S(1)}, bf16[64,128]{1,0:T(8,128)(2,1)S(1)}, u32[]{:S(2)}, u32[]{:S(2)}) collective-permute-start(bf16[64,128]{1,0:T(8,128)(2,1)S(1)} %get-tuple-element.40), channel_id=1, source_target_pairs={{0,1},{1,0},{2,3},{3,2},{4,5},{5,4},{6,7},{7,6},{8,9},{9,8},{10,11... | collective-permute-start | bytes 49160 | tf_op jit(solution)/shard_map/ppermute | solution.py:333

commit v8 on v7

--- a/solution.py
+++ b/solution.py
@@ -14,6 +14,7 @@
 SIDE = 4
 LANE = 128
 EXTRA = 32
+TAIL = 8
 UP = 2.0**18
 TOP = 13.0
 SWAP = [(0, 1), (1, 0)]
@@ -207,6 +208,7 @@
     for k in range(1, got.shape[0]):
         total = total + got[k].astype(F32)
     top = jnp.max(jnp.max(jnp.abs(total), axis=0), axis=0, keepdims=True)
+    top = jnp.maximum(top, 2.0**-100)
     power = jnp.clip(jnp.floor(jnp.log2(top)), -100.0, 120.0)
     factor = jnp.exp2(TOP - power)
     for i in range(far):
@@ -301,7 +303,7 @@
     )
     step = lax.all_to_all(step, "yl", 0, 0, tiled=True)
     size = far * chip
-    step = call(scaled_kernel, jax.ShapeDtypeStruct((size + 16, half), F32), (step,))
+    step = call(scaled_kernel, jax.ShapeDtypeStruct((size + TAIL, half), F32), (step,))
     step = step.astype(jnp.float16)
     own_2, step = lax.optimization_barrier((own_2, step))
     sib_2 = lax.ppermute(own_2, "c", SWAP)

time: 274 us -> 274 us (level)
  no operation moved by 1% of the time
where the time goes in v8:
time: 274 us; the launch traced here: 273 us
  blocking collectives  130 us (47%)
  starting transfers between devices  117 us (43%)
  waiting for transfers between devices  13.1 us (5%)
  Pallas kernels  8.62 us (3%)
  other arithmetic  3.16 us (1%)
    all_to_all x1, starting transfers between devices, body(): got = lax.all_to_all(sent, ('yh', 'yl', 'c'), 0, 0, tiled=True)  87.3 us
    all_gather x1, blocking collectives, body(): own = lax.all_gather(own, 'fs', axis=0)  62.5 us
    all_gather x1, blocking collectives, body(): shares = lax.all_gather(step, ('yh', 'yl'), axis=0)  37 us
    all_to_all x2, blocking collectives, body(): step = lax.all_to_all(step, 'yl', 0, 0, tiled=True)  30.3 us
    all_to_all x1, starting transfers between devices, body(): step = lax.all_to_all(step, ('yh', 'c'), 0, 0, tiled=True)  15.9 us
    all_to_all x1, waiting for transfers between devices, body(): step = lax.all_to_all(step, ('yh', 'c'), 0, 0, tiled=True)  10.2 us
    pallas_call x7, Pallas kernels, call(): pl.pallas_call(kernel, out_shape=out, in_specs=[pl.BlockSpec(memory_space...  8.62 us
    ppermute x1, starting transfers between devices, body(): sib_1 = lax.ppermute(own_1, 'c', SWAP)  8.52 us
  transfers between devices with their start and end apart: 5, of which 3 were waited for; matrix products, arithmetic and copies ran while one was open for 0% of the time, Pallas kernels for 0%

profile of v8, /device:TPU:5, one launch (start us, length us, event | category | flops | bytes accessed | tf_op | source)
XLA Modules:
  0.0 272.5 jit_solution(7335072394736043797)
XLA Ops:
  0.0 0.0 copy-start
  0.0 0.0 copy-start.1
  0.0 0.0 copy-start.2
  0.0 0.0 copy-start.3
  0.0 0.0 copy-start.4
  0.0 0.0 copy-start.5
  0.0 1.9 shard_map.145
  1.9 87.3 %all-to-all-start = ((bf16[32,96,128]{2,1,0:T(8,128)(2,1)}), bf16[32,96,128]{2,1,0:T(8,128)(2,1)S(1)}, u32[]{:S(2)}, u32[]{:S(2)}) async-start(bf16[32,96,128]{2,1,0:T(8,128)(2,1)} %shard_map.145), calls=%async_computation | async-start | bytes 1572864 | tf_op jit(solution)/shard_map/all_to_all | solution.py:271
  89.2 0.0 copy-done
  89.2 0.0 copy-done.1
  89.3 0.0 copy-done.2
  89.3 0.0 copy-done.3
  89.3 0.0 copy-done.4
  89.4 0.0 copy-done.5
  89.4 0.1 multiply_convert_fusion.2
  89.5 62.5 %all-gather.3 = f16[16,1056,128]{2,1,0:T(8,128)(2,1)} all-gather(f16[1,1056,128]{2,1,0:T(8,128)(2,1)S(1)} %multiply_convert_fusion.2), channel_id=1, replica_groups=mesh['grp'=2,'fs'=16,'yh'=4,'yl'=4,'c'=2] {'fs'}, dimensions={0}, use_global_device_ids=true | all-gather | bytes 4595712 | tf_op jit(solution)/shard_map/all_gather | solution.py:276
  152.0 0.0 all-to-all-done.got
  152.0 2.1 multiply_convert_fusion.1.own_ref
  154.1 8.5 %collective-permute-start = (bf16[16,528,128]{2,1,0:T(8,128)(2,1)S(1)}, bf16[16,528,128]{2,1,0:T(8,128)(2,1)S(1)}, u32[]{:S(2)}, u32[]{:S(2)}) collective-permute-start(bf16[16,528,128]{2,1,0:T(8,128)(2,1)S(1)} %multiply_convert_fusion.1.own_ref), channel_id=1, source_target_pairs={{0,1},{1,0},{2,3},{3,2},{4,5},{5,4},{6,7},{7,6},{8,9},{9,8},{10,11... | collective-permute-start | bytes 6488072 | tf_op jit(solution)/shard_map/ppermute | solution.py:283
  162.6 0.0 slice-start
  162.6 0.9 shard_map.146
  163.5 0.7 slice-done
  164.2 0.5 multiply_convert_fusion.own_ref
  164.7 1.8 collective-permute-done.sib_ref
  166.5 1.8 shard_map.147
  168.3 18.2 %all_to_all.20.got = bf16[4,4,128,128]{3,2,1,0:T(8,128)(2,1)S(1)} all-to-all(bf16[4,4,128,128]{3,2,1,0:T(8,128)(2,1)S(1)} %shard_map.147), channel_id=1, replica_groups=mesh['grp'=2,'fs'=16,'yh'=4,'yl'=4,'c'=2] {'yl'}, dimensions={0} | all-to-all | bytes 1048576 | tf_op jit(solution)/shard_map/all_to_all | solution.py:304
  186.5 0.1 shard_map.148
  186.6 3.3 %collective-permute-start.1 = (bf16[16,528,128]{2,1,0:T(8,128)(2,1)S(1)}, bf16[16,528,128]{2,1,0:T(8,128)(2,1)S(1)}, u32[]{:S(2)}, u32[]{:S(2)}) collective-permute-start(bf16[16,528,128]{2,1,0:T(8,128)(2,1)S(1)} %multiply_convert_fusion.own_ref), channel_id=1, source_target_pairs={{0,1},{1,0},{2,3},{3,2},{4,5},{5,4},{6,7},{7,6},{8,9},{9,8},{10,11... | collective-permute-start | bytes 6488072 | tf_op jit(solution)/shard_map/ppermute | solution.py:309
  190.0 37.0 %all-gather.4 = f16[8320,128]{1,0:T(8,128)(2,1)S(1)} all-gather(f16[520,128]{1,0:T(8,128)(2,1)S(1)} %convert_element_type.65), channel_id=2, replica_groups=mesh['grp'=2,'fs'=16,'yh'=4,'yl'=4,'c'=2] {'yh','yl'}, dimensions={0}, use_global_device_ids=true | all-gather | bytes 2263040 | tf_op jit(solution)/shard_map/all_gather | solution.py:310
  226.9 0.4 multiply_add_fusion
  227.3 0.0 collective-permute-done.1.sib_ref
  227.3 2.3 shard_map.149
  229.7 12.1 %all_to_all.21.got = bf16[4,4,128,128]{3,2,1,0:T(8,128)(2,1)S(1)} all-to-all(bf16[4,4,128,128]{3,2,1,0:T(8,128)(2,1)S(1)} %get-tuple-element.38), channel_id=1, replica_groups=mesh['grp'=2,'fs'=16,'yh'=4,'yl'=4,'c'=2] {'yl'}, dimensions={0} | all-to-all | bytes 1048576 | tf_op jit(solution)/shard_map/all_to_all | solution.py:336
  241.8 0.7 shard_map.150
  242.5 15.9 %all-to-all-start.3 = ((bf16[8,64,128]{2,1,0:T(8,128)(2,1)}), bf16[8,64,128]{2,1,0:T(8,128)(2,1)S(1)}, u32[]{:S(2)}, u32[]{:S(2)}) async-start(bf16[8,64,128]{2,1,0:T(8,128)(2,1)} %bitcast.22), calls=%async_computation.3 | async-start | bytes 262144 | tf_op jit(solution)/shard_map/all_to_all | solution.py:339
  258.5 1.9 collective-permute-start.2
  260.4 1.1 collective-permute-done.2.other_ref
  261.6 10.2 %all-to-all-done.3.sums = bf16[8,64,128]{2,1,0:T(8,128)(2,1)S(1)} async-done(((bf16[8,64,128]{2,1,0:T(8,128)(2,1)}), bf16[8,64,128]{2,1,0:T(8,128)(2,1)S(1)}, u32[]{:S(2)}, u32[]{:S(2)}) %all-to-all-start.3) | async-done | bytes 131104 | tf_op jit(solution)/shard_map/all_to_all | solution.py:339
  271.7 0.8 shard_map.151
  (10 shorter events, 0.1 us)
Async XLA Ops:
  0.0 89.2 %copy-start = (f32[128,176]{0,1:T(8,128)S(1)}, f32[128,176]{0,1:T(8,128)}, u32[]{:S(2)}) copy-start(f32[128,176]{0,1:T(8,128)} %param.17) | copy-start | bytes 270340
  0.0 89.2 %copy-start.1 = (f32[128,176]{0,1:T(8,128)S(1)}, f32[128,176]{0,1:T(8,128)}, u32[]{:S(2)}) copy-start(f32[128,176]{0,1:T(8,128)} %param.19) | copy-start | bytes 270340
  0.0 89.3 %copy-start.2 = (f32[176,128]{1,0:T(8,128)S(1)}, f32[176,128]{1,0:T(8,128)}, u32[]{:S(2)}) copy-start(f32[176,128]{1,0:T(8,128)} %param.21) | copy-start | bytes 270340
  0.0 89.3 %copy-start.3 = (f32[128,176]{0,1:T(8,128)S(1)}, f32[128,176]{0,1:T(8,128)}, u32[]{:S(2)}) copy-start(f32[128,176]{0,1:T(8,128)} %param.24) | copy-start | bytes 270340
  0.0 89.3 %copy-start.4 = (f32[128,176]{0,1:T(8,128)S(1)}, f32[128,176]{0,1:T(8,128)}, u32[]{:S(2)}) copy-start(f32[128,176]{0,1:T(8,128)} %param.26) | copy-start | bytes 270340
  0.0 89.3 %copy-start.5 = (f32[176,128]{1,0:T(8,128)S(1)}, f32[176,128]{1,0:T(8,128)}, u32[]{:S(2)}) copy-start(f32[176,128]{1,0:T(8,128)} %param.28) | copy-start | bytes 270340
  1.9 150.0 %all-to-all-start = ((bf16[32,96,128]{2,1,0:T(8,128)(2,1)}), bf16[32,96,128]{2,1,0:T(8,128)(2,1)S(1)}, u32[]{:S(2)}, u32[]{:S(2)}) async-start(bf16[32,96,128]{2,1,0:T(8,128)(2,1)} %shard_map.145), calls=%async_computation | async-start | bytes 1572864 | tf_op jit(solution)/shard_map/all_to_all | solution.py:271
  154.1 12.4 %collective-permute-start = (bf16[16,528,128]{2,1,0:T(8,128)(2,1)S(1)}, bf16[16,528,128]{2,1,0:T(8,128)(2,1)S(1)}, u32[]{:S(2)}, u32[]{:S(2)}) collective-permute-start(bf16[16,528,128]{2,1,0:T(8,128)(2,1)S(1)} %multiply_convert_fusion.1.own_ref), channel_id=1, source_target_pairs={{0,1},{1,0},{2,3},{3,2},{4,5},{5,4},{6,7},{7,6},{8,9},{9,8},{10,11... | collective-permute-start | bytes 6488072 | tf_op jit(solution)/shard_map/ppermute | solution.py:283
  162.6 1.6 slice-start
  186.6 40.7 %collective-permute-start.1 = (bf16[16,528,128]{2,1,0:T(8,128)(2,1)S(1)}, bf16[16,528,128]{2,1,0:T(8,128)(2,1)S(1)}, u32[]{:S(2)}, u32[]{:S(2)}) collective-permute-start(bf16[16,528,128]{2,1,0:T(8,128)(2,1)S(1)} %multiply_convert_fusion.own_ref), channel_id=1, source_target_pairs={{0,1},{1,0},{2,3},{3,2},{4,5},{5,4},{6,7},{7,6},{8,9},{9,8},{10,11... | collective-permute-start | bytes 6488072 | tf_op jit(solution)/shard_map/ppermute | solution.py:309
  242.5 29.2 %all-to-all-start.3 = ((bf16[8,64,128]{2,1,0:T(8,128)(2,1)}), bf16[8,64,128]{2,1,0:T(8,128)(2,1)S(1)}, u32[]{:S(2)}, u32[]{:S(2)}) async-start(bf16[8,64,128]{2,1,0:T(8,128)(2,1)} %bitcast.22), calls=%async_computation.3 | async-start | bytes 262144 | tf_op jit(solution)/shard_map/all_to_all | solution.py:339
  258.5 3.1 %collective-permute-start.2 = (bf16[64,128]{1,0:T(8,128)(2,1)S(1)}, bf16[64,128]{1,0:T(8,128)(2,1)S(1)}, u32[]{:S(2)}, u32[]{:S(2)}) collective-permute-start(bf16[64,128]{1,0:T(8,128)(2,1)S(1)} %get-tuple-element.40), channel_id=1, source_target_pairs={{0,1},{1,0},{2,3},{3,2},{4,5},{5,4},{6,7},{7,6},{8,9},{9,8},{10,11... | collective-permute-start | bytes 49160 | tf_op jit(solution)/shard_map/ppermute | solution.py:335

commit v9 on v8

--- a/solution.py
+++ b/solution.py
@@ -31,9 +31,9 @@
     return lax.axis_index("yh") * SIDE + lax.axis_index("yl")
 
 
-def seat(other):
+def seat(got, other):
     core = lax.axis_index("c")
-    return chip_index() * CORES + (1 - core if other else core)
+    return got.shape[0] - 1 - chip_index() * CORES - (1 - core if other else core)
 
 
 def wide_row(a):
@@ -68,7 +68,7 @@
             ext[at + 1 : at + 2, :] = wide_row(u[:, LANE:])
     tail = ext[...].astype(BF)
     for k in range(peers):
-        c = k % CORES
+        c = (peers - 1 - k) % CORES
         out_ref[k, :feats, :] = t_ref[:, c * half : (c + 1) * half]
         out_ref[k, feats:, :] = tail
 
@@ -88,7 +88,7 @@
 def columns(got, rows, ref):
     feats = got.shape[1] - EXTRA
     for p in range(got.shape[0]):
-        v = got[p, feats : feats + 8, :].astype(F32)
+        v = got[got.shape[0] - 1 - p, feats : feats + 8, :].astype(F32)
         ref[p : p + 1, :] = v[rows : rows + 1] + v[rows + 1 : rows + 2] + v[rows + 2 : rows + 3]
     return jnp.transpose(ref[...])
 
@@ -136,13 +136,14 @@
 
 def first_half_kernel(hid, got, own_ref, h_ref, hd_ref, g_ref):
     feats = got.shape[1] - EXTRA
-    normalize(0, lambda p: got[p, :feats, :].astype(F32), got, h_ref, g_ref)
-    hd_ref[...] = hidden_of(hid, 0, own_ref, seat(0), got, h_ref)
+    last = got.shape[0] - 1
+    normalize(0, lambda p: got[last - p, :feats, :].astype(F32), got, h_ref, g_ref)
+    hd_ref[...] = hidden_of(hid, 0, own_ref, seat(got, 0), got, h_ref)
 
 
 def second_half_kernel(hid, got, h_ref, hd_own, own_ref, sib_ref, out_ref, hd_ref):
     hd_ref[:hid, :] = hd_own[...]
-    hd_ref[hid:, :] = hidden_of(hid, 0, sib_ref, seat(1), got, h_ref)
+    hd_ref[hid:, :] = hidden_of(hid, 0, sib_ref, seat(got, 1), got, h_ref)
 
     def store(z, part):
         out_ref[z % SIDE, z // SIDE] = part
@@ -158,14 +159,14 @@
     for p in range(got.shape[0]):
         chip, c = divmod(p, CORES)
         part = sums[chip % SIDE, chip // SIDE, c * feats : (c + 1) * feats, :]
-        mid = got[p, :feats, :].astype(F32) + 0.5 * part * scales[:, p : p + 1]
+        mid = got[got.shape[0] - 1 - p, :feats, :].astype(F32) + 0.5 * part * scales[:, p : p + 1]
         s_ref[pl.ds(p * feats, feats), :] = mid.astype(BF)
     mine = chip_index() * CORES * feats
     mid_ref[...] = s_ref[pl.ds(mine, CORES * feats), :]
     there_ref[...] = s_ref[pl.ds(mine + (1 - lax.axis_index("c")) * feats, feats), :]
     normalize(1, lambda p: s_ref[pl.ds(p * feats, feats), :].astype(F32), got, h_ref, g_ref)
-    hd_ref[:hid, :] = hidden_of(hid, 1, own_ref, seat(0), got, h_ref)
-    hd_ref[hid:, :] = hidden_of(hid, 1, sib_ref, seat(1), got, h_ref)
+    hd_ref[:hid, :] = hidden_of(hid, 1, own_ref, seat(got, 0), got, h_ref)
+    hd_ref[hid:, :] = hidden_of(hid, 1, sib_ref, seat(got, 1), got, h_ref)
 
     def store(z, part):
         out_ref[z % SIDE, z // SIDE] = part
@@ -184,7 +185,7 @@
     feats = got.shape[1] - EXTRA
     half = got.shape[2]
     core = lax.axis_index("c")
-    scale = down_column(got, seat(0), 1, feats)
+    scale = down_column(got, seat(got, 0), 1, feats)
     here = mid_ref[pl.ds(core * feats, feats), :].astype(F32)
     other = other_ref[...].astype(F32)
     for c in range(CORES):
@@ -268,7 +269,10 @@
         limit=56 << 20,
         space=pltpu.HBM,
     )
-    got = lax.all_to_all(sent, ("yh", "yl", "c"), 0, 0, tiled=True)
+    back = [list(range(peers - 1, -1, -1))]
+    got = lax.all_to_all(
+        sent, ("yh", "yl", "c"), 0, 0, tiled=True, axis_index_groups=back
+    )
 
     rows = 3 * hid
     own = jnp.concatenate([gate_1.T, up_1.T, down_1, gate_2.T, up_2.T, down_2], axis=0)

time: 274 us -> 272 us (level)
  no operation moved by 1% of the time
where the time goes in v9:
time: 272 us; the launch traced here: 271 us
  blocking collectives  129 us (47%)
  starting transfers between devices  117 us (43%)
  waiting for transfers between devices  13.1 us (5%)
  Pallas kernels  8.62 us (3%)
  other arithmetic  3.16 us (1%)
    all_to_all x1, starting transfers between devices, body(): lax.all_to_all(sent, ('yh', 'yl', 'c'), 0, 0, tiled=True, axis_index_grou...  87.9 us
    all_gather x1, blocking collectives, body(): own = lax.all_gather(own, 'fs', axis=0)  62.4 us
    all_gather x1, blocking collectives, body(): shares = lax.all_gather(step, ('yh', 'yl'), axis=0)  36.9 us
    all_to_all x2, blocking collectives, body(): step = lax.all_to_all(step, 'yl', 0, 0, tiled=True)  29.6 us
    all_to_all x1, starting transfers between devices, body(): step = lax.all_to_all(step, ('yh', 'c'), 0, 0, tiled=True)  14.6 us
    all_to_all x1, waiting for transfers between devices, body(): step = lax.all_to_all(step, ('yh', 'c'), 0, 0, tiled=True)  10.2 us
    ppermute x1, starting transfers between devices, body(): sib_1 = lax.ppermute(own_1, 'c', SWAP)  8.83 us
    pallas_call x7, Pallas kernels, call(): pl.pallas_call(kernel, out_shape=out, in_specs=[pl.BlockSpec(memory_space...  8.62 us
  transfers between devices with their start and end apart: 5, of which 3 were waited for; matrix products, arithmetic and copies ran while one was open for 0% of the time, Pallas kernels for 0%

profile of v9, /device:TPU:5, one launch (start us, length us, event | category | flops | bytes accessed | tf_op | source)
XLA Modules:
  0.0 271.4 jit_solution(116011512490597817)
XLA Ops:
  0.0 0.0 copy-start
  0.0 0.0 copy-start.1
  0.0 0.0 copy-start.2
  0.0 0.0 copy-start.3
  0.0 0.0 copy-start.4
  0.0 0.0 copy-start.5
  0.0 1.9 shard_map.145
  1.9 87.9 %all-to-all-start = ((bf16[32,96,128]{2,1,0:T(8,128)(2,1)}), bf16[32,96,128]{2,1,0:T(8,128)(2,1)S(1)}, u32[]{:S(2)}, u32[]{:S(2)}) async-start(bf16[32,96,128]{2,1,0:T(8,128)(2,1)} %shard_map.145), calls=%async_computation | async-start | bytes 1572864 | tf_op jit(solution)/shard_map/all_to_all | solution.py:273
  89.9 0.0 copy-done
  89.9 0.0 copy-done.1
  89.9 0.0 copy-done.2
  90.0 0.0 copy-done.3
  90.0 0.0 copy-done.4
  90.0 0.0 copy-done.5
  90.1 0.1 multiply_convert_fusion.2
  90.1 62.4 %all-gather.3 = f16[16,1056,128]{2,1,0:T(8,128)(2,1)} all-gather(f16[1,1056,128]{2,1,0:T(8,128)(2,1)S(1)} %multiply_convert_fusion.2), channel_id=1, replica_groups=mesh['grp'=2,'fs'=16,'yh'=4,'yl'=4,'c'=2] {'fs'}, dimensions={0}, use_global_device_ids=true | all-gather | bytes 4595712 | tf_op jit(solution)/shard_map/all_gather | solution.py:280
  152.6 0.0 all-to-all-done.got
  152.6 2.1 multiply_convert_fusion.1.own_ref
  154.7 8.8 %collective-permute-start = (bf16[16,528,128]{2,1,0:T(8,128)(2,1)S(1)}, bf16[16,528,128]{2,1,0:T(8,128)(2,1)S(1)}, u32[]{:S(2)}, u32[]{:S(2)}) collective-permute-start(bf16[16,528,128]{2,1,0:T(8,128)(2,1)S(1)} %multiply_convert_fusion.1.own_ref), channel_id=1, source_target_pairs={{0,1},{1,0},{2,3},{3,2},{4,5},{5,4},{6,7},{7,6},{8,9},{9,8},{10,11... | collective-permute-start | bytes 6488072 | tf_op jit(solution)/shard_map/ppermute | solution.py:287
  163.5 0.0 slice-start
  163.5 0.9 shard_map.146
  164.5 0.7 slice-done
  165.1 0.5 multiply_convert_fusion.own_ref
  165.6 1.8 collective-permute-done.sib_ref
  167.4 1.8 shard_map.147
  169.2 18.0 %all_to_all.20.got = bf16[4,4,128,128]{3,2,1,0:T(8,128)(2,1)S(1)} all-to-all(bf16[4,4,128,128]{3,2,1,0:T(8,128)(2,1)S(1)} %shard_map.147), channel_id=1, replica_groups=mesh['grp'=2,'fs'=16,'yh'=4,'yl'=4,'c'=2] {'yl'}, dimensions={0} | all-to-all | bytes 1048576 | tf_op jit(solution)/shard_map/all_to_all | solution.py:308
  187.2 0.1 shard_map.148
  187.4 3.3 %collective-permute-start.1 = (bf16[16,528,128]{2,1,0:T(8,128)(2,1)S(1)}, bf16[16,528,128]{2,1,0:T(8,128)(2,1)S(1)}, u32[]{:S(2)}, u32[]{:S(2)}) collective-permute-start(bf16[16,528,128]{2,1,0:T(8,128)(2,1)S(1)} %multiply_convert_fusion.own_ref), channel_id=1, source_target_pairs={{0,1},{1,0},{2,3},{3,2},{4,5},{5,4},{6,7},{7,6},{8,9},{9,8},{10,11... | collective-permute-start | bytes 6488072 | tf_op jit(solution)/shard_map/ppermute | solution.py:313
  190.7 36.9 %all-gather.4 = f16[8320,128]{1,0:T(8,128)(2,1)S(1)} all-gather(f16[520,128]{1,0:T(8,128)(2,1)S(1)} %convert_element_type.65), channel_id=2, replica_groups=mesh['grp'=2,'fs'=16,'yh'=4,'yl'=4,'c'=2] {'yh','yl'}, dimensions={0}, use_global_device_ids=true | all-gather | bytes 2263040 | tf_op jit(solution)/shard_map/all_gather | solution.py:314
  227.7 0.4 multiply_add_fusion
  228.1 0.0 collective-permute-done.1.sib_ref
  228.1 2.3 shard_map.149
  230.4 11.6 %all_to_all.21.got = bf16[4,4,128,128]{3,2,1,0:T(8,128)(2,1)S(1)} all-to-all(bf16[4,4,128,128]{3,2,1,0:T(8,128)(2,1)S(1)} %get-tuple-element.38), channel_id=1, replica_groups=mesh['grp'=2,'fs'=16,'yh'=4,'yl'=4,'c'=2] {'yl'}, dimensions={0} | all-to-all | bytes 1048576 | tf_op jit(solution)/shard_map/all_to_all | solution.py:340
  242.0 0.7 shard_map.150
  242.7 14.6 %all-to-all-start.3 = ((bf16[8,64,128]{2,1,0:T(8,128)(2,1)}), bf16[8,64,128]{2,1,0:T(8,128)(2,1)S(1)}, u32[]{:S(2)}, u32[]{:S(2)}) async-start(bf16[8,64,128]{2,1,0:T(8,128)(2,1)} %bitcast.22), calls=%async_computation.3 | async-start | bytes 262144 | tf_op jit(solution)/shard_map/all_to_all | solution.py:343
  257.4 1.9 collective-permute-start.2
  259.3 1.1 collective-permute-done.2.other_ref
  260.5 10.2 %all-to-all-done.3.sums = bf16[8,64,128]{2,1,0:T(8,128)(2,1)S(1)} async-done(((bf16[8,64,128]{2,1,0:T(8,128)(2,1)}), bf16[8,64,128]{2,1,0:T(8,128)(2,1)S(1)}, u32[]{:S(2)}, u32[]{:S(2)}) %all-to-all-start.3) | async-done | bytes 131104 | tf_op jit(solution)/shard_map/all_to_all | solution.py:343
  270.7 0.8 shard_map.151
  (10 shorter events, 0.1 us)
Async XLA Ops:
  0.0 89.9 %copy-start = (f32[128,176]{0,1:T(8,128)S(1)}, f32[128,176]{0,1:T(8,128)}, u32[]{:S(2)}) copy-start(f32[128,176]{0,1:T(8,128)} %param.17) | copy-start | bytes 270340
  0.0 89.9 %copy-start.1 = (f32[128,176]{0,1:T(8,128)S(1)}, f32[128,176]{0,1:T(8,128)}, u32[]{:S(2)}) copy-start(f32[128,176]{0,1:T(8,128)} %param.19) | copy-start | bytes 270340
  0.0 89.9 %copy-start.2 = (f32[176,128]{1,0:T(8,128)S(1)}, f32[176,128]{1,0:T(8,128)}, u32[]{:S(2)}) copy-start(f32[176,128]{1,0:T(8,128)} %param.21) | copy-start | bytes 270340
  0.0 90.0 %copy-start.3 = (f32[128,176]{0,1:T(8,128)S(1)}, f32[128,176]{0,1:T(8,128)}, u32[]{:S(2)}) copy-start(f32[128,176]{0,1:T(8,128)} %param.24) | copy-start | bytes 270340
  0.0 90.0 %copy-start.4 = (f32[128,176]{0,1:T(8,128)S(1)}, f32[128,176]{0,1:T(8,128)}, u32[]{:S(2)}) copy-start(f32[128,176]{0,1:T(8,128)} %param.26) | copy-start | bytes 270340
  0.0 90.0 %copy-start.5 = (f32[176,128]{1,0:T(8,128)S(1)}, f32[176,128]{1,0:T(8,128)}, u32[]{:S(2)}) copy-start(f32[176,128]{1,0:T(8,128)} %param.28) | copy-start | bytes 270340
  1.9 150.6 %all-to-all-start = ((bf16[32,96,128]{2,1,0:T(8,128)(2,1)}), bf16[32,96,128]{2,1,0:T(8,128)(2,1)S(1)}, u32[]{:S(2)}, u32[]{:S(2)}) async-start(bf16[32,96,128]{2,1,0:T(8,128)(2,1)} %shard_map.145), calls=%async_computation | async-start | bytes 1572864 | tf_op jit(solution)/shard_map/all_to_all | solution.py:273
  154.7 12.7 %collective-permute-start = (bf16[16,528,128]{2,1,0:T(8,128)(2,1)S(1)}, bf16[16,528,128]{2,1,0:T(8,128)(2,1)S(1)}, u32[]{:S(2)}, u32[]{:S(2)}) collective-permute-start(bf16[16,528,128]{2,1,0:T(8,128)(2,1)S(1)} %multiply_convert_fusion.1.own_ref), channel_id=1, source_target_pairs={{0,1},{1,0},{2,3},{3,2},{4,5},{5,4},{6,7},{7,6},{8,9},{9,8},{10,11... | collective-permute-start | bytes 6488072 | tf_op jit(solution)/shard_map/ppermute | solution.py:287
  163.5 1.6 slice-start
  187.4 40.7 %collective-permute-start.1 = (bf16[16,528,128]{2,1,0:T(8,128)(2,1)S(1)}, bf16[16,528,128]{2,1,0:T(8,128)(2,1)S(1)}, u32[]{:S(2)}, u32[]{:S(2)}) collective-permute-start(bf16[16,528,128]{2,1,0:T(8,128)(2,1)S(1)} %multiply_convert_fusion.own_ref), channel_id=1, source_target_pairs={{0,1},{1,0},{2,3},{3,2},{4,5},{5,4},{6,7},{7,6},{8,9},{9,8},{10,11... | collective-permute-start | bytes 6488072 | tf_op jit(solution)/shard_map/ppermute | solution.py:313
  242.7 27.9 %all-to-all-start.3 = ((bf16[8,64,128]{2,1,0:T(8,128)(2,1)}), bf16[8,64,128]{2,1,0:T(8,128)(2,1)S(1)}, u32[]{:S(2)}, u32[]{:S(2)}) async-start(bf16[8,64,128]{2,1,0:T(8,128)(2,1)} %bitcast.22), calls=%async_computation.3 | async-start | bytes 262144 | tf_op jit(solution)/shard_map/all_to_all | solution.py:343
  257.4 3.1 %collective-permute-start.2 = (bf16[64,128]{1,0:T(8,128)(2,1)S(1)}, bf16[64,128]{1,0:T(8,128)(2,1)S(1)}, u32[]{:S(2)}, u32[]{:S(2)}) collective-permute-start(bf16[64,128]{1,0:T(8,128)(2,1)S(1)} %get-tuple-element.40), channel_id=1, source_target_pairs={{0,1},{1,0},{2,3},{3,2},{4,5},{5,4},{6,7},{7,6},{8,9},{9,8},{10,11... | collective-permute-start | bytes 49160 | tf_op jit(solution)/shard_map/ppermute | solution.py:339

commit v10 on v9

--- a/solution.py
+++ b/solution.py
@@ -6,6 +6,7 @@
 from jax.experimental import pallas as pl
 from jax.experimental.pallas import tpu as pltpu
 from jax.sharding import Mesh, PartitionSpec as P
+
 
 epsilon = 1e-06
 BF = jnp.bfloat16
@@ -47,7 +48,7 @@
     count = 8
     sources, out_ref = refs[:count], refs[count]
     t_ref, held, ext, sems = refs[count + 1], refs[count + 2 : 2 * count + 2], *refs[-2:]
-    peers, rows, half = out_ref.shape
+    peers, _, half = out_ref.shape
     feats = t_hbm.shape[0]
     copies = [pltpu.make_async_copy(t_hbm, t_ref, sems.at[count])]
     for k in range(count):
@@ -73,7 +74,7 @@
         out_ref[k, feats:, :] = tail
 
 
-def vec_column(got, peer, which, feats, col, size):
+def vec_column(got, peer, which, feats, size):
     rows = got[peer, feats + 8 : feats + EXTRA, :].astype(F32)
     rows = rows[0:8] + rows[8:16] + rows[16:24]
     turned = jnp.transpose(rows)
@@ -112,7 +113,7 @@
 def hidden_of(hid, block, w, peer, got, h_ref):
     feats = got.shape[1] - EXTRA
     chunks, _, lane = w.shape
-    sg, su = vec_column(got, peer, (2 * block, 2 * block + 1), feats, block, hid)
+    sg, su = vec_column(got, peer, (2 * block, 2 * block + 1), feats, hid)
     acc = jnp.zeros((2 * hid, got.shape[2]), F32)
     for z in range(0, chunks, 2):
         lhs = jnp.concatenate([w[z, : 2 * hid, :], w[z + 1, : 2 * hid, :]], axis=1)
@@ -231,7 +232,7 @@
     )(*args)
 
 
-def body(
+def blocks(
     tokens,
     gain_1,
     gate_1,
@@ -296,6 +297,7 @@
     )
     own_2, h, hd = lax.optimization_barrier((own[:, rows:], h, hd))
     own_2 = restored(own_2)
+    sib_2 = lax.ppermute(own_2, "c", SWAP)
     own_2, sib_1, h, hd = lax.optimization_barrier((own_2, sib_1, h, hd))
     step = call(
         functools.partial(second_half_kernel, hid),
@@ -309,8 +311,6 @@
     size = far * chip
     step = call(scaled_kernel, jax.ShapeDtypeStruct((size + TAIL, half), F32), (step,))
     step = step.astype(jnp.float16)
-    own_2, step = lax.optimization_barrier((own_2, step))
-    sib_2 = lax.ppermute(own_2, "c", SWAP)
     shares = lax.all_gather(step, ("yh", "yl"), axis=0)
     factor = jnp.exp2(shares[:, size].astype(F32) - TOP)
     shares, factor = lax.optimization_barrier((shares, factor))
@@ -355,5 +355,5 @@
     block = (P(tp), P("fs", tp), P(tp), P("fs", tp), P(tp), P(tp, "fs"), P(tp))
     rows = P(("grp", "fs"), tp)
     return jax.shard_map(
-        body, mesh=wide, in_specs=(rows, *block, *block), out_specs=rows, check_vma=False
-    )
+        blocks, mesh=wide, in_specs=(rows, *block, *block), out_specs=rows, check_vma=False
+    )

time: 272 us -> 272 us (level)
  blocking collectives: 129 us -> 110 us
  waiting for transfers between devices: 13.1 us -> 24.6 us
  starting transfers between devices: 117 us -> 122 us
    all_to_all x2 -> x1, blocking collectives: 29.6 us -> 13.2 us  [blocks(): step = lax.all_to_all(step, 'yl', 0, 0, tiled=True)]
    all_to_all x2 -> x3, waiting for transfers between devices: 10.2 us -> 21.7 us  [the longest x1 11.5 us: blocks(): step = lax.all_to_all(step, 'yl', 0, 0, tiled=True)]
    all_to_all x2 -> x3, starting transfers between devices: 103 us -> 109 us  [the longest x1 87.9 us: blocks(): lax.all_to_all(sent, ('yh', 'yl', 'c'), 0, 0, tiled=True, axis_index_grou...]
    all_gather x2, blocking collectives: 99.4 us -> 96.6 us  [the longest x1 62.4 us: blocks(): own = lax.all_gather(own, 'fs', axis=0)]
  transfers between devices with their start and end apart: 5 -> 6, of which waited for: 3 -> 4; matrix products, arithmetic and copies ran while one was open for 0% -> 0% of each run, Pallas kernels for 0% -> 0%
where the time goes in v10:
time: 272 us; the launch traced here: 271 us
  starting transfers between devices  122 us (45%)
  blocking collectives  110 us (40%)
  waiting for transfers between devices  24.6 us (9%)
  Pallas kernels  10.2 us (4%)
  other arithmetic  3.16 us (1%)
    all_to_all x1, starting transfers between devices, blocks(): lax.all_to_all(sent, ('yh', 'yl', 'c'), 0, 0, tiled=True, axis_index_grou...  87.9 us
    all_gather x1, blocking collectives, blocks(): own = lax.all_gather(own, 'fs', axis=0)  62.4 us
    all_gather x1, blocking collectives, blocks(): shares = lax.all_gather(step, ('yh', 'yl'), axis=0)  34.2 us
    all_to_all x1, starting transfers between devices, blocks(): step = lax.all_to_all(step, ('yh', 'c'), 0, 0, tiled=True)  16.5 us
    all_to_all x1, blocking collectives, blocks(): step = lax.all_to_all(step, 'yl', 0, 0, tiled=True)  13.2 us
    all_to_all x1, waiting for transfers between devices, blocks(): step = lax.all_to_all(step, 'yl', 0, 0, tiled=True)  11.5 us
    pallas_call x7, Pallas kernels, call(): pl.pallas_call(kernel, out_shape=out, in_specs=[pl.BlockSpec(memory_space...  10.2 us
    all_to_all x1, waiting for transfers between devices, blocks(): step = lax.all_to_all(step, ('yh', 'c'), 0, 0, tiled=True)  10.2 us
  transfers between devices with their start and end apart: 6, of which 4 were waited for; matrix products, arithmetic and copies ran while one was open for 0% of the time, Pallas kernels for 0%

profile of v10, /device:TPU:5, one launch (start us, length us, event | category | flops | bytes accessed | tf_op | source)
XLA Modules:
  0.0 271.4 jit_solution(14820356506397290593)
XLA Ops:
  0.0 0.0 copy-start.1
  0.0 0.0 copy-start.2
  0.0 0.0 copy-start.3
  0.0 0.0 copy-start.4
  0.0 0.0 copy-start.5
  0.0 0.0 copy-start.6
  0.0 1.9 shard_map.145
  1.9 87.9 %all-to-all-start = ((bf16[32,96,128]{2,1,0:T(8,128)(2,1)}), bf16[32,96,128]{2,1,0:T(8,128)(2,1)S(1)}, u32[]{:S(2)}, u32[]{:S(2)}) async-start(bf16[32,96,128]{2,1,0:T(8,128)(2,1)} %shard_map.145), calls=%async_computation | async-start | bytes 1572864 | tf_op jit(solution)/shard_map/all_to_all | solution.py:274
  89.9 0.0 copy-done.1
  89.9 0.0 copy-done.2
  89.9 0.0 copy-done.3
  90.0 0.0 copy-done.4
  90.0 0.0 copy-done.5
  90.0 0.0 copy-done.6
  90.1 0.1 multiply_convert_fusion.2
  90.1 62.4 %all-gather.3 = f16[16,1056,128]{2,1,0:T(8,128)(2,1)} all-gather(f16[1,1056,128]{2,1,0:T(8,128)(2,1)S(1)} %multiply_convert_fusion.2), channel_id=1, replica_groups=mesh['grp'=2,'fs'=16,'yh'=4,'yl'=4,'c'=2] {'fs'}, dimensions={0}, use_global_device_ids=true | all-gather | bytes 4595712 | tf_op jit(solution)/shard_map/all_gather | solution.py:281
  152.6 0.0 all-to-all-done.got
  152.6 2.1 multiply_convert_fusion.1.own_ref
  154.7 8.8 %collective-permute-start = (bf16[16,528,128]{2,1,0:T(8,128)(2,1)S(1)}, bf16[16,528,128]{2,1,0:T(8,128)(2,1)S(1)}, u32[]{:S(2)}, u32[]{:S(2)}) collective-permute-start(bf16[16,528,128]{2,1,0:T(8,128)(2,1)S(1)} %multiply_convert_fusion.1.own_ref), channel_id=1, source_target_pairs={{0,1},{1,0},{2,3},{3,2},{4,5},{5,4},{6,7},{7,6},{8,9},{9,8},{10,11... | collective-permute-start | bytes 6488072 | tf_op jit(solution)/shard_map/ppermute | solution.py:288
  163.5 0.0 slice-start
  163.5 0.9 shard_map.146
  164.5 0.7 slice-done
  165.1 0.5 multiply_convert_fusion.own_ref
  165.6 1.8 collective-permute-done.sib_ref
  167.4 1.8 shard_map.147
  169.2 0.0 copy-start
  169.2 0.8 copy-done
  170.0 4.1 %all-to-all-start.1 = ((bf16[4,4,128,128]{3,2,1,0:T(8,128)(2,1)}), bf16[4,4,128,128]{3,2,1,0:T(8,128)(2,1)S(1)}, u32[]{:S(2)}, u32[]{:S(2)}) async-start(bf16[4,4,128,128]{3,2,1,0:T(8,128)(2,1)} %copy-done), calls=%async_computation.1 | async-start | bytes 1048576 | tf_op jit(solution)/shard_map/all_to_all | solution.py:310
  174.2 2.6 collective-permute-start.1
  176.8 11.5 %all-to-all-done.1.got = bf16[4,4,128,128]{3,2,1,0:T(8,128)(2,1)S(1)} async-done(((bf16[4,4,128,128]{3,2,1,0:T(8,128)(2,1)}), bf16[4,4,128,128]{3,2,1,0:T(8,128)(2,1)S(1)}, u32[]{:S(2)}, u32[]{:S(2)}) %all-to-all-start.1) | async-done | bytes 524320 | tf_op jit(solution)/shard_map/all_to_all | solution.py:310
  188.2 0.1 shard_map.148
  188.4 34.2 %all-gather.4 = f16[8320,128]{1,0:T(8,128)(2,1)S(1)} all-gather(f16[520,128]{1,0:T(8,128)(2,1)S(1)} %convert_element_type.65), channel_id=2, replica_groups=mesh['grp'=2,'fs'=16,'yh'=4,'yl'=4,'c'=2] {'yh','yl'}, dimensions={0}, use_global_device_ids=true | all-gather | bytes 2263040 | tf_op jit(solution)/shard_map/all_gather | solution.py:314
  222.6 0.4 multiply_add_fusion
  223.0 0.0 collective-permute-done.1.sib_ref
  223.0 3.9 %shard_map.149 = (bf16[4,4,128,128]{3,2,1,0:T(8,128)(2,1)S(1)}, bf16[128,128]{1,0:T(8,128)(2,1)S(1)}, bf16[64,128]{1,0:T(8,128)(2,1)S(1)}) custom-call(f32[4,4,128,128]{3,2,1,0:T(8,128)S(1)} %bitcast.35, bf16[32,96,128]{2,1,0:T(8,128)(2,1)S(1)} %all-to-all-done.got, bf16[16,528,128]{2,1,0:T(8,128)(2,1)S(1)} %multiply_convert_fusion.own_ref, ...), custom_call_target="tpu_custom_call" | custom-call | flops 553648128 | bytes 1048576 | tf_op jit(solution)/shard_map/pallas_call | solution.py:224
  226.9 13.2 %all_to_all.20.got = bf16[4,4,128,128]{3,2,1,0:T(8,128)(2,1)S(1)} all-to-all(bf16[4,4,128,128]{3,2,1,0:T(8,128)(2,1)S(1)} %get-tuple-element.34), channel_id=1, replica_groups=mesh['grp'=2,'fs'=16,'yh'=4,'yl'=4,'c'=2] {'yl'}, dimensions={0} | all-to-all | bytes 1048576 | tf_op jit(solution)/shard_map/all_to_all | solution.py:340
  240.1 0.7 shard_map.150
  240.8 16.5 %all-to-all-start.3 = ((bf16[8,64,128]{2,1,0:T(8,128)(2,1)}), bf16[8,64,128]{2,1,0:T(8,128)(2,1)S(1)}, u32[]{:S(2)}, u32[]{:S(2)}) async-start(bf16[8,64,128]{2,1,0:T(8,128)(2,1)} %bitcast.22), calls=%async_computation.3 | async-start | bytes 262144 | tf_op jit(solution)/shard_map/all_to_all | solution.py:343
  257.3 1.9 collective-permute-start.2
  259.2 1.1 collective-permute-done.2.other_ref
  260.4 10.2 %all-to-all-done.3.sums = bf16[8,64,128]{2,1,0:T(8,128)(2,1)S(1)} async-done(((bf16[8,64,128]{2,1,0:T(8,128)(2,1)}), bf16[8,64,128]{2,1,0:T(8,128)(2,1)S(1)}, u32[]{:S(2)}, u32[]{:S(2)}) %all-to-all-start.3) | async-done | bytes 131104 | tf_op jit(solution)/shard_map/all_to_all | solution.py:343
  270.6 0.8 shard_map.151
  (10 shorter events, 0.1 us)
Async XLA Ops:
  0.0 89.9 %copy-start.1 = (f32[128,176]{0,1:T(8,128)S(1)}, f32[128,176]{0,1:T(8,128)}, u32[]{:S(2)}) copy-start(f32[128,176]{0,1:T(8,128)} %param.17) | copy-start | bytes 270340
  0.0 89.9 %copy-start.2 = (f32[128,176]{0,1:T(8,128)S(1)}, f32[128,176]{0,1:T(8,128)}, u32[]{:S(2)}) copy-start(f32[128,176]{0,1:T(8,128)} %param.19) | copy-start | bytes 270340
  0.0 89.9 %copy-start.3 = (f32[176,128]{1,0:T(8,128)S(1)}, f32[176,128]{1,0:T(8,128)}, u32[]{:S(2)}) copy-start(f32[176,128]{1,0:T(8,128)} %param.21) | copy-start | bytes 270340
  0.0 90.0 %copy-start.4 = (f32[128,176]{0,1:T(8,128)S(1)}, f32[128,176]{0,1:T(8,128)}, u32[]{:S(2)}) copy-start(f32[128,176]{0,1:T(8,128)} %param.24) | copy-start | bytes 270340
  0.0 90.0 %copy-start.5 = (f32[128,176]{0,1:T(8,128)S(1)}, f32[128,176]{0,1:T(8,128)}, u32[]{:S(2)}) copy-start(f32[128,176]{0,1:T(8,128)} %param.26) | copy-start | bytes 270340
  0.0 90.0 %copy-start.6 = (f32[176,128]{1,0:T(8,128)S(1)}, f32[176,128]{1,0:T(8,128)}, u32[]{:S(2)}) copy-start(f32[176,128]{1,0:T(8,128)} %param.28) | copy-start | bytes 270340
  1.9 150.6 %all-to-all-start = ((bf16[32,96,128]{2,1,0:T(8,128)(2,1)}), bf16[32,96,128]{2,1,0:T(8,128)(2,1)S(1)}, u32[]{:S(2)}, u32[]{:S(2)}) async-start(bf16[32,96,128]{2,1,0:T(8,128)(2,1)} %shard_map.145), calls=%async_computation | async-start | bytes 1572864 | tf_op jit(solution)/shard_map/all_to_all | solution.py:274
  154.7 12.7 %collective-permute-start = (bf16[16,528,128]{2,1,0:T(8,128)(2,1)S(1)}, bf16[16,528,128]{2,1,0:T(8,128)(2,1)S(1)}, u32[]{:S(2)}, u32[]{:S(2)}) collective-permute-start(bf16[16,528,128]{2,1,0:T(8,128)(2,1)S(1)} %multiply_convert_fusion.1.own_ref), channel_id=1, source_target_pairs={{0,1},{1,0},{2,3},{3,2},{4,5},{5,4},{6,7},{7,6},{8,9},{9,8},{10,11... | collective-permute-start | bytes 6488072 | tf_op jit(solution)/shard_map/ppermute | solution.py:288
  163.5 1.6 slice-start
  169.2 0.8 copy-start
  170.0 18.2 %all-to-all-start.1 = ((bf16[4,4,128,128]{3,2,1,0:T(8,128)(2,1)}), bf16[4,4,128,128]{3,2,1,0:T(8,128)(2,1)S(1)}, u32[]{:S(2)}, u32[]{:S(2)}) async-start(bf16[4,4,128,128]{3,2,1,0:T(8,128)(2,1)} %copy-done), calls=%async_computation.1 | async-start | bytes 1048576 | tf_op jit(solution)/shard_map/all_to_all | solution.py:310
  174.2 48.8 %collective-permute-start.1 = (bf16[16,528,128]{2,1,0:T(8,128)(2,1)S(1)}, bf16[16,528,128]{2,1,0:T(8,128)(2,1)}, u32[]{:S(2)}, u32[]{:S(2)}) collective-permute-start(bf16[16,528,128]{2,1,0:T(8,128)(2,1)S(1)} %multiply_convert_fusion.own_ref), channel_id=1, source_target_pairs={{0,1},{1,0},{2,3},{3,2},{4,5},{5,4},{6,7},{7,6},{8,9},{9,8},{10,11... | collective-permute-start | bytes 6488072 | tf_op jit(solution)/shard_map/ppermute | solution.py:300
  240.8 29.8 %all-to-all-start.3 = ((bf16[8,64,128]{2,1,0:T(8,128)(2,1)}), bf16[8,64,128]{2,1,0:T(8,128)(2,1)S(1)}, u32[]{:S(2)}, u32[]{:S(2)}) async-start(bf16[8,64,128]{2,1,0:T(8,128)(2,1)} %bitcast.22), calls=%async_computation.3 | async-start | bytes 262144 | tf_op jit(solution)/shard_map/all_to_all | solution.py:343
  257.3 3.1 %collective-permute-start.2 = (bf16[64,128]{1,0:T(8,128)(2,1)S(1)}, bf16[64,128]{1,0:T(8,128)(2,1)S(1)}, u32[]{:S(2)}, u32[]{:S(2)}) collective-permute-start(bf16[64,128]{1,0:T(8,128)(2,1)S(1)} %get-tuple-element.36), channel_id=1, source_target_pairs={{0,1},{1,0},{2,3},{3,2},{4,5},{5,4},{6,7},{7,6},{8,9},{9,8},{10,11... | collective-permute-start | bytes 49160 | tf_op jit(solution)/shard_map/ppermute | solution.py:339
